TPU v7x, 512 devices: a whole 4x8x8 slice. The times are simulated.
512 devices in a mesh: sp: 64 (over z, y), fs: 4 (over x), tp: 2 (over core).
Axes of the slice: x: 4, y: 8, z: 8, core: 2. Of those that a mesh axis runs over, the one named last changes fastest.
Arguments:
- tokens: bfloat16 [4, 8192, 2048], P('fs', ('sp', 'tp')), may hold values from -6 to 6
- norm_gain: float32 [2048], replicated, may hold values from 0.1 to 1.9
- rec_query: bfloat16 [2048, 512], P('sp', 'tp'), may hold values from -0.125 to 0.125
- rec_input: bfloat16 [2048, 512], P('sp', 'tp'), may hold values from -0.125 to 0.125
- rec_forward: bfloat16 [2048, 512], P('sp', 'tp'), may hold values from -0.125 to 0.125
- rec_backward: bfloat16 [2048, 512], P('sp', 'tp'), may hold values from -0.125 to 0.125
- forget_gap: float32 [2, 512], P(None, 'tp'), may hold values from 0 to 0.06
- log_decay: float32 [4, 2, 4, 8192], P('fs', None, 'tp', 'sp'), may hold values from -0.7 to 0
- rec_gain: float32 [512], P('tp'), may hold values from 0.1 to 1.9
- conv_value: bfloat16 [2048, 512], P('sp', 'tp'), may hold values from -0.125 to 0.125
- conv_gate: bfloat16 [2048, 512], P('sp', 'tp'), may hold values from -0.125 to 0.125
- conv_kernel: bfloat16 [31, 512], P(None, 'tp'), may hold values from -3.1 to 3.1
- conv_gain: float32 [512], P('tp'), may hold values from 0.1 to 1.9
- out_rec: bfloat16 [512, 2048], P('tp', 'sp'), may hold values from -0.1875 to 0.1875
- out_conv: bfloat16 [512, 2048], P('tp', 'sp'), may hold values from -0.1875 to 0.1875
Outputs:
- mixed: bfloat16 [4, 8192, 2048], P('fs', ('sp', 'tp'))
All inputs are finite; a program needn't handle non-finite values.
Results may differ from a plain program's by a relative error of at most 0.017.
Values may be sent and summed in bfloat16 or wider, within the bound.
No kernel may reach another device: no remote copies, remote signals or barrier semaphores. Data moves between devices by JAX's collectives and lax.ppermute only.
A program may use at most 64 MiB of HBM per device.

v0:
```python
import jax
import jax.numpy as jnp
from jax import lax
from jax.sharding import Mesh
from jax.sharding import PartitionSpec as P

KD = 128
VD = 128
BLOCK = 64
SP = ("sp_0", "sp_1")
SP_TP = ("sp_0", "sp_1", "tp")


EPS = 1e-06


def filled_with(x, identity):
    return jax.tree.map(
        lambda a, e: jnp.broadcast_to(jnp.asarray(e, a.dtype), a.shape), x, identity
    )


def prefix_by_axis(x, axes, combine, identity, reverse):
    before = start = filled_with(x, identity)
    running = x
    for axis in reversed(axes):
        size, here = (lax.axis_size(axis), lax.axis_index(axis))
        pieces = jax.tree.map(
            lambda part, kind: lax.all_gather(part.astype(kind), axis),
            running,
            (jnp.bfloat16, jnp.bfloat16),
        )
        inside, running = (start, start)
        for k in reversed(range(size)) if reverse else range(size):
            passed = k > here if reverse else k < here
            running = combine(
                running, jax.tree.map(lambda part, own: part[k].astype(own.dtype), pieces, x)
            )
            inside = jax.tree.map(lambda new, old: jnp.where(passed, new, old), running, inside)
        before = combine(inside, before)
    return before


def padded_2(cells, sides, width):
    for axis, dim in sides:
        count = lax.axis_size(axis)
        ends = count - 1
        head = lax.slice_in_dim(cells, 0, width, axis=dim)
        tail = lax.slice_in_dim(cells, cells.shape[dim] - width, cells.shape[dim], axis=dim)
        cells = jnp.concatenate(
            [
                lax.ppermute(tail, axis, [(i, (i + 1) % count) for i in range(ends)]),
                cells,
                lax.ppermute(head, axis, [((i + 1) % count, i) for i in range(ends)]),
            ],
            axis=dim,
        )
    return cells


def over_pieces(x, axis):
    return lax.all_gather(x, axis).sum(0)


def in_order(tiles, dim):
    tiles = jnp.moveaxis(tiles, 0, dim)
    dims = tiles.shape
    return tiles.reshape(*dims[:dim], dims[dim] * dims[dim + 1], *dims[dim + 2 :])


def sent_to_all(x, axis):
    copies = jnp.broadcast_to(x, (lax.axis_size(axis), *x.shape))
    return lax.all_to_all(copies, axis, split_axis=0, concat_axis=0, tiled=True)


def gathered_copies(x, axis, dim):
    return in_order(sent_to_all(x, axis), dim)


def in_one_piece(arrays, axis, dim, along):
    widths = [a.shape[along] for a in arrays]
    both = jnp.concatenate(arrays, axis=along)
    result = lax.all_gather(both, axis, axis=dim, tiled=True)
    return tuple(jnp.split(result, [sum(widths[:k]) for k in range(1, len(widths))], axis=along))


def cut_along(x, dim, size):
    before, after = (x.shape[:dim], x.shape[dim + 1 :])
    return jnp.moveaxis(x.reshape(*before, size, -1, *after), dim, 0)


def summed_on_arrival(x, axis, dim):
    tiles = cut_along(x, dim, lax.axis_size(axis))
    arrived = lax.all_to_all(tiles, axis, split_axis=0, concat_axis=0, tiled=True)
    return arrived.astype(jnp.float32).sum(axis=0)


def block_pass(queries, key_rows, value_rows, log_gate):
    heads_n, length_n, key_dim = queries.shape
    value_dim = value_rows.shape[-1]
    blocks = length_n // BLOCK

    def split_blocks(tensor):
        return tensor.reshape(heads_n, blocks, BLOCK, tensor.shape[-1]).transpose(1, 0, 2, 3)

    def join_blocks(tensor):
        return tensor.transpose(1, 0, 2, 3).reshape(heads_n, length_n, tensor.shape[-1])

    lower_mask = jnp.tril(jnp.ones((BLOCK, BLOCK), bool))

    def advance(carried, inputs):
        states, offset = carried
        query_b, key_b, value_b, gate_b = inputs
        cumulative = jnp.cumsum(gate_b, axis=1)
        query_g = query_b * jnp.exp(cumulative)
        key_g = key_b * jnp.exp(-cumulative)
        scores = jnp.einsum("htd,hsd->hts", query_g, key_g)
        scores = jnp.where(lower_mask, scores, 0.0)
        result = jnp.einsum("hts,hse->hte", scores, value_b)
        result = result + jnp.einsum("htd,hde->hte", query_g, states)
        last_g = cumulative[:, -1, :]
        weighted = key_b * jnp.exp(last_g[:, None, :] - cumulative)
        states = jnp.exp(last_g)[:, :, None] * states + jnp.einsum(
            "hsd,hse->hde", weighted, value_b
        )
        decayed = query_b * jnp.exp(offset[:, None, :] + cumulative)
        return ((states, offset + last_g), (result, decayed))

    start_state = jnp.zeros((heads_n, key_dim, value_dim), jnp.float32)
    start_offset = jnp.zeros((heads_n, key_dim), jnp.float32)
    inputs = (
        split_blocks(queries),
        split_blocks(key_rows),
        split_blocks(value_rows),
        split_blocks(log_gate),
    )
    final_pair, outputs = lax.scan(advance, (start_state, start_offset), inputs)
    return (join_blocks(outputs[0]), join_blocks(outputs[1]), final_pair[1], final_pair[0])


def chain_combine(first_part, second_part):
    return (
        first_part[0] * second_part[0],
        second_part[0][:, :, None] * first_part[1] + second_part[1],
    )


def recurrence(query_pre, input_pre, forward_pre, backward_pre, forget_gap, log_decay, rec_gain):
    heads_local = log_decay.shape[2]
    row_count = query_pre.shape[0]

    def to_heads(tensor):
        return tensor.astype(jnp.float32).reshape(row_count, heads_local, -1).transpose(1, 0, 2)

    def gate_terms(pre_act, gap_row, decay_row):
        closing = jax.nn.sigmoid(-to_heads(pre_act)) * gap_row.reshape(heads_local, 1, -1)
        return (closing, jnp.log1p(-closing) + decay_row[:, :, None])

    queries = jax.nn.silu(to_heads(query_pre)) * KD ** (-0.5)
    values = to_heads(input_pre)
    keys_fwd, gate_fwd = gate_terms(forward_pre, forget_gap[0], log_decay[0, 0])
    keys_bwd, gate_bwd = gate_terms(backward_pre, forget_gap[1], log_decay[0, 1])
    identity = (
        jnp.ones((heads_local, KD), jnp.float32),
        jnp.zeros((heads_local, KD, VD), jnp.float32),
    )
    local_fwd, decayed_fwd, offset_fwd, state_fwd = block_pass(queries, keys_fwd, values, gate_fwd)
    incoming_fwd = prefix_by_axis(
        (jnp.exp(offset_fwd), state_fwd), SP, chain_combine, identity, False
    )
    forward = local_fwd + jnp.einsum("htd,hde->hte", decayed_fwd, incoming_fwd[1])
    local_bwd, decayed_bwd, offset_bwd, state_bwd = block_pass(
        jnp.flip(queries, 1), jnp.flip(keys_bwd, 1), jnp.flip(values, 1), jnp.flip(gate_bwd, 1)
    )
    incoming_bwd = prefix_by_axis(
        (jnp.exp(offset_bwd), state_bwd), SP, chain_combine, identity, True
    )
    backward = jnp.flip(local_bwd + jnp.einsum("htd,hde->hte", decayed_bwd, incoming_bwd[1]), 1)
    joined = forward + backward
    joined = joined * lax.rsqrt(jnp.mean(joined * joined, axis=-1, keepdims=True) + EPS)
    joined = joined * rec_gain.reshape(heads_local, 1, VD)
    return joined.transpose(1, 0, 2).reshape(row_count, heads_local * VD).astype(jnp.bfloat16)


def convolve(conv_pre, glu_pre, conv_kernel, conv_gain):
    gated = (conv_pre.astype(jnp.float32) * jax.nn.sigmoid(glu_pre.astype(jnp.float32))).astype(
        jnp.bfloat16
    )
    half_width = conv_kernel.shape[0] // 2
    padded = padded_2(gated, ((SP, 0),), half_width)
    convolved = lax.conv_general_dilated(
        padded.astype(jnp.float32)[None],
        conv_kernel.astype(jnp.float32)[:, None, :],
        (1,),
        "VALID",
        dimension_numbers=("NWC", "WIO", "NWC"),
        feature_group_count=gated.shape[1],
    )[0]
    totals = (
        over_pieces(jnp.sum(convolved, axis=-1), "tp"),
        over_pieces(jnp.sum(convolved * convolved, axis=-1), "tp"),
    )
    full_width = convolved.shape[1] * lax.axis_size("tp")
    mean_c = (totals[0] / full_width)[:, None]
    variance = (totals[1] / full_width)[:, None] - mean_c * mean_c
    return jax.nn.silu((convolved - mean_c) * lax.rsqrt(variance + EPS) * conv_gain).astype(
        jnp.bfloat16
    )


def body(
    tokens,
    norm_gain,
    rec_query,
    rec_input,
    rec_forward,
    rec_backward,
    forget_gap,
    log_decay,
    rec_gain,
    conv_value,
    conv_gate,
    conv_kernel,
    conv_gain,
    out_rec,
    out_conv,
):
    row_values = tokens[0].astype(jnp.float32)
    normed = row_values * lax.rsqrt(jnp.mean(row_values * row_values, axis=-1, keepdims=True) + EPS)
    normed = (normed * norm_gain).astype(jnp.bfloat16)
    whole = gathered_copies(normed, "tp", 0)
    row_count = whole.shape[0]
    pieces = in_one_piece(
        (rec_query, rec_input, rec_forward, rec_backward, conv_value, conv_gate), SP, 0, 1
    )
    results = tuple(
        (
            jnp.dot(whole, weight_piece, preferred_element_type=jnp.float32)
            for weight_piece in pieces
        )
    )
    projected = tuple((result.astype(jnp.bfloat16) for result in results))
    rec_out = recurrence(
        projected[0], projected[1], projected[2], projected[3], forget_gap, log_decay, rec_gain
    )
    conv_out = convolve(projected[4], projected[5], conv_kernel, conv_gain)
    both_out = jnp.concatenate([rec_out, conv_out], axis=1)
    out_local = jnp.concatenate([out_rec, out_conv], axis=0)
    full_columns = lax.all_gather(out_local, SP, axis=1, tiled=True)
    own_rows = row_count // lax.axis_size("tp")
    rows_part = lax.slice_in_dim(both_out, 0, own_rows * lax.axis_size("tp"), axis=0)
    mixed = summed_on_arrival(
        jnp.dot(rows_part, full_columns, preferred_element_type=jnp.float32).astype(jnp.bfloat16),
        "tp",
        0,
    ).astype(jnp.bfloat16)
    return mixed[None]


def solution(mesh):
    finer = Mesh(
        mesh.devices.reshape(8, 8, mesh.shape["fs"], mesh.shape["tp"]), ("sp_0", "sp_1", "fs", "tp")
    )
    placed = (
        P("fs", SP_TP, None),
        P(),
        P(SP, "tp"),
        P(SP, "tp"),
        P(SP, "tp"),
        P(SP, "tp"),
        P(None, "tp"),
        P("fs", None, "tp", SP),
        P("tp"),
        P(SP, "tp"),
        P(SP, "tp"),
        P(None, "tp"),
        P("tp"),
        P("tp", SP),
        P("tp", SP),
    )
    return jax.shard_map(
        body, mesh=finer, in_specs=placed, out_specs=P("fs", SP_TP, None), check_vma=False
    )
```

profile of v0, /device:TPU:1, one launch (start us, length us, event | category | flops | bytes accessed | tf_op | source)
XLA Modules:
  0.0 313.2 jit_solution(1878238298609700286)
XLA Ops:
  6.5 0.7 constant_dynamic-update-slice_fusion.5
  7.3 0.7 constant_dynamic-update-slice_fusion.4
  8.0 0.7 constant_dynamic-update-slice_fusion.3
  8.7 0.7 constant_dynamic-update-slice_fusion.2
  9.4 0.7 constant_dynamic-update-slice_fusion.1
  10.1 0.7 constant_dynamic-update-slice_fusion
  10.9 0.6 copy-done.1
  11.5 1.1 fusion.91
  12.6 1.1 fusion.93
  13.7 0.9 broadcast_in_dim.40
  14.6 10.3 %all-to-all-start = ((bf16[2,64,2048]{2,1,0:T(8,128)(2,1)}), bf16[2,64,2048]{2,1,0:T(8,128)(2,1)S(1)}, u32[]{:S(2)}, u32[]{:S(2)}) async-start(bf16[2,64,2048]{2,1,0:T(8,128)(2,1)} %broadcast_in_dim.40), calls=%async_computation | async-start | bytes 1048576 | tf_op jit(solution)/shard_map/all_to_all | solution.py:73
  25.0 1.3 pad_maximum_fusion
  26.5 0.8 fusion.348
  27.2 0.7 slice_bitcast_fusion.33
  27.9 78.6 %all-gather.13.cloned.1.call-done = bf16[2048,1536]{1,0:T(8,128)(2,1)} async-done(((bf16[32,1536]{1,0:T(8,128)(2,1)}), bf16[2048,1536]{1,0:T(8,128)(2,1)}) %all-gather.13.cloned.1.call-update) | async-done | bytes 6291472 | tf_op jit(solution)/shard_map/all_gather | solution.py:83
  106.5 1.5 fusion.77
  108.1 1.5 fusion.79
  109.7 1.5 fusion.75
  111.2 1.5 fusion.84
  112.8 0.1 fusion.185
  113.3 1.7 while.35
  113.4 0.1 reduce_window_sum.28
  113.5 0.3 fusion.381
  113.7 0.1 fusion.382
  113.9 0.2 convolution_add_fusion.9
  114.2 0.1 reduce_window_sum.28
  114.3 0.3 fusion.381
  114.6 0.1 fusion.382
  114.8 0.2 convolution_add_fusion.9
  115.1 11.5 %all-gather.7 = bf16[8,2,128]{2,1,0:T(2,128)(2,1)S(1)} all-gather(bf16[1,2,128]{2,1,0:T(2,128)(2,1)S(1)} %fusion.316), channel_id=4, replica_groups=mesh['sp_0'=8,'sp_1'=8,'fs'=4,'tp'=2] {'sp_1'}, dimensions={0}, use_global_device_ids=true | all-gather | bytes 4608 | tf_op jit(solution)/shard_map/all_gather | solution.py:29
  126.6 12.0 %all_gather.67 = bf16[8,2,128]{2,1,0:T(2,128)(2,1)S(1)} all-gather(bf16[1,2,128]{2,1,0:T(2,128)(2,1)S(1)} %fusion.298), channel_id=1, replica_groups=mesh['sp_0'=8,'sp_1'=8,'fs'=4,'tp'=2] {'sp_0'}, dimensions={0}, use_global_device_ids=true | all-gather | bytes 4608 | tf_op jit(solution)/shard_map/all_gather | solution.py:29
  138.6 1.7 while.34
  138.6 0.1 reduce_window_sum.27
  138.7 0.3 fusion.375
  139.0 0.1 fusion.376
  139.1 0.2 convolution_add_fusion.8
  139.6 0.3 fusion.375
  139.8 0.1 fusion.376
  140.0 0.2 convolution_add_fusion.8
  140.3 20.0 %all-gather.3 = bf16[16,128,128]{2,1,0:T(8,128)(2,1)S(1)} all-gather(bf16[2,128,128]{2,1,0:T(8,128)(2,1)S(1)} %convert_element_type.876), channel_id=5, replica_groups=mesh['sp_0'=8,'sp_1'=8,'fs'=4,'tp'=2] {'sp_1'}, dimensions={0}, use_global_device_ids=true | all-gather | bytes 589824 | tf_op jit(solution)/shard_map/all_gather | solution.py:29
  160.3 0.3 fusion.210
  160.7 21.0 %all_gather.70 = bf16[8,2,128,128]{3,2,1,0:T(8,128)(2,1)S(1)} all-gather(bf16[1,2,128,128]{3,2,1,0:T(8,128)(2,1)S(1)} %fusion.210), channel_id=1, replica_groups=mesh['sp_0'=8,'sp_1'=8,'fs'=4,'tp'=2] {'sp_0'}, dimensions={0}, use_global_device_ids=true | all-gather | bytes 589824 | tf_op jit(solution)/shard_map/all_gather | solution.py:29
  181.8 1.2 convolution_add_fusion.4
  183.0 0.2 rev.20
  183.2 0.1 copy.58
  183.3 1.6 fusion.70
  184.9 1.6 fusion.69
  186.5 1.4 collective-permute-start
  187.8 1.3 collective-permute-start.1
  189.2 14.3 %all-gather.6 = bf16[8,2,128]{2,1,0:T(2,128)(2,1)S(1)} all-gather(bf16[1,2,128]{2,1,0:T(2,128)(2,1)S(1)} %fusion.315), channel_id=2, replica_groups=mesh['sp_0'=8,'sp_1'=8,'fs'=4,'tp'=2] {'sp_1'}, dimensions={0}, use_global_device_ids=true | all-gather | bytes 4608 | tf_op jit(solution)/shard_map/all_gather | solution.py:29
  203.4 11.7 %all_gather.61 = bf16[8,2,128]{2,1,0:T(2,128)(2,1)S(1)} all-gather(bf16[1,2,128]{2,1,0:T(2,128)(2,1)S(1)} %fusion.297), channel_id=1, replica_groups=mesh['sp_0'=8,'sp_1'=8,'fs'=4,'tp'=2] {'sp_0'}, dimensions={0}, use_global_device_ids=true | all-gather | bytes 4608 | tf_op jit(solution)/shard_map/all_gather | solution.py:29
  215.2 18.9 %all-gather.1 = bf16[16,128,128]{2,1,0:T(8,128)(2,1)S(1)} all-gather(bf16[2,128,128]{2,1,0:T(8,128)(2,1)S(1)} %convert_element_type.791), channel_id=3, replica_groups=mesh['sp_0'=8,'sp_1'=8,'fs'=4,'tp'=2] {'sp_1'}, dimensions={0}, use_global_device_ids=true | all-gather | bytes 589824 | tf_op jit(solution)/shard_map/all_gather | solution.py:29
  234.1 0.3 fusion.211
  234.4 19.2 %all_gather.64 = bf16[8,2,128,128]{3,2,1,0:T(8,128)(2,1)S(1)} all-gather(bf16[1,2,128,128]{3,2,1,0:T(8,128)(2,1)S(1)} %fusion.211), channel_id=1, replica_groups=mesh['sp_0'=8,'sp_1'=8,'fs'=4,'tp'=2] {'sp_0'}, dimensions={0}, use_global_device_ids=true | all-gather | bytes 589824 | tf_op jit(solution)/shard_map/all_gather | solution.py:29
  253.6 1.2 multiply_reduce_fusion
  254.9 0.1 copy.73
  255.1 2.2 fusion.349
  257.3 0.1 fusion.159
  257.4 39.5 %all-gather.9 = f32[2,1,128]{2,1,0:T(1,128)S(1)} all-gather(f32[1,1,128]{2,1,0:T(1,128)S(1)} %bitcast.769), channel_id=7, replica_groups=mesh['sp_0'=8,'sp_1'=8,'fs'=4,'tp'=2] {'tp'}, dimensions={0}, use_global_device_ids=true | all-gather | bytes 1536 | tf_op jit(solution)/shard_map/all_gather | solution.py:62
  297.0 1.8 all-gather.8
  298.8 0.1 multiply_convert_fusion
  299.0 2.4 convolution_convert_fusion
  301.4 4.1 %all_to_all.10 = bf16[2,64,2048]{2,1,0:T(8,128)(2,1)S(1)} all-to-all(bf16[2,64,2048]{2,1,0:T(8,128)(2,1)S(1)} %bitcast.748), channel_id=1, replica_groups=mesh['sp_0'=8,'sp_1'=8,'fs'=4,'tp'=2] {'tp'}, dimensions={0} | all-to-all | bytes 1048576 | tf_op jit(solution)/shard_map/all_to_all | solution.py:94
  305.5 0.8 reduce_sum.72
  (74 shorter events, 1.3 us)
Async XLA Ops:
  6.5 248.6 %copy-start = (bf16[31,256]{1,0:T(8,128)(2,1)S(1)}, bf16[31,256]{1,0:T(8,128)(2,1)}, u32[]{:S(2)}) copy-start(bf16[31,256]{1,0:T(8,128)(2,1)} %param.30) | copy-start | bytes 47620
  6.5 100.0 %all-gather.13.cloned.1.call-start = ((), (), s32[]{:S(2)}) async-start(), calls=%async_computation.2 | async-start | bytes 6389760 | tf_op jit(solution)/shard_map/all_gather | solution.py:83
  10.9 0.6 copy-start.1
  14.6 13.3 %all-to-all-start = ((bf16[2,64,2048]{2,1,0:T(8,128)(2,1)}), bf16[2,64,2048]{2,1,0:T(8,128)(2,1)S(1)}, u32[]{:S(2)}, u32[]{:S(2)}) async-start(bf16[2,64,2048]{2,1,0:T(8,128)(2,1)} %broadcast_in_dim.40), calls=%async_computation | async-start | bytes 1048576 | tf_op jit(solution)/shard_map/all_to_all | solution.py:73
  25.0 274.0 %all-gather.15.cloned.1.call-start = ((), (), s32[]{:S(2)}) async-start(), calls=%async_computation.3 | async-start | bytes 2129920 | tf_op jit(solution)/shard_map/all_gather | solution.py:249
  181.8 73.1 %copy-start.2 = (f32[256]{0:T(256)S(1)}, f32[256]{0:T(256)}, u32[]{:S(2)}) copy-start(f32[256]{0:T(256)} %param.27) | copy-start | bytes 3076
  183.3 115.5 %copy-start.3 = (f32[256]{0:T(256)S(1)}, f32[256]{0:T(256)}, u32[]{:S(2)}) copy-start(f32[256]{0:T(256)} %param.31) | copy-start | bytes 3076
  186.5 68.6 %collective-permute-start = (bf16[15,256]{1,0:T(8,128)(2,1)S(1)}, bf16[15,256]{1,0:T(8,128)(2,1)S(1)}, u32[]{:S(2)}, u32[]{:S(2)}) collective-permute-start(bf16[15,256]{1,0:T(8,128)(2,1)S(1)} %get-tuple-element.275), channel_id=1, source_target_pairs={{0,8},{8,16},{16,24},{24,32},{32,40},{40,48},{48,56},{56,64},{64,7... | collective-permute-start | bytes 23048 | tf_op jit(solution)/shard_map/ppermute | solution.py:52
  187.8 67.2 %collective-permute-start.1 = (bf16[15,256]{1,0:T(8,128)(2,1)S(1)}, bf16[15,256]{1,0:T(8,128)(2,1)S(1)}, u32[]{:S(2)}, u32[]{:S(2)}) collective-permute-start(bf16[15,256]{1,0:T(8,128)(2,1)S(1)} %get-tuple-element.276), channel_id=1, source_target_pairs={{8,0},{16,8},{24,16},{32,24},{40,32},{48,40},{56,48},{64,56},{72,6... | collective-permute-start | bytes 23048 | tf_op jit(solution)/shard_map/ppermute | solution.py:54
Sparse Core Ops, SparseCore 0:
  11.7 94.8 all-gather.12
  109.6 77.7 all-gather.14
where the time goes:
time: 314 us; the launch traced here: 313 us
  blocking collectives  174 us (55%)
  waiting for transfers between devices  78.7 us (25%)
  matrix products  18.8 us (6%)
  between operations  13.9 us (4%)
  starting transfers between devices  13 us (4%)
  local copies, waits for them, and re-layouts  8.26 us (3%)
  other arithmetic  6.42 us (2%)
    all_gather x8, blocking collectives, prefix_by_axis(): lax.all_gather(part.astype(kind), axis)  128 us
    all_gather x1, waiting for transfers between devices, in_one_piece(): result = lax.all_gather(both, axis, axis=dim, tiled=True)  78.6 us
    all_gather x2, blocking collectives, over_pieces(): return lax.all_gather(x, axis).sum(0)  41.3 us
    all_to_all x1, starting transfers between devices, sent_to_all(): return lax.all_to_all(copies, axis, split_axis=0, concat_axis=0, tiled=True)  10.3 us
    dot_general x6, matrix products, body(): jnp.dot(whole, weight_piece, preferred_element_type=jnp.float32)  9.27 us
  transfers between devices with their start and end apart: 5, of which 1 were waited for; matrix products, arithmetic and copies ran while one was open for 8% of the time, Pallas kernels for 0%

commit v1 on v0

v1 whole, which is shorter than its diff:
```python
import functools

import jax
import jax.numpy as jnp
from jax import lax
from jax.experimental import pallas as pl
from jax.experimental.pallas import tpu as pltpu
from jax.sharding import Mesh
from jax.sharding import PartitionSpec as P

KD = 128
BLOCK = 64
EPS = 1e-06
Z, Y, X, C = "sp_0", "sp_1", "fs", "tp"
F32, BF16 = jnp.float32, jnp.bfloat16
NN = (((1,), (0,)), ((), ()))
NT = (((1,), (1,)), ((), ()))
TN = (((0,), (0,)), ((), ()))


def dot(a, b, dims):
    return lax.dot_general(a, b, dims, preferred_element_type=F32)


def sigmoid(x):
    return 1.0 / (1.0 + jnp.exp(-x))


def lanes(rows):
    return lax.broadcasted_iota(jnp.int32, (rows, 128), 1)


def triangles():
    r = lax.broadcasted_iota(jnp.int32, (128, 128), 0)
    c = lax.broadcasted_iota(jnp.int32, (128, 128), 1)
    same = (r // BLOCK) == (c // BLOCK)
    return same & (c <= r), same & (c >= r)


def split_dot(mask, x):
    hi = x.astype(BF16)
    lo = (x - hi.astype(F32)).astype(BF16)
    return dot(mask, hi, NN) + dot(mask, lo, NN)


def gate_keys(a, gap):
    return gap * sigmoid(-a)


def states_kernel(
    x_ref, w_ref, ld_ref, gap_ref,
    a_ref, v_ref, c_ref, gated_ref, send_ref, before_ref, offset_ref,
    chunk_s, chunk_t,
):
    step = pl.program_id(0)
    rows = x_ref.shape[0]
    acc = jnp.zeros((rows, 256), F32)
    acc_g = jnp.zeros((rows, 32), F32)
    for k in range(8):
        xk = x_ref[:, 256 * k : 256 * (k + 1)]
        acc += dot(xk, w_ref[k, :256, :], NN)
        acc_g += dot(xk, w_ref[k, 256:, :], NT)
    pre_a = acc[:, :128].astype(BF16)
    pre_v = acc[:, 128:].astype(BF16)
    a_ref[...] = pre_a
    v_ref[...] = pre_v
    glu = acc_g.astype(BF16).astype(F32)
    gated = pre_a.astype(F32)[:, 96:128] * sigmoid(glu)
    gated_ref[...] = gated.astype(BF16)
    lower, upper = triangles()
    lower_f, upper_f = lower.astype(F32), upper.astype(F32)
    lower_b, upper_b = lower_f.astype(BF16), upper_f.astype(BF16)
    lane = lanes(128)
    lane1 = lanes(1)
    for b in range(rows // 128):
        a = pre_a[128 * b : 128 * (b + 1)].astype(F32)
        v = pre_v[128 * b : 128 * (b + 1)]
        k = gate_keys(a, gap_ref[...])
        g = jnp.log1p(-k)
        ld = ld_ref[b]
        cum_f = split_dot(lower_b, g) + jnp.sum(lower_f * ld[0:1], axis=1, keepdims=True)
        cum_b = split_dot(upper_b, g) + jnp.sum(upper_f * ld[1:2], axis=1, keepdims=True)
        cum = jnp.where(lane < 32, cum_f, cum_b)
        c_ref[128 * b : 128 * (b + 1), :] = cum
        for h in range(2):
            part = slice(64 * h, 64 * (h + 1))
            cc = cum[part]
            tot = jnp.where(lane1 < 32, cc[63:64], cc[0:1])
            kd = (k[part] * jnp.exp(tot - cc)).astype(BF16)
            st = dot(v[part], kd, TN)
            packed = st[:64] + pltpu.roll(st[64:], 64, 1)
            tot8 = jnp.broadcast_to(tot, (8, 128))
            tot8 = jnp.where(lanes(8) < 64, tot8, pltpu.roll(tot8, 64, 1))
            idx = step * (rows // 64) + 2 * b + h
            chunk_s[idx] = packed
            chunk_t[idx] = tot8

    @pl.when(step == pl.num_programs(0) - 1)
    def _():
        n = chunk_s.shape[0]
        fwd = (lanes(64) % 64) < 32
        fwd8 = (lanes(8) % 64) < 32
        s = jnp.zeros((64, 128), F32)
        off = jnp.zeros((8, 128), F32)
        befores, offs = [None] * n, [None] * n
        for i in range(n):
            j = n - 1 - i
            befores[i], offs[i] = s, off
            tt = jnp.where(fwd8, chunk_t[i], chunk_t[j])
            sc = jnp.where(fwd, chunk_s[i], chunk_s[j])
            s = s * jnp.exp(tt)[0:1] + sc
            off = off + tt
        for i in range(n):
            j = n - 1 - i
            before_ref[i] = jnp.where(fwd, befores[i], befores[j]).astype(BF16)
            offset_ref[i] = jnp.where(fwd8, offs[i], offs[j])
        dec = jnp.exp(off)[0:1]
        hi = dec.astype(BF16)
        lo = (dec - hi.astype(F32)).astype(BF16)
        row = lax.broadcasted_iota(jnp.int32, (16, 128), 0)
        tail = jnp.where(row == 0, hi.astype(F32), jnp.where(row == 1, lo.astype(F32), 0.0))
        s = s.astype(BF16)
        tail = tail.astype(BF16)
        for i in range(8):
            send_ref[i, :64, :] = s
            send_ref[i, 64:, :] = tail


def local_kernel(a_ref, v_ref, c_ref, gap_ref, before_ref, offset_ref, out_ref, qd_ref):
    lower, upper = triangles()
    lane = lanes(128)
    for b in range(a_ref.shape[0] // 128):
        rows = slice(128 * b, 128 * (b + 1))
        a = a_ref[rows, :].astype(F32)
        v = v_ref[rows, :]
        cum = c_ref[rows, :]
        k = gate_keys(a, gap_ref[...])
        q = a * sigmoid(a) * (KD ** -0.5)
        q = jnp.where(lane < 32, pltpu.roll(q, 64, 1), pltpu.roll(q, 96, 1))
        q = jnp.where(lane < 64, q, 0.0)
        qg = q * jnp.exp(cum)
        kn = (k * jnp.exp(-cum)).astype(BF16)
        qf = jnp.where(lane < 32, qg, 0.0).astype(BF16)
        qb = jnp.where(lane < 32, 0.0, qg).astype(BF16)
        qh = qg.astype(BF16)
        scores = jnp.where(lower, dot(qf, kn, NT), 0.0) + jnp.where(upper, dot(qb, kn, NT), 0.0)
        out = dot(scores.astype(BF16), v, NN)
        for h in range(2):
            part = slice(64 * h, 64 * (h + 1))
            to = slice(128 * b + 64 * h, 128 * b + 64 * (h + 1))
            sb = before_ref[2 * b + h]
            full = jnp.concatenate([sb, pltpu.roll(sb.astype(F32), 64, 1).astype(BF16)], axis=0)
            out_ref[to, :] = out[part] + dot(qh[part], full, NT)
            qd_ref[to, :] = (qg[part] * jnp.exp(offset_ref[2 * b + h][0:1])).astype(BF16)


def conv_kernel_body(g_ref, left_ref, right_ref, w_ref, out_ref, pad):
    n = g_ref.shape[0]
    pad[0:16, :] = left_ref[...].astype(F32)
    pad[16 : 16 + n, :] = g_ref[...].astype(F32)
    pad[16 + n : 32 + n, :] = right_ref[...].astype(F32)
    w = w_ref[...]
    for blk in range(n // 64):
        acc = jnp.zeros((64, 32), F32)
        for j in range(31):
            acc += pad[64 * blk + j + 1 : 64 * blk + j + 65, :] * w[j : j + 1, :]
        out_ref[blk] = jnp.concatenate([acc[16 * q : 16 * (q + 1)] for q in range(4)], axis=1).astype(BF16)


def merge_kernel(z_ref, recv_ref, local_ref, qd_ref, conv_ref, send_ref):
    z = z_ref[0]
    fwd = (lanes(64) % 64) < 32
    fwd1 = (lanes(1) % 64) < 32
    s = jnp.zeros((64, 128), F32)
    for i in range(8):
        j = 7 - i
        sc = jnp.where(fwd, recv_ref[i, :64, :].astype(F32), recv_ref[j, :64, :].astype(F32))
        di = recv_ref[i, 64:80, :].astype(F32)
        dj = recv_ref[j, 64:80, :].astype(F32)
        dec = jnp.where(fwd1, di[0:1] + di[1:2], dj[0:1] + dj[1:2])
        pass_f = jnp.where(i < z, 1, 0)
        pass_b = jnp.where(j > z, 1, 0)
        passed = jnp.where(fwd, pass_f, pass_b) > 0
        s = jnp.where(passed, s * dec + sc, s)
    full = jnp.concatenate([s, pltpu.roll(s, 64, 1)], axis=0).astype(BF16)
    for blk in range(16):
        rows = slice(64 * blk, 64 * (blk + 1))
        out = local_ref[rows, :] + dot(qd_ref[rows, :], full, NT)
        send_ref[blk, :64, :] = out.astype(BF16)
        send_ref[blk, 64:, :] = conv_ref[blk]


def output_kernel(recv_ref, rec_gain_ref, conv_gain_ref, w_ref, out_ref, act):
    @pl.when(pl.program_id(0) == 0)
    def _():
        for c in range(2):
            for h in range(2):
                rec = sum(recv_ref[(4 * h + q) * 2 + c, :64, :].astype(F32) for q in range(4))
                rec = rec * lax.rsqrt(jnp.mean(rec * rec, axis=1, keepdims=True) + EPS)
                rec = rec * rec_gain_ref[2 * c + h : 2 * c + h + 1, :]
                at = 128 * (4 * c + h)
                act[:, at : at + 128] = rec.astype(BF16)
        lane = lanes(16) // 32
        blocks = []
        for c in range(2):
            for m in range(2):
                parts = [recv_ref[(4 * m + q) * 2 + c, 64:80, :].astype(F32) for q in range(4)]
                groups = []
                for g in range(4):
                    value = jnp.zeros((16, 128), F32)
                    for q in range(4):
                        moved = parts[q] if q == g else pltpu.roll(parts[q], (32 * (q - g)) % 128, 1)
                        value = jnp.where(lane == q, moved, value)
                    groups.append(value)
                blocks.append(jnp.concatenate(groups, axis=0))
        total = sum(jnp.sum(b, axis=1, keepdims=True) for b in blocks)
        square = sum(jnp.sum(b * b, axis=1, keepdims=True) for b in blocks)
        mean = total / 512.0
        scale = lax.rsqrt(square / 512.0 - mean * mean + EPS)
        for c in range(2):
            for m in range(2):
                n = 2 * c + m
                y = (blocks[n] - mean) * scale * conv_gain_ref[n : n + 1, :]
                at = 128 * (4 * c + 2 + m)
                act[:, at : at + 128] = (y * sigmoid(y)).astype(BF16)

    acc = jnp.zeros(out_ref.shape, F32)
    for b in range(8):
        acc += dot(act[:, 128 * b : 128 * (b + 1)], w_ref[b], NT)
    out_ref[...] = acc.astype(BF16)


def full(shape):
    return pl.BlockSpec(shape, lambda *_: (0,) * len(shape))


def spec(shape, at):
    return pl.BlockSpec(shape, at)


def body(
    tokens, norm_gain, rec_query, rec_input, rec_forward, rec_backward, forget_gap, log_decay,
    rec_gain, conv_value, conv_gate, conv_kernel, conv_gain, out_rec, out_conv,
):
    y, z, xi = lax.axis_index(Y), lax.axis_index(Z), lax.axis_index(X)

    rows_in = tokens[0].astype(F32)
    normed = rows_in * lax.rsqrt(jnp.mean(rows_in * rows_in, axis=-1, keepdims=True) + EPS)
    normed = (normed * norm_gain).astype(BF16)
    seq = lax.all_gather(normed, (Y, C), axis=0, tiled=True)

    def per_y(w):
        return w.reshape(32, 8, 32).transpose(1, 0, 2)

    values = jnp.repeat(rec_input.reshape(32, 2, 128).transpose(1, 0, 2), 4, axis=0)
    ld = jnp.repeat(log_decay[0].transpose(1, 0, 2), 4, axis=0)
    ld_hi = lax.reduce_precision(ld, 8, 7)
    ld_mid = lax.reduce_precision(ld - ld_hi, 8, 7)
    ld_lo = lax.reduce_precision(ld - ld_hi - ld_mid, 8, 7)
    ld3 = jnp.stack([ld_hi, ld_mid, ld_lo], axis=1).astype(BF16).reshape(8, 24, 32)
    ld3 = jnp.pad(ld3, ((0, 0), (0, 8), (0, 64)))
    outs = jnp.concatenate([out_rec, out_conv], axis=0).reshape(4, 128, 32)
    outs = lax.dynamic_index_in_dim(outs, xi, 0, keepdims=False).T
    first = jnp.concatenate(
        [
            per_y(rec_forward), per_y(rec_backward), per_y(rec_query), per_y(conv_value), values,
            per_y(conv_gate), ld3, jnp.broadcast_to(outs, (8, 32, 128)),
        ],
        axis=2,
    )
    first = lax.all_to_all(first, Y, split_axis=0, concat_axis=0, tiled=True)
    main = first[:, :, :256].reshape(256, 256)
    gate_t = first[:, :, 256:288].reshape(256, 32).T
    decays = first[:, :24, 288:320].astype(F32).reshape(8, 3, 2, 128).sum(axis=1)
    out_cols = first[:, :, 384:].reshape(256, 128)
    second = jnp.broadcast_to(jnp.concatenate([main, gate_t], axis=0), (8, 288, 256))
    weights = lax.all_to_all(second, Z, split_axis=0, concat_axis=0, tiled=True)
    out_w = lax.all_gather(out_cols, Z, axis=0, tiled=True)
    out_w = lax.all_gather(out_w, (C, X), axis=0)

    gains = lax.all_gather(jnp.stack([rec_gain, conv_gain]), C)
    rec_gains = gains[:, 0].reshape(4, 128)
    conv_gains = gains[:, 1].reshape(4, 128)
    gap = lax.dynamic_index_in_dim(forget_gap.reshape(2, 8, 32), y, 1, keepdims=False)
    gap = jnp.pad(gap.reshape(1, 64), ((0, 0), (0, 64)))
    taps = lax.dynamic_index_in_dim(conv_kernel.reshape(31, 8, 32), y, 1, keepdims=False)
    taps = jnp.pad(taps.astype(F32), ((0, 1), (0, 0)))

    n = seq.shape[0]
    tile = 256
    pre_a, pre_v, cum, gated, sent, before, offset = pl.pallas_call(
        states_kernel,
        grid=(n // tile,),
        in_specs=[
            spec((tile, 2048), lambda i: (i, 0)),
            full((8, 288, 256)),
            spec((tile // 128, 2, 128), lambda i: (i, 0, 0)),
            full((1, 128)),
        ],
        out_specs=[
            spec((tile, 128), lambda i: (i, 0)),
            spec((tile, 128), lambda i: (i, 0)),
            spec((tile, 128), lambda i: (i, 0)),
            spec((tile, 32), lambda i: (i, 0)),
            full((8, 80, 128)),
            full((16, 64, 128)),
            full((16, 8, 128)),
        ],
        out_shape=[
            jax.ShapeDtypeStruct((n, 128), BF16),
            jax.ShapeDtypeStruct((n, 128), BF16),
            jax.ShapeDtypeStruct((n, 128), F32),
            jax.ShapeDtypeStruct((n, 32), BF16),
            jax.ShapeDtypeStruct((8, 80, 128), BF16),
            jax.ShapeDtypeStruct((16, 64, 128), BF16),
            jax.ShapeDtypeStruct((16, 8, 128), F32),
        ],
        scratch_shapes=[pltpu.VMEM((16, 64, 128), F32), pltpu.VMEM((16, 8, 128), F32)],
        name="states",
    )(seq, weights, decays, gap)

    arrived = lax.all_to_all(sent, Z, split_axis=0, concat_axis=0, tiled=True)
    left = lax.ppermute(gated[n - 16 :], Z, [(i, i + 1) for i in range(7)])
    right = lax.ppermute(gated[:16], Z, [(i + 1, i) for i in range(7)])
    local, decayed = pl.pallas_call(
        local_kernel,
        out_shape=[jax.ShapeDtypeStruct((n, 128), F32), jax.ShapeDtypeStruct((n, 128), BF16)],
        name="local",
    )(pre_a, pre_v, cum, gap, before, offset)
    convolved = pl.pallas_call(
        conv_kernel_body,
        out_shape=jax.ShapeDtypeStruct((16, 16, 128), BF16),
        scratch_shapes=[pltpu.VMEM((n + 32, 32), F32)],
        name="conv",
    )(gated, left, right, taps)
    merged = pl.pallas_call(
        merge_kernel,
        in_specs=[pl.BlockSpec(memory_space=pltpu.SMEM)]
        + [pl.BlockSpec(memory_space=pltpu.VMEM)] * 4,
        out_shape=jax.ShapeDtypeStruct((16, 80, 128), BF16),
        name="merge",
    )(z.reshape(1).astype(jnp.int32), arrived, local, decayed, convolved)
    mine = lax.all_to_all(merged, (Y, C), split_axis=0, concat_axis=0, tiled=True)
    mixed = pl.pallas_call(
        output_kernel,
        grid=(4,),
        in_specs=[
            full((16, 80, 128)), full((4, 128)), full((4, 128)),
            spec((8, 512, 128), lambda i: (0, i, 0)),
        ],
        out_specs=spec((64, 512), lambda i: (0, i)),
        out_shape=jax.ShapeDtypeStruct((64, 2048), BF16),
        scratch_shapes=[pltpu.VMEM((64, 1024), BF16)],
        name="output",
    )(mine, rec_gains, conv_gains, out_w)
    return mixed[None]


def solution(mesh):
    finer = Mesh(
        mesh.devices.reshape(8, 8, mesh.shape["fs"], mesh.shape["tp"]), (Z, Y, X, C)
    )
    sp, sp_tp = (Z, Y), (Z, Y, C)
    row = P(sp, C)
    placed = (
        P(X, sp_tp, None), P(), row, row, row, row, P(None, C), P(X, None, C, sp), P(C),
        row, row, P(None, C), P(C), P(C, sp), P(C, sp),
    )
    return jax.shard_map(
        body, mesh=finer, in_specs=placed, out_specs=P(X, sp_tp, None), check_vma=False
    )
```

time: 314 us -> 165 us (0.53)
  blocking collectives: 174 us -> 52.8 us
  waiting for transfers between devices: 78.7 us -> 36.5 us
  Pallas kernels: 0 us -> 21.9 us
  matrix products: 18.8 us -> 0 us
  starting transfers between devices: 13 us -> 20.4 us
  local copies, waits for them, and re-layouts: 8.26 us -> 13.2 us
    all_gather x10 -> x2, blocking collectives: 170 us -> 35.8 us  [the longest x1 34 us: body(): out_w = lax.all_gather(out_cols, Z, axis=0, tiled=True)]
    all_gather x2, waiting for transfers between devices: 78.6 us -> 0.01 us  [the longest x1 0.01 us: body(): seq = lax.all_gather(normed, (Y, C), axis=0, tiled=True)]
    all_to_all x1 -> x3, waiting for transfers between devices: 0.01 us -> 36.5 us  [the longest x1 25.7 us: body(): weights = lax.all_to_all(second, Z, split_axis=0, concat_axis=0, tiled=True)]
    pallas_call x0 -> x5, Pallas kernels: none -> 21.9 us  [the longest x1 8.09 us: body(): pl.pallas_call(states_kernel, grid=(n // tile,), in_specs=[spec((tile, 20...]
    dot_general x21 -> x0, matrix products: 16.6 us -> none  [the longest x6 9.27 us: body(): jnp.dot(whole, weight_piece, preferred_element_type=jnp.float32)]
    all_to_all x1, blocking collectives: 4.12 us -> 17 us  [body(): first = lax.all_to_all(first, Y, split_axis=0, concat_axis=0, tiled=True)]
    all_to_all x1 -> x3, starting transfers between devices: 10.3 us -> 15.8 us  [the longest x1 8.84 us: body(): lax.all_to_all(merged, (Y, C), split_axis=0, concat_axis=0, tiled=True)]
    reshape x2 -> x12, local copies, waits for them, and re-layouts: 0.2 us -> 5.29 us  [the longest x5 4.12 us: per_y(): return w.reshape(32, 8, 32).transpose(1, 0, 2)]
  transfers between devices with their start and end apart: 5 -> 7, of which waited for: 1 -> 2; matrix products, arithmetic and copies ran while one was open for 8% -> 7% of each run, Pallas kernels for 0% -> 10%
where the time goes in v1:
time: 165 us; the launch traced here: 164 us
  blocking collectives  52.8 us (32%)
  waiting for transfers between devices  36.5 us (22%)
  Pallas kernels  21.9 us (13%)
  starting transfers between devices  20.4 us (12%)
  between operations  13.7 us (8%)
  local copies, waits for them, and re-layouts  13.2 us (8%)
  other arithmetic  4.98 us (3%)
    all_gather x1, blocking collectives, body(): out_w = lax.all_gather(out_cols, Z, axis=0, tiled=True)  34 us
    all_to_all x1, waiting for transfers between devices, body(): weights = lax.all_to_all(second, Z, split_axis=0, concat_axis=0, tiled=True)  25.7 us
    all_to_all x1, blocking collectives, body(): first = lax.all_to_all(first, Y, split_axis=0, concat_axis=0, tiled=True)  17 us
    all_to_all x1, waiting for transfers between devices, body(): lax.all_to_all(merged, (Y, C), split_axis=0, concat_axis=0, tiled=True)  10.8 us
    all_to_all x1, starting transfers between devices, body(): lax.all_to_all(merged, (Y, C), split_axis=0, concat_axis=0, tiled=True)  8.84 us
    pallas_call x1, Pallas kernels, body(): pl.pallas_call(states_kernel, grid=(n // tile,), in_specs=[spec((tile, 20...  8.09 us
    pallas_call x1, Pallas kernels, body(): pl.pallas_call(output_kernel, grid=(4,), in_specs=[full((16, 80, 128)), f...  5.14 us
    reshape x5, local copies, waits for them, and re-layouts, per_y(): return w.reshape(32, 8, 32).transpose(1, 0, 2)  4.12 us
  transfers between devices with their start and end apart: 7, of which 2 were waited for; matrix products, arithmetic and copies ran while one was open for 7% of the time, Pallas kernels for 10%

profile of v1, /device:TPU:1, one launch (start us, length us, event | category | flops | bytes accessed | tf_op | source)
XLA Modules:
  0.0 163.6 jit_solution(1035643101914612442)
XLA Ops:
  6.5 0.0 all-gather.6.cloned.1.call-start
  6.5 1.1 fusion
  7.7 1.8 %fusion.2 = bf16[64,2048]{1,0:T(8,128)(2,1)} fusion(bf16[1,64,2048]{2,1,0:T(8,128)(2,1)} %param.15, f32[2048]{0:T(1024)} %param.16, f32[64]{0:T(128)S(1)} %add_rsqrt_fusion), kind=kLoop, calls=%fused_computation.4 | loop fusion | flops 524288 | bytes 532736 | tf_op jit(solution)/shard_map/convert_element_type | solution.py:249
  9.4 0.0 all-gather.6.cloned.1.call-update
  9.5 0.0 all-gather.8.cloned.1.call-start
  9.5 0.7 pad_maximum_fusion.1
  10.3 0.7 broadcast_in_dim.18
  11.1 0.1 convert_element_type.28
  11.1 0.8 reshape.111
  12.0 0.0 copy-start.6
  12.0 0.0 copy-start.3
  12.0 0.8 reshape.112
  12.9 0.8 reshape.113
  13.7 0.8 reshape.114
  14.6 0.8 reshape.117
  15.4 0.7 reshape.115
  16.2 0.2 concatenate.10
  16.4 17.0 %all_to_all.20 = bf16[8,32,512]{2,1,0:T(8,128)(2,1)S(1)} all-to-all(bf16[8,32,512]{2,1,0:T(8,128)(2,1)S(1)} %concatenate.10), channel_id=1, replica_groups=mesh['sp_0'=8,'sp_1'=8,'fs'=4,'tp'=2] {'sp_1'}, dimensions={0} | all-to-all | bytes 524288 | tf_op jit(solution)/shard_map/all_to_all | solution.py:271
  33.4 34.0 %all_gather.21 = bf16[2048,128]{1,0:T(8,128)(2,1)} all-gather(bf16[256,128]{1,0:T(8,128)(2,1)S(1)} %bitcast.44), channel_id=1, replica_groups=mesh['sp_0'=8,'sp_1'=8,'fs'=4,'tp'=2] {'sp_0'}, dimensions={0}, use_global_device_ids=true | all-gather | bytes 589824 | tf_op jit(solution)/shard_map/all_gather | solution.py:278
  67.4 0.0 all-gather.8.cloned.1.call-update
  67.4 0.1 copy.75
  67.6 1.2 broadcast_in_dim.20
  68.7 3.6 %all-to-all-start.1 = ((bf16[8,288,256]{2,1,0:T(8,128)(2,1)}), bf16[8,288,256]{2,1,0:T(8,128)(2,1)S(1)}, u32[]{:S(2)}, u32[]{:S(2)}) async-start(bf16[8,288,256]{2,1,0:T(8,128)(2,1)} %broadcast_in_dim.20), calls=%async_computation.1 | async-start | bytes 2359296 | tf_op jit(solution)/shard_map/all_to_all | solution.py:277
  72.3 0.0 copy-done.6
  72.3 0.1 reshape.124
  72.4 0.1 reshape.125
  72.5 0.0 copy-done.3
  72.5 0.1 reshape.126
  72.6 0.6 pad.15.gap_ref
  73.2 0.1 slice_convert_fusion
  73.3 0.1 reshape.130
  73.4 0.6 reduce_sum.19.ld_ref
  74.1 0.0 copy-start.7
  74.1 0.0 copy-start.8
  74.1 25.7 %all-to-all-done.1.w_ref = bf16[8,288,256]{2,1,0:T(8,128)(2,1)S(1)} async-done(((bf16[8,288,256]{2,1,0:T(8,128)(2,1)}), bf16[8,288,256]{2,1,0:T(8,128)(2,1)S(1)}, u32[]{:S(2)}, u32[]{:S(2)}) %all-to-all-start.1) | async-done | bytes 1179680 | tf_op jit(solution)/shard_map/all_to_all | solution.py:277
  99.8 0.0 copy-start
  99.8 0.0 all-gather.6.cloned.1.call-done.x_ref
  99.8 1.1 copy-done
  100.9 8.1 %states.1 = (bf16[1024,128]{1,0:T(8,128)(2,1)}, bf16[1024,128]{1,0:T(8,128)(2,1)}, f32[1024,128]{1,0:T(8,128)}, bf16[1024,32]{1,0:T(8,128)(2,1)}, bf16[8,80,128]...) custom-call(bf16[1024,2048]{1,0:T(8,128)(2,1)} %all-gather.6.cloned.1.call-done.x_ref, ...), custom_call_target="tpu_custom_call" | custom-call | tf_op jit(solution)/shard_map/states/pallas_call | solution.py:291
  109.0 3.4 %all-to-all-start.2 = ((bf16[8,80,128]{2,1,0:T(8,128)(2,1)}), bf16[8,80,128]{2,1,0:T(8,128)(2,1)S(1)}, u32[]{:S(2)}, u32[]{:S(2)}) async-start(bf16[8,80,128]{2,1,0:T(8,128)(2,1)} %get-tuple-element.14), calls=%async_computation.2 | async-start | bytes 327680 | tf_op jit(solution)/shard_map/all_to_all | solution.py:322
  112.4 0.7 fusion.5
  113.0 3.3 %collective-permute-start = (bf16[16,32]{1,0:T(8,128)(2,1)S(1)}, bf16[16,32]{1,0:T(8,128)(2,1)S(1)}, u32[]{:S(2)}, u32[]{:S(2)}) collective-permute-start(bf16[16,32]{1,0:T(8,128)(2,1)S(1)} %get-tuple-element.24), channel_id=1, source_target_pairs={{0,64},{64,128},{128,192},{192,256},{256,320},{320,384},{384,448},... | collective-permute-start | bytes 3080 | tf_op jit(solution)/shard_map/ppermute | solution.py:323
  116.3 1.3 collective-permute-start.1
  117.6 0.6 pad_convert_fusion.w_ref
  118.2 3.4 %local.1 = (f32[1024,128]{1,0:T(8,128)}, bf16[1024,128]{1,0:T(8,128)(2,1)}) custom-call(bf16[1024,128]{1,0:T(8,128)(2,1)} %get-tuple-element.15.a_ref, bf16[1024,128]{1,0:T(8,128)(2,1)} %get-tuple-element.16.v_ref, f32[1024,128]{1,0:T(8,128)} %get-tuple-element.17.c_ref, f32[1,128]{1,0:T(1,128)} %pad.15.gap_ref, ...), custom_call_target="tpu_custom_call" | custom-call | tf_op jit(solution)/shard_map/local/pallas_call | solution.py:325
  121.7 0.0 collective-permute-done.left_ref
  121.7 0.0 collective-permute-done.1.right_ref
  121.7 0.6 copy-done.4
  122.3 0.0 copy-start.5
  122.3 0.6 copy-done.5
  122.8 2.8 %conv.1.conv_ref = bf16[16,16,128]{2,1,0:T(8,128)(2,1)} custom-call(bf16[1024,32]{1,0:T(8,128)(2,1)} %get-tuple-element.22.g_ref, bf16[16,32]{1,0:T(8,128)(2,1)} %copy-done.4, bf16[16,32]{1,0:T(8,128)(2,1)} %copy-done.5, f32[32,32]{1,0:T(8,128)} %pad_convert_fusion.w_ref), custom_call_target="tpu_custom_call" | custom-call | tf_op jit(solution)/shard_map/conv/pallas_call | solution.py:330
  125.6 0.0 all-to-all-done.2.recv_ref
  125.6 0.0 copy-start.2
  125.6 0.7 copy-done.2
  126.3 2.5 %merge.1 = bf16[16,80,128]{2,1,0:T(8,128)(2,1)} custom-call(s32[1]{0:T(128)} %bitcast.z_ref, bf16[8,80,128]{2,1,0:T(8,128)(2,1)} %copy-done.2, f32[1024,128]{1,0:T(8,128)} %get-tuple-element.20.local_ref, bf16[1024,128]{1,0:T(8,128)(2,1)} %get-tuple-element.21.qd_ref, bf16[16,16,128]{2,1,0:T(8,128)(2,1)} %conv.1.conv_ref), custom_call_target="tpu_custom_call" | custom-call | tf_op jit(solution)/shard_map/merge/pallas_call | solution.py:336
  128.7 8.8 %all-to-all-start.3 = ((bf16[16,80,128]{2,1,0:T(8,128)(2,1)}), bf16[16,80,128]{2,1,0:T(8,128)(2,1)S(1)}, u32[]{:S(2)}, u32[]{:S(2)}) async-start(bf16[16,80,128]{2,1,0:T(8,128)(2,1)} %merge.1), calls=%async_computation.3 | async-start | bytes 655360 | tf_op jit(solution)/shard_map/all_to_all | solution.py:343
  137.6 0.0 copy-done.7
  137.6 0.0 copy-done.8
  137.6 1.8 %all-gather.2 = f32[2,2,256]{2,1,0:T(2,128)S(1)} all-gather(f32[1,2,256]{2,1,0:T(2,128)S(1)} %maximum_bitcast_fusion), channel_id=2, replica_groups=mesh['sp_0'=8,'sp_1'=8,'fs'=4,'tp'=2] {'tp'}, dimensions={0}, use_global_device_ids=true | all-gather | bytes 6144 | tf_op jit(solution)/shard_map/all_gather | solution.py:281
  139.4 0.6 fusion.6
  140.0 0.0 all-gather.8.cloned.1.call-done
  140.0 10.8 %all-to-all-done.3.recv_ref = bf16[16,80,128]{2,1,0:T(8,128)(2,1)S(1)} async-done(((bf16[16,80,128]{2,1,0:T(8,128)(2,1)}), bf16[16,80,128]{2,1,0:T(8,128)(2,1)S(1)}, u32[]{:S(2)}, u32[]{:S(2)}) %all-to-all-start.3) | async-done | bytes 327712 | tf_op jit(solution)/shard_map/all_to_all | solution.py:343
  150.8 0.7 copy-done.1
  151.6 5.1 %output.1 = bf16[64,2048]{1,0:T(8,128)(2,1)} custom-call(bf16[16,80,128]{2,1,0:T(8,128)(2,1)} %copy-done.1, f32[4,128]{1,0:T(4,128)} %bitcast.57, f32[4,128]{1,0:T(4,128)} %bitcast.56, bf16[8,2048,128]{2,1,0:T(8,128)(2,1)} %bitcast.41), custom_call_target="tpu_custom_call" | custom-call | tf_op jit(solution)/shard_map/output/pallas_call | solution.py:344
  (26 shorter events, 0.3 us)
Async XLA Ops:
  6.5 93.2 %all-gather.6.cloned.1.call-start = ((), (), s32[]{:S(2)}) async-start(), calls=%async_computation.4 | async-start | bytes 4456448 | tf_op jit(solution)/shard_map/all_gather | solution.py:250
  9.5 130.6 %all-gather.8.cloned.1.call-start = ((), (), s32[]{:S(2)}) async-start(), calls=%async_computation.5 | async-start | bytes 4718592 | tf_op jit(solution)/shard_map/all_gather | solution.py:279
  12.0 60.3 %copy-start.6 = (f32[2,256]{1,0:T(2,128)S(1)}, f32[2,256]{1,0:T(2,128)}, u32[]{:S(2)}) copy-start(f32[2,256]{1,0:T(2,128)} %param.21) | copy-start | bytes 6148
  12.0 60.5 %copy-start.3 = (bf16[31,256]{1,0:T(8,128)(2,1)S(1)}, bf16[31,256]{1,0:T(8,128)(2,1)}, u32[]{:S(2)}) copy-start(bf16[31,256]{1,0:T(8,128)(2,1)} %param.26) | copy-start | bytes 47620
  68.7 31.0 %all-to-all-start.1 = ((bf16[8,288,256]{2,1,0:T(8,128)(2,1)}), bf16[8,288,256]{2,1,0:T(8,128)(2,1)S(1)}, u32[]{:S(2)}, u32[]{:S(2)}) async-start(bf16[8,288,256]{2,1,0:T(8,128)(2,1)} %broadcast_in_dim.20), calls=%async_computation.1 | async-start | bytes 2359296 | tf_op jit(solution)/shard_map/all_to_all | solution.py:277
  74.1 63.5 %copy-start.7 = (f32[256]{0:T(256)S(1)}, f32[256]{0:T(256)}, u32[]{:S(2)}) copy-start(f32[256]{0:T(256)} %param.27) | copy-start | bytes 3076
  74.1 63.5 %copy-start.8 = (f32[256]{0:T(256)S(1)}, f32[256]{0:T(256)}, u32[]{:S(2)}) copy-start(f32[256]{0:T(256)} %param.23) | copy-start | bytes 3076
  99.8 1.1 copy-start
  109.0 16.7 %all-to-all-start.2 = ((bf16[8,80,128]{2,1,0:T(8,128)(2,1)}), bf16[8,80,128]{2,1,0:T(8,128)(2,1)S(1)}, u32[]{:S(2)}, u32[]{:S(2)}) async-start(bf16[8,80,128]{2,1,0:T(8,128)(2,1)} %get-tuple-element.14), calls=%async_computation.2 | async-start | bytes 327680 | tf_op jit(solution)/shard_map/all_to_all | solution.py:322
  113.0 8.6 %collective-permute-start = (bf16[16,32]{1,0:T(8,128)(2,1)S(1)}, bf16[16,32]{1,0:T(8,128)(2,1)S(1)}, u32[]{:S(2)}, u32[]{:S(2)}) collective-permute-start(bf16[16,32]{1,0:T(8,128)(2,1)S(1)} %get-tuple-element.24), channel_id=1, source_target_pairs={{0,64},{64,128},{128,192},{192,256},{256,320},{320,384},{384,448},... | collective-permute-start | bytes 3080 | tf_op jit(solution)/shard_map/ppermute | solution.py:323
  116.3 5.4 %collective-permute-start.1 = (bf16[16,32]{1,0:T(8,128)(2,1)S(1)}, bf16[16,32]{1,0:T(8,128)(2,1)S(1)}, u32[]{:S(2)}, u32[]{:S(2)}) collective-permute-start(bf16[16,32]{1,0:T(8,128)(2,1)S(1)} %get-tuple-element.23), channel_id=1, source_target_pairs={{64,0},{128,64},{192,128},{256,192},{320,256},{384,320},{448,384},... | collective-permute-start | bytes 3080 | tf_op jit(solution)/shard_map/ppermute | solution.py:324
  121.7 0.6 copy-start.4
  122.3 0.6 copy-start.5
  125.6 0.7 copy-start.2
  128.7 22.1 %all-to-all-start.3 = ((bf16[16,80,128]{2,1,0:T(8,128)(2,1)}), bf16[16,80,128]{2,1,0:T(8,128)(2,1)S(1)}, u32[]{:S(2)}, u32[]{:S(2)}) async-start(bf16[16,80,128]{2,1,0:T(8,128)(2,1)} %merge.1), calls=%async_computation.3 | async-start | bytes 655360 | tf_op jit(solution)/shard_map/all_to_all | solution.py:343
  150.8 0.7 copy-start.1
Sparse Core Ops, SparseCore 0:
  9.6 51.0 all-gather.5
  67.5 36.9 all-gather.7

commit v2 on v1

--- a/solution.py
+++ b/solution.py
@@ -1,5 +1,3 @@
-import functools
-
 import jax
 import jax.numpy as jnp
 from jax import lax
@@ -47,10 +45,74 @@
     return gap * sigmoid(-a)
 
 
+def norm_kernel(x_ref, gain_ref, out_ref):
+    x = x_ref[...].astype(F32)
+    scale = lax.rsqrt(jnp.mean(x * x, axis=1, keepdims=True) + EPS)
+    out_ref[...] = (x * scale * gain_ref[...]).astype(BF16)
+
+
+def first_kernel(
+    x_ref, rf_ref, rb_ref, rq_ref, cv_ref, cg_ref, ri_ref, ld_ref, rec_ref, conv_ref, out_ref
+):
+    x = x_ref[0]
+    lane = lanes(32)
+    group = lane // 32
+    row = lax.broadcasted_iota(jnp.int32, (32, 128), 0)
+    at = pl.multiple_of(128 * (x % 2), 128)
+    mine = jnp.where(x < 2, rec_ref[pl.ds(at, 128), :].astype(F32), conv_ref[pl.ds(at, 128), :].astype(F32))
+    outs = mine.T.astype(BF16)
+    for m in range(2):
+        cols = slice(128 * m, 128 * (m + 1))
+        src = [r[:, cols].astype(F32) for r in (rf_ref, rb_ref, rq_ref, cv_ref)]
+        gate = cg_ref[:, cols].astype(F32)
+        decays = jnp.zeros((32, 128), F32)
+        for d in range(2):
+            rest = jnp.broadcast_to(ld_ref[d, m : m + 1, :], (8, 128))
+            for s in range(3):
+                part = rest.astype(BF16).astype(F32)
+                rest = rest - part
+                low = pltpu.roll(part, 32, 1)[0:1]
+                high = pltpu.roll(part, 64, 1)[0:1]
+                decays = jnp.where(row == 2 * s + d, low, decays)
+                decays = jnp.where(row == 6 + 2 * s + d, high, decays)
+        for q in range(4):
+            y = 4 * m + q
+            a = jnp.zeros((32, 128), F32)
+            for p in range(4):
+                shift = (32 * (p - q)) % 128
+                moved = pltpu.roll(src[p], shift, 1) if shift else src[p]
+                a = jnp.where(group == p, moved, a)
+            out_ref[y, :, 0:128] = a.astype(BF16)
+            out_ref[y, :, 128:256] = ri_ref[:, cols]
+            shift = (-32 * q) % 128
+            moved = pltpu.roll(gate, shift, 1) if shift else gate
+            out_ref[y, :, 256:384] = jnp.where(group == 0, moved, decays).astype(BF16)
+            out_ref[y, :, 384:512] = outs
+
+
+def second_kernel(first_ref, out_ref, cols_ref, ld_ref):
+    lane = lanes(8)
+    gates = []
+    for y in range(8):
+        third = first_ref[y, :, 256:384].astype(F32)
+        gates.append(third)
+        cols_ref[32 * y : 32 * (y + 1), :] = first_ref[y, :, 384:512]
+        low = third[0:2] + third[2:4] + third[4:6]
+        high = third[6:8] + third[8:10] + third[10:12]
+        low = jnp.concatenate([low, low, low, low], axis=0)
+        high = jnp.concatenate([high, high, high, high], axis=0)
+        ld_ref[y] = jnp.where(lane < 96, pltpu.roll(low, 96, 1), pltpu.roll(high, 64, 1))[0:2]
+    gate_t = jnp.concatenate(gates, axis=0).T[0:32].astype(BF16)
+    for i in range(8):
+        for y in range(8):
+            out_ref[i, 32 * y : 32 * (y + 1), :] = first_ref[y, :, 0:256]
+        out_ref[i, 256:288, :] = gate_t
+
+
 def states_kernel(
     x_ref, w_ref, ld_ref, gap_ref,
     a_ref, v_ref, c_ref, gated_ref, send_ref, before_ref, offset_ref,
-    chunk_s, chunk_t,
+    chunk_s, chunk_t, edge,
 ):
     step = pl.program_id(0)
     rows = x_ref.shape[0]
@@ -67,6 +129,17 @@
     glu = acc_g.astype(BF16).astype(F32)
     gated = pre_a.astype(F32)[:, 96:128] * sigmoid(glu)
     gated_ref[...] = gated.astype(BF16)
+
+    @pl.when(step == 0)
+    def _():
+        edge[...] = jnp.concatenate([gated[:16], gated[:16], gated[:16], gated[:16]], axis=1)
+
+    @pl.when(step == pl.num_programs(0) - 1)
+    def _():
+        last = gated[rows - 16 :]
+        last = jnp.concatenate([last, last, last, last], axis=1)
+        edge[...] = jnp.where(lanes(16) < 32, edge[...], last)
+
     lower, upper = triangles()
     lower_f, upper_f = lower.astype(F32), upper.astype(F32)
     lower_b, upper_b = lower_f.astype(BF16), upper_f.astype(BF16)
@@ -123,10 +196,29 @@
         tail = tail.astype(BF16)
         for i in range(8):
             send_ref[i, :64, :] = s
-            send_ref[i, 64:, :] = tail
-
-
-def local_kernel(a_ref, v_ref, c_ref, gap_ref, before_ref, offset_ref, out_ref, qd_ref):
+            send_ref[i, 64:80, :] = tail
+            send_ref[i, 80:96, :] = edge[...].astype(BF16)
+
+
+def local_kernel(
+    a_ref, v_ref, c_ref, gap_ref, before_ref, offset_ref, g_ref, taps_ref,
+    out_ref, qd_ref, conv_ref, edge_ref, pad,
+):
+    n = g_ref.shape[0]
+    zeros = jnp.zeros((16, 32), F32)
+    pad[0:16, :] = zeros
+    pad[16 : 16 + n, :] = g_ref[...].astype(F32)
+    pad[16 + n : 32 + n, :] = zeros
+    taps = taps_ref[...]
+    for blk in range(n // 64):
+        acc = jnp.zeros((64, 32), F32)
+        for j in range(31):
+            acc += pad[64 * blk + j + 1 : 64 * blk + j + 65, :] * taps[j : j + 1, :]
+        conv_ref[blk] = jnp.concatenate([acc[16 * q : 16 * (q + 1)] for q in range(4)], axis=1).astype(BF16)
+        if blk == 0:
+            edge_ref[0] = acc[0:16]
+        if blk == n // 64 - 1:
+            edge_ref[1] = acc[48:64]
     lower, upper = triangles()
     lane = lanes(128)
     for b in range(a_ref.shape[0] // 128):
@@ -154,21 +246,25 @@
             qd_ref[to, :] = (qg[part] * jnp.exp(offset_ref[2 * b + h][0:1])).astype(BF16)
 
 
-def conv_kernel_body(g_ref, left_ref, right_ref, w_ref, out_ref, pad):
-    n = g_ref.shape[0]
-    pad[0:16, :] = left_ref[...].astype(F32)
-    pad[16 : 16 + n, :] = g_ref[...].astype(F32)
-    pad[16 + n : 32 + n, :] = right_ref[...].astype(F32)
-    w = w_ref[...]
-    for blk in range(n // 64):
-        acc = jnp.zeros((64, 32), F32)
-        for j in range(31):
-            acc += pad[64 * blk + j + 1 : 64 * blk + j + 65, :] * w[j : j + 1, :]
-        out_ref[blk] = jnp.concatenate([acc[16 * q : 16 * (q + 1)] for q in range(4)], axis=1).astype(BF16)
-
-
-def merge_kernel(z_ref, recv_ref, local_ref, qd_ref, conv_ref, send_ref):
+def merge_kernel(z_ref, recv_ref, local_ref, qd_ref, conv_ref, edge_ref, taps_ref, send_ref):
     z = z_ref[0]
+    heads = jnp.zeros((16, 128), F32)
+    tails = jnp.zeros((16, 128), F32)
+    for i in range(8):
+        other = recv_ref[i, 80:96, :].astype(F32)
+        tails = jnp.where(i == z - 1, other, tails)
+        heads = jnp.where(i == z + 1, other, heads)
+    zeros = jnp.zeros((16, 32), F32)
+    before = jnp.concatenate([tails[:, 32:64], zeros], axis=0)
+    after = jnp.concatenate([zeros, heads[:, 0:32]], axis=0)
+    first, last = edge_ref[0], edge_ref[1]
+    taps = taps_ref[...]
+    for j in range(15):
+        first += before[j + 1 : j + 17] * taps[j : j + 1, :]
+        last += after[j + 1 : j + 17] * taps[16 + j : 17 + j, :]
+    first = jnp.concatenate([first] * 4, axis=1).astype(BF16)
+    last = jnp.concatenate([last] * 4, axis=1).astype(BF16)
+    lane16 = lanes(16)
     fwd = (lanes(64) % 64) < 32
     fwd1 = (lanes(1) % 64) < 32
     s = jnp.zeros((64, 128), F32)
@@ -187,7 +283,12 @@
         rows = slice(64 * blk, 64 * (blk + 1))
         out = local_ref[rows, :] + dot(qd_ref[rows, :], full, NT)
         send_ref[blk, :64, :] = out.astype(BF16)
-        send_ref[blk, 64:, :] = conv_ref[blk]
+        packed = conv_ref[blk]
+        if blk == 0:
+            packed = jnp.where(lane16 < 32, first, packed)
+        if blk == 15:
+            packed = jnp.where(lane16 >= 96, last, packed)
+        send_ref[blk, 64:, :] = packed
 
 
 def output_kernel(recv_ref, rec_gain_ref, conv_gain_ref, w_ref, out_ref, act):
@@ -244,36 +345,31 @@
 ):
     y, z, xi = lax.axis_index(Y), lax.axis_index(Z), lax.axis_index(X)
 
-    rows_in = tokens[0].astype(F32)
-    normed = rows_in * lax.rsqrt(jnp.mean(rows_in * rows_in, axis=-1, keepdims=True) + EPS)
-    normed = (normed * norm_gain).astype(BF16)
+    normed = pl.pallas_call(
+        norm_kernel, out_shape=jax.ShapeDtypeStruct((64, 2048), BF16), name="norm"
+    )(tokens[0], norm_gain.reshape(1, 2048))
     seq = lax.all_gather(normed, (Y, C), axis=0, tiled=True)
 
-    def per_y(w):
-        return w.reshape(32, 8, 32).transpose(1, 0, 2)
-
-    values = jnp.repeat(rec_input.reshape(32, 2, 128).transpose(1, 0, 2), 4, axis=0)
-    ld = jnp.repeat(log_decay[0].transpose(1, 0, 2), 4, axis=0)
-    ld_hi = lax.reduce_precision(ld, 8, 7)
-    ld_mid = lax.reduce_precision(ld - ld_hi, 8, 7)
-    ld_lo = lax.reduce_precision(ld - ld_hi - ld_mid, 8, 7)
-    ld3 = jnp.stack([ld_hi, ld_mid, ld_lo], axis=1).astype(BF16).reshape(8, 24, 32)
-    ld3 = jnp.pad(ld3, ((0, 0), (0, 8), (0, 64)))
-    outs = jnp.concatenate([out_rec, out_conv], axis=0).reshape(4, 128, 32)
-    outs = lax.dynamic_index_in_dim(outs, xi, 0, keepdims=False).T
-    first = jnp.concatenate(
-        [
-            per_y(rec_forward), per_y(rec_backward), per_y(rec_query), per_y(conv_value), values,
-            per_y(conv_gate), ld3, jnp.broadcast_to(outs, (8, 32, 128)),
-        ],
-        axis=2,
+    first = pl.pallas_call(
+        first_kernel,
+        in_specs=[pl.BlockSpec(memory_space=pltpu.SMEM)]
+        + [pl.BlockSpec(memory_space=pltpu.VMEM)] * 9,
+        out_shape=jax.ShapeDtypeStruct((8, 32, 512), BF16),
+        name="first",
+    )(
+        xi.reshape(1).astype(jnp.int32), rec_forward, rec_backward, rec_query, conv_value,
+        conv_gate, rec_input, log_decay[0], out_rec, out_conv,
     )
     first = lax.all_to_all(first, Y, split_axis=0, concat_axis=0, tiled=True)
-    main = first[:, :, :256].reshape(256, 256)
-    gate_t = first[:, :, 256:288].reshape(256, 32).T
-    decays = first[:, :24, 288:320].astype(F32).reshape(8, 3, 2, 128).sum(axis=1)
-    out_cols = first[:, :, 384:].reshape(256, 128)
-    second = jnp.broadcast_to(jnp.concatenate([main, gate_t], axis=0), (8, 288, 256))
+    second, out_cols, decays = pl.pallas_call(
+        second_kernel,
+        out_shape=[
+            jax.ShapeDtypeStruct((8, 288, 256), BF16),
+            jax.ShapeDtypeStruct((256, 128), BF16),
+            jax.ShapeDtypeStruct((8, 2, 128), F32),
+        ],
+        name="second",
+    )(first)
     weights = lax.all_to_all(second, Z, split_axis=0, concat_axis=0, tiled=True)
     out_w = lax.all_gather(out_cols, Z, axis=0, tiled=True)
     out_w = lax.all_gather(out_w, (C, X), axis=0)
@@ -302,7 +398,7 @@
             spec((tile, 128), lambda i: (i, 0)),
             spec((tile, 128), lambda i: (i, 0)),
             spec((tile, 32), lambda i: (i, 0)),
-            full((8, 80, 128)),
+            full((8, 96, 128)),
             full((16, 64, 128)),
             full((16, 8, 128)),
         ],
@@ -311,35 +407,35 @@
             jax.ShapeDtypeStruct((n, 128), BF16),
             jax.ShapeDtypeStruct((n, 128), F32),
             jax.ShapeDtypeStruct((n, 32), BF16),
-            jax.ShapeDtypeStruct((8, 80, 128), BF16),
+            jax.ShapeDtypeStruct((8, 96, 128), BF16),
             jax.ShapeDtypeStruct((16, 64, 128), BF16),
             jax.ShapeDtypeStruct((16, 8, 128), F32),
         ],
-        scratch_shapes=[pltpu.VMEM((16, 64, 128), F32), pltpu.VMEM((16, 8, 128), F32)],
+        scratch_shapes=[
+            pltpu.VMEM((16, 64, 128), F32), pltpu.VMEM((16, 8, 128), F32), pltpu.VMEM((16, 128), F32)
+        ],
         name="states",
     )(seq, weights, decays, gap)
 
     arrived = lax.all_to_all(sent, Z, split_axis=0, concat_axis=0, tiled=True)
-    left = lax.ppermute(gated[n - 16 :], Z, [(i, i + 1) for i in range(7)])
-    right = lax.ppermute(gated[:16], Z, [(i + 1, i) for i in range(7)])
-    local, decayed = pl.pallas_call(
+    local, decayed, convolved, edges = pl.pallas_call(
         local_kernel,
-        out_shape=[jax.ShapeDtypeStruct((n, 128), F32), jax.ShapeDtypeStruct((n, 128), BF16)],
+        out_shape=[
+            jax.ShapeDtypeStruct((n, 128), F32),
+            jax.ShapeDtypeStruct((n, 128), BF16),
+            jax.ShapeDtypeStruct((16, 16, 128), BF16),
+            jax.ShapeDtypeStruct((2, 16, 32), F32),
+        ],
+        scratch_shapes=[pltpu.VMEM((n + 32, 32), F32)],
         name="local",
-    )(pre_a, pre_v, cum, gap, before, offset)
-    convolved = pl.pallas_call(
-        conv_kernel_body,
-        out_shape=jax.ShapeDtypeStruct((16, 16, 128), BF16),
-        scratch_shapes=[pltpu.VMEM((n + 32, 32), F32)],
-        name="conv",
-    )(gated, left, right, taps)
+    )(pre_a, pre_v, cum, gap, before, offset, gated, taps)
     merged = pl.pallas_call(
         merge_kernel,
         in_specs=[pl.BlockSpec(memory_space=pltpu.SMEM)]
-        + [pl.BlockSpec(memory_space=pltpu.VMEM)] * 4,
+        + [pl.BlockSpec(memory_space=pltpu.VMEM)] * 6,
         out_shape=jax.ShapeDtypeStruct((16, 80, 128), BF16),
         name="merge",
-    )(z.reshape(1).astype(jnp.int32), arrived, local, decayed, convolved)
+    )(z.reshape(1).astype(jnp.int32), arrived, local, decayed, convolved, edges, taps)
     mine = lax.all_to_all(merged, (Y, C), split_axis=0, concat_axis=0, tiled=True)
     mixed = pl.pallas_call(
         output_kernel,

time: 165 us -> 157 us (0.952)
  local copies, waits for them, and re-layouts: 13.2 us -> 6.9 us
  Pallas kernels: 21.9 us -> 26.8 us
  other arithmetic: 4.98 us -> 0.62 us
  blocking collectives: 52.8 us -> 50.2 us
    reshape x9 -> x0, local copies, waits for them, and re-layouts: 5.03 us -> none  [the longest x5 4.12 us: per_y(): return w.reshape(32, 8, 32).transpose(1, 0, 2)]
    ppermute x2 -> x0, starting transfers between devices: 4.54 us -> none  [the longest x1 3.25 us: body(): left = lax.ppermute(gated[n - 16:], Z, [(i, i + 1) for i in range(7)])]
    all_to_all x1, starting transfers between devices: 8.84 us -> 12.4 us  [body(): lax.all_to_all(merged, (Y, C), split_axis=0, concat_axis=0, tiled=True)]
    all_to_all x1, waiting for transfers between devices: 0.01 us -> 3.29 us  [body(): arrived = lax.all_to_all(sent, Z, split_axis=0, concat_axis=0, tiled=True)]
    pallas_call x1 -> x3, Pallas kernels: 2.76 us -> 5.86 us  [the longest x1 2.17 us: body(): pl.pallas_call(second_kernel, out_shape=[jax.ShapeDtypeStruct((8, 288, 25...]
    all_gather x1, blocking collectives: 34 us -> 31.2 us  [body(): out_w = lax.all_gather(out_cols, Z, axis=0, tiled=True)]
    all_to_all x1, waiting for transfers between devices: 25.7 us -> 23.7 us  [body(): weights = lax.all_to_all(second, Z, split_axis=0, concat_axis=0, tiled=True)]
    broadcast_in_dim x4 -> x0, local copies, waits for them, and re-layouts: 1.88 us -> none  [the longest x1 1.17 us: body(): jnp.broadcast_to(jnp.concatenate([main, gate_t], axis=0), (8, 288, 256))]
  transfers between devices with their start and end apart: 7 -> 5, of which waited for: 2 -> 3; matrix products, arithmetic and copies ran while one was open for 7% -> 3% of each run, Pallas kernels for 10% -> 13%
where the time goes in v2:
time: 157 us; the launch traced here: 156 us
  blocking collectives  50.2 us (32%)
  waiting for transfers between devices  37.9 us (24%)
  Pallas kernels  26.8 us (17%)
  starting transfers between devices  19.9 us (13%)
  between operations  13.5 us (9%)
  local copies, waits for them, and re-layouts  6.9 us (4%)
    all_gather x1, blocking collectives, body(): out_w = lax.all_gather(out_cols, Z, axis=0, tiled=True)  31.2 us
    all_to_all x1, waiting for transfers between devices, body(): weights = lax.all_to_all(second, Z, split_axis=0, concat_axis=0, tiled=True)  23.7 us
    all_to_all x1, blocking collectives, body(): first = lax.all_to_all(first, Y, split_axis=0, concat_axis=0, tiled=True)  17.2 us
    all_to_all x1, starting transfers between devices, body(): lax.all_to_all(merged, (Y, C), split_axis=0, concat_axis=0, tiled=True)  12.4 us
    all_to_all x1, waiting for transfers between devices, body(): lax.all_to_all(merged, (Y, C), split_axis=0, concat_axis=0, tiled=True)  10.8 us
    pallas_call x1, Pallas kernels, body(): pl.pallas_call(states_kernel, grid=(n // tile,), in_specs=[spec((tile, 20...  8.84 us
    unnamed x17, local copies, waits for them, and re-layouts  5.42 us
    pallas_call x1, Pallas kernels, body(): pl.pallas_call(output_kernel, grid=(4,), in_specs=[full((16, 80, 128)), f...  5.15 us
  transfers between devices with their start and end apart: 5, of which 3 were waited for; matrix products, arithmetic and copies ran while one was open for 3% of the time, Pallas kernels for 13%

profile of v2, /device:TPU:1, one launch (start us, length us, event | category | flops | bytes accessed | tf_op | source)
XLA Modules:
  0.0 155.8 jit_solution(2931897717674833987)
XLA Ops:
  6.5 0.0 copy-start.4
  6.5 0.0 all-gather.6.cloned.1.call-start
  6.5 1.8 %norm.1 = bf16[64,2048]{1,0:T(8,128)(2,1)} custom-call(bf16[64,2048]{1,0:T(8,128)(2,1)} %bitcast.20, f32[1,2048]{1,0:T(1,128)} %bitcast.22), custom_call_target="tpu_custom_call" | custom-call | tf_op jit(solution)/shard_map/norm/pallas_call | solution.py:348
  8.4 0.0 all-gather.6.cloned.1.call-update
  8.4 0.0 all-gather.8.cloned.1.call-start
  8.4 1.4 copy.20.rec_ref
  9.9 1.4 copy.21.conv_ref
  11.3 1.9 %first.1 = bf16[8,32,512]{2,1,0:T(8,128)(2,1)} custom-call(s32[1]{0:T(128)} %bitcast.3.x_ref, bf16[32,256]{1,0:T(8,128)(2,1)} %rf_ref.1, bf16[32,256]{1,0:T(8,128)(2,1)} %rb_ref.1, bf16[32,256]{1,0:T(8,128)(2,1)} %rq_ref.1, bf16[32,256]{1,0:T(8,128)(2,1)} %cv_ref.1, bf16[32,256]{1,0:T(8,128)(2,1)} %cg_ref.1, bf16[32,256]{1,0:T(8,128)(2,1)} %ri_ref.1, ...), custom_call_target="tpu_custom_call" | custom-call | tf_op jit(solution)/shard_map/first/pallas_call | solution.py:353
  13.2 17.2 %all_to_all.20.first_ref = bf16[8,32,512]{2,1,0:T(8,128)(2,1)} all-to-all(bf16[8,32,512]{2,1,0:T(8,128)(2,1)} %first.1), channel_id=1, replica_groups=mesh['sp_0'=8,'sp_1'=8,'fs'=4,'tp'=2] {'sp_1'}, dimensions={0} | all-to-all | bytes 524288 | tf_op jit(solution)/shard_map/all_to_all | solution.py:363
  30.4 2.2 %second.1 = (bf16[8,288,256]{2,1,0:T(8,128)(2,1)}, bf16[256,128]{1,0:T(8,128)(2,1)}, f32[8,2,128]{2,1,0:T(2,128)}) custom-call(bf16[8,32,512]{2,1,0:T(8,128)(2,1)} %all_to_all.20.first_ref), custom_call_target="tpu_custom_call" | custom-call | tf_op jit(solution)/shard_map/second/pallas_call | solution.py:364
  32.6 31.2 %all_gather.21 = bf16[2048,128]{1,0:T(8,128)(2,1)} all-gather(bf16[256,128]{1,0:T(8,128)(2,1)} %get-tuple-element.32), channel_id=1, replica_groups=mesh['sp_0'=8,'sp_1'=8,'fs'=4,'tp'=2] {'sp_0'}, dimensions={0}, use_global_device_ids=true | all-gather | bytes 589824 | tf_op jit(solution)/shard_map/all_gather | solution.py:374
  63.8 0.0 all-gather.8.cloned.1.call-update
  63.8 0.0 copy-start.3
  63.8 4.0 %all-to-all-start.1 = ((bf16[8,288,256]{2,1,0:T(8,128)(2,1)}), bf16[8,288,256]{2,1,0:T(8,128)(2,1)S(1)}, u32[]{:S(2)}, u32[]{:S(2)}) async-start(bf16[8,288,256]{2,1,0:T(8,128)(2,1)} %get-tuple-element.19), calls=%async_computation.1 | async-start | bytes 2359296 | tf_op jit(solution)/shard_map/all_to_all | solution.py:373
  67.8 0.0 copy-done.4
  67.8 0.1 reshape.24
  67.9 0.1 reshape.25
  68.0 0.6 pad.10.gap_ref
  68.6 23.7 %all-to-all-done.1.w_ref = bf16[8,288,256]{2,1,0:T(8,128)(2,1)S(1)} async-done(((bf16[8,288,256]{2,1,0:T(8,128)(2,1)}), bf16[8,288,256]{2,1,0:T(8,128)(2,1)S(1)}, u32[]{:S(2)}, u32[]{:S(2)}) %all-to-all-start.1) | async-done | bytes 1179680 | tf_op jit(solution)/shard_map/all_to_all | solution.py:373
  92.3 0.0 copy-start
  92.3 0.0 all-gather.6.cloned.1.call-done.x_ref
  92.3 1.1 copy-done
  93.4 0.0 copy-start.5
  93.4 0.0 copy-start.6
  93.4 8.8 %states.1 = (bf16[1024,128]{1,0:T(8,128)(2,1)}, bf16[1024,128]{1,0:T(8,128)(2,1)}, f32[1024,128]{1,0:T(8,128)}, bf16[1024,32]{1,0:T(8,128)(2,1)}, bf16[8,96,128]...) custom-call(bf16[1024,2048]{1,0:T(8,128)(2,1)} %all-gather.6.cloned.1.call-done.x_ref, ...), custom_call_target="tpu_custom_call" | custom-call | tf_op jit(solution)/shard_map/states/pallas_call | solution.py:387
  102.3 3.4 %all-to-all-start.2 = ((bf16[8,96,128]{2,1,0:T(8,128)(2,1)}), bf16[8,96,128]{2,1,0:T(8,128)(2,1)S(1)}, u32[]{:S(2)}, u32[]{:S(2)}) async-start(bf16[8,96,128]{2,1,0:T(8,128)(2,1)} %get-tuple-element.21), calls=%async_computation.2 | async-start | bytes 393216 | tf_op jit(solution)/shard_map/all_to_all | solution.py:420
  105.7 0.0 copy-done.3
  105.7 0.1 reshape.26
  105.8 0.6 pad_convert_fusion.taps_ref
  106.4 4.5 %local.1 = (f32[1024,128]{1,0:T(8,128)}, bf16[1024,128]{1,0:T(8,128)(2,1)}, bf16[16,16,128]{2,1,0:T(8,128)(2,1)}, f32[2,16,32]{2,1,0:T(8,128)}) custom-call(bf16[1024,128]{1,0:T(8,128)(2,1)} %get-tuple-element.22.a_ref, bf16[1024,128]{1,0:T(8,128)(2,1)} %get-tuple-element.23.v_ref, f32[1024,128]{1,0:T(8,128)} %get-tuple-element.24.c_ref, ...), custom_call_target="tpu_custom_call" | custom-call | tf_op jit(solution)/shard_map/local/pallas_call | solution.py:421
  110.9 3.3 %all-to-all-done.2.recv_ref = bf16[8,96,128]{2,1,0:T(8,128)(2,1)S(1)} async-done(((bf16[8,96,128]{2,1,0:T(8,128)(2,1)}), bf16[8,96,128]{2,1,0:T(8,128)(2,1)S(1)}, u32[]{:S(2)}, u32[]{:S(2)}) %all-to-all-start.2) | async-done | bytes 196640 | tf_op jit(solution)/shard_map/all_to_all | solution.py:420
  114.2 0.0 copy-start.2
  114.2 0.7 copy-done.2
  114.9 2.5 %merge.1 = bf16[16,80,128]{2,1,0:T(8,128)(2,1)} custom-call(s32[1]{0:T(128)} %bitcast.z_ref, bf16[8,96,128]{2,1,0:T(8,128)(2,1)} %copy-done.2, f32[1024,128]{1,0:T(8,128)} %get-tuple-element.28.local_ref, bf16[1024,128]{1,0:T(8,128)(2,1)} %get-tuple-element.29.qd_ref, bf16[16,16,128]{2,1,0:T(8,128)(2,1)} %get-tuple-element.30.conv_ref, ...), custom_call_target="tpu_custom_call" | custom-call | tf_op jit(solution)/shard_map/merge/pallas_call | solution.py:432
  117.4 12.4 %all-to-all-start.3 = ((bf16[16,80,128]{2,1,0:T(8,128)(2,1)}), bf16[16,80,128]{2,1,0:T(8,128)(2,1)S(1)}, u32[]{:S(2)}, u32[]{:S(2)}) async-start(bf16[16,80,128]{2,1,0:T(8,128)(2,1)} %merge.1), calls=%async_computation.3 | async-start | bytes 655360 | tf_op jit(solution)/shard_map/all_to_all | solution.py:439
  129.8 0.0 copy-done.5
  129.8 0.0 copy-done.6
  129.9 1.8 %all-gather.2 = f32[2,2,256]{2,1,0:T(2,128)S(1)} all-gather(f32[1,2,256]{2,1,0:T(2,128)S(1)} %maximum_bitcast_fusion), channel_id=2, replica_groups=mesh['sp_0'=8,'sp_1'=8,'fs'=4,'tp'=2] {'tp'}, dimensions={0}, use_global_device_ids=true | all-gather | bytes 6144 | tf_op jit(solution)/shard_map/all_gather | solution.py:377
  131.7 0.6 fusion
  132.3 0.0 all-gather.8.cloned.1.call-done
  132.3 10.8 %all-to-all-done.3.recv_ref = bf16[16,80,128]{2,1,0:T(8,128)(2,1)S(1)} async-done(((bf16[16,80,128]{2,1,0:T(8,128)(2,1)}), bf16[16,80,128]{2,1,0:T(8,128)(2,1)S(1)}, u32[]{:S(2)}, u32[]{:S(2)}) %all-to-all-start.3) | async-done | bytes 327712 | tf_op jit(solution)/shard_map/all_to_all | solution.py:439
  143.1 0.0 copy-start.1
  143.1 0.7 copy-done.1
  143.8 5.2 %output.1 = bf16[64,2048]{1,0:T(8,128)(2,1)} custom-call(bf16[16,80,128]{2,1,0:T(8,128)(2,1)} %copy-done.1, f32[4,128]{1,0:T(4,128)} %bitcast.24, f32[4,128]{1,0:T(4,128)} %bitcast.23, bf16[8,2048,128]{2,1,0:T(8,128)(2,1)} %bitcast.19), custom_call_target="tpu_custom_call" | custom-call | tf_op jit(solution)/shard_map/output/pallas_call | solution.py:440
  (4 shorter events, 0.0 us)
Async XLA Ops:
  6.5 61.3 %copy-start.4 = (f32[2,256]{1,0:T(2,128)S(1)}, f32[2,256]{1,0:T(2,128)}, u32[]{:S(2)}) copy-start(f32[2,256]{1,0:T(2,128)} %param.21) | copy-start | bytes 6148
  6.5 85.8 %all-gather.6.cloned.1.call-start = ((), (), s32[]{:S(2)}) async-start(), calls=%async_computation.4 | async-start | bytes 4456448 | tf_op jit(solution)/shard_map/all_gather | solution.py:351
  8.4 123.9 %all-gather.8.cloned.1.call-start = ((), (), s32[]{:S(2)}) async-start(), calls=%async_computation.5 | async-start | bytes 4718592 | tf_op jit(solution)/shard_map/all_gather | solution.py:375
  63.8 41.9 %copy-start.3 = (bf16[31,256]{1,0:T(8,128)(2,1)S(1)}, bf16[31,256]{1,0:T(8,128)(2,1)}, u32[]{:S(2)}) copy-start(bf16[31,256]{1,0:T(8,128)(2,1)} %param.26) | copy-start | bytes 47620
  63.8 28.5 %all-to-all-start.1 = ((bf16[8,288,256]{2,1,0:T(8,128)(2,1)}), bf16[8,288,256]{2,1,0:T(8,128)(2,1)S(1)}, u32[]{:S(2)}, u32[]{:S(2)}) async-start(bf16[8,288,256]{2,1,0:T(8,128)(2,1)} %get-tuple-element.19), calls=%async_computation.1 | async-start | bytes 2359296 | tf_op jit(solution)/shard_map/all_to_all | solution.py:373
  92.3 1.1 copy-start
  93.4 36.4 %copy-start.5 = (f32[256]{0:T(256)S(1)}, f32[256]{0:T(256)}, u32[]{:S(2)}) copy-start(f32[256]{0:T(256)} %param.27) | copy-start | bytes 3076
  93.4 36.4 %copy-start.6 = (f32[256]{0:T(256)S(1)}, f32[256]{0:T(256)}, u32[]{:S(2)}) copy-start(f32[256]{0:T(256)} %param.23) | copy-start | bytes 3076
  102.3 12.0 %all-to-all-start.2 = ((bf16[8,96,128]{2,1,0:T(8,128)(2,1)}), bf16[8,96,128]{2,1,0:T(8,128)(2,1)S(1)}, u32[]{:S(2)}, u32[]{:S(2)}) async-start(bf16[8,96,128]{2,1,0:T(8,128)(2,1)} %get-tuple-element.21), calls=%async_computation.2 | async-start | bytes 393216 | tf_op jit(solution)/shard_map/all_to_all | solution.py:420
  114.2 0.7 copy-start.2
  117.4 25.7 %all-to-all-start.3 = ((bf16[16,80,128]{2,1,0:T(8,128)(2,1)}), bf16[16,80,128]{2,1,0:T(8,128)(2,1)S(1)}, u32[]{:S(2)}, u32[]{:S(2)}) async-start(bf16[16,80,128]{2,1,0:T(8,128)(2,1)} %merge.1), calls=%async_computation.3 | async-start | bytes 655360 | tf_op jit(solution)/shard_map/all_to_all | solution.py:439
  143.1 0.7 copy-start.1
Sparse Core Ops, SparseCore 0:
  9.5 50.2 all-gather.5
  63.9 42.1 all-gather.7

commit v3 on v2

--- a/solution.py
+++ b/solution.py
@@ -52,15 +52,10 @@
 
 
 def first_kernel(
-    x_ref, rf_ref, rb_ref, rq_ref, cv_ref, cg_ref, ri_ref, ld_ref, rec_ref, conv_ref, out_ref
+    rf_ref, rb_ref, rq_ref, cv_ref, cg_ref, ri_ref, ld_ref, rec_ref, conv_ref, out_ref
 ):
-    x = x_ref[0]
-    lane = lanes(32)
-    group = lane // 32
+    group = lanes(32) // 32
     row = lax.broadcasted_iota(jnp.int32, (32, 128), 0)
-    at = pl.multiple_of(128 * (x % 2), 128)
-    mine = jnp.where(x < 2, rec_ref[pl.ds(at, 128), :].astype(F32), conv_ref[pl.ds(at, 128), :].astype(F32))
-    outs = mine.T.astype(BF16)
     for m in range(2):
         cols = slice(128 * m, 128 * (m + 1))
         src = [r[:, cols].astype(F32) for r in (rf_ref, rb_ref, rq_ref, cv_ref)]
@@ -87,47 +82,52 @@
             shift = (-32 * q) % 128
             moved = pltpu.roll(gate, shift, 1) if shift else gate
             out_ref[y, :, 256:384] = jnp.where(group == 0, moved, decays).astype(BF16)
-            out_ref[y, :, 384:512] = outs
-
-
-def second_kernel(first_ref, out_ref, cols_ref, ld_ref):
+            out_ref[y, :, 384:640] = rec_ref[...]
+            out_ref[y, :, 640:896] = conv_ref[...]
+
+
+def second_kernel(first_ref, w_ref, w2_ref, cols_ref, ld_ref):
     lane = lanes(8)
-    gates = []
+    keys, values, gates = [], [], []
     for y in range(8):
         third = first_ref[y, :, 256:384].astype(F32)
+        keys.append(first_ref[y, :, 0:128].astype(F32))
+        values.append(first_ref[y, :, 128:256].astype(F32))
         gates.append(third)
-        cols_ref[32 * y : 32 * (y + 1), :] = first_ref[y, :, 384:512]
+        cols_ref[32 * y : 32 * (y + 1), :] = first_ref[y, :, 384:896]
         low = third[0:2] + third[2:4] + third[4:6]
         high = third[6:8] + third[8:10] + third[10:12]
         low = jnp.concatenate([low, low, low, low], axis=0)
         high = jnp.concatenate([high, high, high, high], axis=0)
         ld_ref[y] = jnp.where(lane < 96, pltpu.roll(low, 96, 1), pltpu.roll(high, 64, 1))[0:2]
-    gate_t = jnp.concatenate(gates, axis=0).T[0:32].astype(BF16)
+    keys = jnp.concatenate(keys, axis=0).T.astype(BF16)
+    w_ref[0:128, :] = jnp.concatenate(values, axis=0).T.astype(BF16)
+    w_ref[128:224, :] = keys[0:96]
+    gates = jnp.concatenate(gates, axis=0).T[0:32].astype(BF16)
     for i in range(8):
-        for y in range(8):
-            out_ref[i, 32 * y : 32 * (y + 1), :] = first_ref[y, :, 0:256]
-        out_ref[i, 256:288, :] = gate_t
+        w2_ref[i, 0:32, :] = keys[96:128]
+        w2_ref[i, 32:64, :] = gates
 
 
 def states_kernel(
-    x_ref, w_ref, ld_ref, gap_ref,
+    x_ref, w_ref, w2_ref, ld_ref, gap_ref,
     a_ref, v_ref, c_ref, gated_ref, send_ref, before_ref, offset_ref,
     chunk_s, chunk_t, edge,
 ):
     step = pl.program_id(0)
     rows = x_ref.shape[0]
-    acc = jnp.zeros((rows, 256), F32)
-    acc_g = jnp.zeros((rows, 32), F32)
+    acc = jnp.zeros((rows, 224), F32)
+    acc_g = jnp.zeros((rows, 64), F32)
     for k in range(8):
         xk = x_ref[:, 256 * k : 256 * (k + 1)]
-        acc += dot(xk, w_ref[k, :256, :], NN)
-        acc_g += dot(xk, w_ref[k, 256:, :], NT)
-    pre_a = acc[:, :128].astype(BF16)
-    pre_v = acc[:, 128:].astype(BF16)
+        acc += dot(xk, w_ref[k], NT)
+        acc_g += dot(xk, w2_ref[k], NT)
+    pre_v = acc[:, :128].astype(BF16)
+    pre_a = jnp.concatenate([acc[:, 128:], jnp.zeros((rows, 32), F32)], axis=1).astype(BF16)
     a_ref[...] = pre_a
     v_ref[...] = pre_v
     glu = acc_g.astype(BF16).astype(F32)
-    gated = pre_a.astype(F32)[:, 96:128] * sigmoid(glu)
+    gated = glu[:, 0:32] * sigmoid(glu[:, 32:64])
     gated_ref[...] = gated.astype(BF16)
 
     @pl.when(step == 0)
@@ -326,8 +326,8 @@
                 act[:, at : at + 128] = (y * sigmoid(y)).astype(BF16)
 
     acc = jnp.zeros(out_ref.shape, F32)
-    for b in range(8):
-        acc += dot(act[:, 128 * b : 128 * (b + 1)], w_ref[b], NT)
+    for c in range(2):
+        acc += dot(act[:, 512 * c : 512 * (c + 1)], w_ref[c], NT)
     out_ref[...] = acc.astype(BF16)
 
 
@@ -343,36 +343,32 @@
     tokens, norm_gain, rec_query, rec_input, rec_forward, rec_backward, forget_gap, log_decay,
     rec_gain, conv_value, conv_gate, conv_kernel, conv_gain, out_rec, out_conv,
 ):
-    y, z, xi = lax.axis_index(Y), lax.axis_index(Z), lax.axis_index(X)
-
+    y, z = lax.axis_index(Y), lax.axis_index(Z)
+
+    first = pl.pallas_call(
+        first_kernel, out_shape=jax.ShapeDtypeStruct((8, 32, 896), BF16), name="first"
+    )(
+        rec_forward, rec_backward, rec_query, conv_value, conv_gate, rec_input, log_decay[0],
+        out_rec.T, out_conv.T,
+    )
+    first = lax.all_to_all(first, Y, split_axis=0, concat_axis=0, tiled=True)
     normed = pl.pallas_call(
         norm_kernel, out_shape=jax.ShapeDtypeStruct((64, 2048), BF16), name="norm"
     )(tokens[0], norm_gain.reshape(1, 2048))
     seq = lax.all_gather(normed, (Y, C), axis=0, tiled=True)
-
-    first = pl.pallas_call(
-        first_kernel,
-        in_specs=[pl.BlockSpec(memory_space=pltpu.SMEM)]
-        + [pl.BlockSpec(memory_space=pltpu.VMEM)] * 9,
-        out_shape=jax.ShapeDtypeStruct((8, 32, 512), BF16),
-        name="first",
-    )(
-        xi.reshape(1).astype(jnp.int32), rec_forward, rec_backward, rec_query, conv_value,
-        conv_gate, rec_input, log_decay[0], out_rec, out_conv,
-    )
-    first = lax.all_to_all(first, Y, split_axis=0, concat_axis=0, tiled=True)
-    second, out_cols, decays = pl.pallas_call(
+    second, second2, out_cols, decays = pl.pallas_call(
         second_kernel,
         out_shape=[
-            jax.ShapeDtypeStruct((8, 288, 256), BF16),
-            jax.ShapeDtypeStruct((256, 128), BF16),
+            jax.ShapeDtypeStruct((224, 256), BF16),
+            jax.ShapeDtypeStruct((8, 64, 256), BF16),
+            jax.ShapeDtypeStruct((256, 512), BF16),
             jax.ShapeDtypeStruct((8, 2, 128), F32),
         ],
         name="second",
     )(first)
-    weights = lax.all_to_all(second, Z, split_axis=0, concat_axis=0, tiled=True)
-    out_w = lax.all_gather(out_cols, Z, axis=0, tiled=True)
-    out_w = lax.all_gather(out_w, (C, X), axis=0)
+    weights2 = lax.all_to_all(second2, Z, split_axis=0, concat_axis=0, tiled=True)
+    weights = lax.all_gather(second, Z, axis=0)
+    out_w = lax.all_gather(out_cols, (C, Z), axis=0, tiled=True).reshape(2, 2048, 512)
 
     gains = lax.all_gather(jnp.stack([rec_gain, conv_gain]), C)
     rec_gains = gains[:, 0].reshape(4, 128)
@@ -389,7 +385,8 @@
         grid=(n // tile,),
         in_specs=[
             spec((tile, 2048), lambda i: (i, 0)),
-            full((8, 288, 256)),
+            full((8, 224, 256)),
+            full((8, 64, 256)),
             spec((tile // 128, 2, 128), lambda i: (i, 0, 0)),
             full((1, 128)),
         ],
@@ -415,7 +412,7 @@
             pltpu.VMEM((16, 64, 128), F32), pltpu.VMEM((16, 8, 128), F32), pltpu.VMEM((16, 128), F32)
         ],
         name="states",
-    )(seq, weights, decays, gap)
+    )(seq, weights, weights2, decays, gap)
 
     arrived = lax.all_to_all(sent, Z, split_axis=0, concat_axis=0, tiled=True)
     local, decayed, convolved, edges = pl.pallas_call(
@@ -442,7 +439,7 @@
         grid=(4,),
         in_specs=[
             full((16, 80, 128)), full((4, 128)), full((4, 128)),
-            spec((8, 512, 128), lambda i: (0, i, 0)),
+            spec((2, 512, 512), lambda i: (0, i, 0)),
         ],
         out_specs=spec((64, 512), lambda i: (0, i)),
         out_shape=jax.ShapeDtypeStruct((64, 2048), BF16),

time: 157 us -> 142 us (0.904)
  waiting for transfers between devices: 37.9 us -> 16.1 us
  starting transfers between devices: 19.9 us -> 33.1 us
  blocking collectives: 50.2 us -> 47.5 us
  local copies, waits for them, and re-layouts: 6.9 us -> 4.28 us
    all_to_all x1, waiting for transfers between devices: 23.7 us -> 0.01 us  [body(): lax.all_to_all(second2, Z, split_axis=0, concat_axis=0, tiled=True)]
    all_to_all x1, starting transfers between devices: 4 us -> 14.5 us  [body(): lax.all_to_all(second2, Z, split_axis=0, concat_axis=0, tiled=True)]
    all_gather x1, blocking collectives: 31.2 us -> 25.6 us  [body(): weights = lax.all_gather(second, Z, axis=0)]
    unnamed x17 -> x13, local copies, waits for them, and re-layouts: 5.42 us -> 2.12 us
    all_to_all x1, blocking collectives: 17.2 us -> 20 us  [body(): first = lax.all_to_all(first, Y, split_axis=0, concat_axis=0, tiled=True)]
    all_to_all x1, starting transfers between devices: 3.4 us -> 5.73 us  [body(): arrived = lax.all_to_all(sent, Z, split_axis=0, concat_axis=0, tiled=True)]
    all_to_all x1, waiting for transfers between devices: 3.29 us -> 5.23 us  [body(): arrived = lax.all_to_all(sent, Z, split_axis=0, concat_axis=0, tiled=True)]
  transfers between devices with their start and end apart: 5 -> 5, of which waited for: 3 -> 2; matrix products, arithmetic and copies ran while one was open for 3% -> 2% of each run, Pallas kernels for 13% -> 14%
where the time goes in v3:
time: 142 us; the launch traced here: 141 us
  blocking collectives  47.5 us (33%)
  starting transfers between devices  33.1 us (23%)
  Pallas kernels  26.3 us (19%)
  waiting for transfers between devices  16.1 us (11%)
  between operations  13.5 us (10%)
  local copies, waits for them, and re-layouts  4.28 us (3%)
    all_gather x1, blocking collectives, body(): weights = lax.all_gather(second, Z, axis=0)  25.6 us
    all_to_all x1, blocking collectives, body(): first = lax.all_to_all(first, Y, split_axis=0, concat_axis=0, tiled=True)  20 us
    all_to_all x1, starting transfers between devices, body(): lax.all_to_all(second2, Z, split_axis=0, concat_axis=0, tiled=True)  14.5 us
    all_to_all x1, starting transfers between devices, body(): lax.all_to_all(merged, (Y, C), split_axis=0, concat_axis=0, tiled=True)  12.8 us
    all_to_all x1, waiting for transfers between devices, body(): lax.all_to_all(merged, (Y, C), split_axis=0, concat_axis=0, tiled=True)  10.8 us
    pallas_call x1, Pallas kernels, body(): pl.pallas_call(states_kernel, grid=(n // tile,), in_specs=[spec((tile, 20...  8.6 us
    all_to_all x1, starting transfers between devices, body(): arrived = lax.all_to_all(sent, Z, split_axis=0, concat_axis=0, tiled=True)  5.73 us
    all_to_all x1, waiting for transfers between devices, body(): arrived = lax.all_to_all(sent, Z, split_axis=0, concat_axis=0, tiled=True)  5.23 us
  transfers between devices with their start and end apart: 5, of which 2 were waited for; matrix products, arithmetic and copies ran while one was open for 2% of the time, Pallas kernels for 14%

profile of v3, /device:TPU:1, one launch (start us, length us, event | category | flops | bytes accessed | tf_op | source)
XLA Modules:
  0.0 141.2 jit_solution(10493926098891268443)
XLA Ops:
  6.5 0.0 all-gather.6.cloned.1.call-start
  6.5 1.8 %norm.1 = bf16[64,2048]{1,0:T(8,128)(2,1)} custom-call(bf16[64,2048]{1,0:T(8,128)(2,1)} %bitcast.23, f32[1,2048]{1,0:T(1,128)} %bitcast.27), custom_call_target="tpu_custom_call" | custom-call | tf_op jit(solution)/shard_map/norm/pallas_call | solution.py:355
  8.4 0.0 all-gather.6.cloned.1.call-update
  8.4 0.0 all-gather.8.cloned.1.call-start
  8.4 1.8 %first.1 = bf16[8,32,896]{2,1,0:T(8,128)(2,1)} custom-call(bf16[32,256]{1,0:T(8,128)(2,1)} %rf_ref.1, bf16[32,256]{1,0:T(8,128)(2,1)} %rb_ref.1, bf16[32,256]{1,0:T(8,128)(2,1)} %rq_ref.1, bf16[32,256]{1,0:T(8,128)(2,1)} %cv_ref.1, bf16[32,256]{1,0:T(8,128)(2,1)} %cg_ref.1, bf16[32,256]{1,0:T(8,128)(2,1)} %ri_ref.1, f32[2,2,128]{2,1,0:T(2,128)} %bitcast.30, ...), custom_call_target="tpu_custom_call" | custom-call | tf_op jit(solution)/shard_map/first/pallas_call | solution.py:348
  10.2 20.0 %all_to_all.20.first_ref = bf16[8,32,896]{2,1,0:T(8,128)(2,1)} all-to-all(bf16[8,32,896]{2,1,0:T(8,128)(2,1)} %first.1), channel_id=1, replica_groups=mesh['sp_0'=8,'sp_1'=8,'fs'=4,'tp'=2] {'sp_1'}, dimensions={0} | all-to-all | bytes 917504 | tf_op jit(solution)/shard_map/all_to_all | solution.py:354
  30.2 0.0 copy-start.3
  30.2 2.0 %second.1 = (bf16[224,256]{1,0:T(8,128)(2,1)}, bf16[8,64,256]{2,1,0:T(8,128)(2,1)}, bf16[256,512]{1,0:T(8,128)(2,1)}, f32[8,2,128]{2,1,0:T(2,128)}) custom-call(bf16[8,32,896]{2,1,0:T(8,128)(2,1)} %all_to_all.20.first_ref), custom_call_target="tpu_custom_call" | custom-call | tf_op jit(solution)/shard_map/second/pallas_call | solution.py:359
  32.3 0.0 all-gather.8.cloned.1.call-update
  32.3 0.8 reshape.23
  33.1 14.5 %all-to-all-start.1 = ((bf16[8,64,256]{2,1,0:T(8,128)(2,1)}), bf16[8,64,256]{2,1,0:T(8,128)(2,1)S(1)}, u32[]{:S(2)}, u32[]{:S(2)}) async-start(bf16[8,64,256]{2,1,0:T(8,128)(2,1)} %get-tuple-element.21), calls=%async_computation.1 | async-start | bytes 524288 | tf_op jit(solution)/shard_map/all_to_all | solution.py:369
  47.6 0.1 reshape.24
  47.6 0.6 pad.10.gap_ref
  48.2 25.6 %all-gather = bf16[1792,256]{1,0:T(8,128)(2,1)} all-gather(bf16[224,256]{1,0:T(8,128)(2,1)} %get-tuple-element.20), channel_id=2, replica_groups=mesh['sp_0'=8,'sp_1'=8,'fs'=4,'tp'=2] {'sp_0'}, dimensions={0}, use_global_device_ids=true | all-gather | bytes 1032192 | tf_op jit(solution)/shard_map/all_gather | solution.py:370
  73.8 0.0 all-to-all-done.1.w2_ref
  73.8 0.0 copy-start.1
  73.8 0.0 all-gather.6.cloned.1.call-done.x_ref
  73.8 0.7 copy-done.1
  74.5 0.0 copy-start.4
  74.5 0.0 copy-start.5
  74.5 8.6 %states.1 = (bf16[1024,128]{1,0:T(8,128)(2,1)}, bf16[1024,128]{1,0:T(8,128)(2,1)}, f32[1024,128]{1,0:T(8,128)}, bf16[1024,32]{1,0:T(8,128)(2,1)}, bf16[8,96,128]...) custom-call(bf16[1024,2048]{1,0:T(8,128)(2,1)} %all-gather.6.cloned.1.call-done.x_ref, ...), custom_call_target="tpu_custom_call" | custom-call | tf_op jit(solution)/shard_map/states/pallas_call | solution.py:383
  83.1 5.7 %all-to-all-start.2 = ((bf16[8,96,128]{2,1,0:T(8,128)(2,1)}), bf16[8,96,128]{2,1,0:T(8,128)(2,1)S(1)}, u32[]{:S(2)}, u32[]{:S(2)}) async-start(bf16[8,96,128]{2,1,0:T(8,128)(2,1)} %get-tuple-element.23), calls=%async_computation.2 | async-start | bytes 393216 | tf_op jit(solution)/shard_map/all_to_all | solution.py:417
  88.9 0.0 copy-done.3
  88.9 0.1 reshape.25
  89.0 0.6 pad_convert_fusion.taps_ref
  89.6 4.5 %local.1 = (f32[1024,128]{1,0:T(8,128)}, bf16[1024,128]{1,0:T(8,128)(2,1)}, bf16[16,16,128]{2,1,0:T(8,128)(2,1)}, f32[2,16,32]{2,1,0:T(8,128)}) custom-call(bf16[1024,128]{1,0:T(8,128)(2,1)} %get-tuple-element.24.a_ref, bf16[1024,128]{1,0:T(8,128)(2,1)} %get-tuple-element.25.v_ref, f32[1024,128]{1,0:T(8,128)} %get-tuple-element.26.c_ref, ...), custom_call_target="tpu_custom_call" | custom-call | tf_op jit(solution)/shard_map/local/pallas_call | solution.py:418
  94.1 5.2 %all-to-all-done.2.recv_ref = bf16[8,96,128]{2,1,0:T(8,128)(2,1)S(1)} async-done(((bf16[8,96,128]{2,1,0:T(8,128)(2,1)}), bf16[8,96,128]{2,1,0:T(8,128)(2,1)S(1)}, u32[]{:S(2)}, u32[]{:S(2)}) %all-to-all-start.2) | async-done | bytes 196640 | tf_op jit(solution)/shard_map/all_to_all | solution.py:417
  99.3 0.0 copy-start.2
  99.3 0.7 copy-done.2
  100.0 2.5 %merge.1 = bf16[16,80,128]{2,1,0:T(8,128)(2,1)} custom-call(s32[1]{0:T(128)} %bitcast.z_ref, bf16[8,96,128]{2,1,0:T(8,128)(2,1)} %copy-done.2, f32[1024,128]{1,0:T(8,128)} %get-tuple-element.30.local_ref, bf16[1024,128]{1,0:T(8,128)(2,1)} %get-tuple-element.31.qd_ref, bf16[16,16,128]{2,1,0:T(8,128)(2,1)} %get-tuple-element.32.conv_ref, ...), custom_call_target="tpu_custom_call" | custom-call | tf_op jit(solution)/shard_map/merge/pallas_call | solution.py:429
  102.5 12.8 %all-to-all-start.3 = ((bf16[16,80,128]{2,1,0:T(8,128)(2,1)}), bf16[16,80,128]{2,1,0:T(8,128)(2,1)S(1)}, u32[]{:S(2)}, u32[]{:S(2)}) async-start(bf16[16,80,128]{2,1,0:T(8,128)(2,1)} %merge.1), calls=%async_computation.3 | async-start | bytes 655360 | tf_op jit(solution)/shard_map/all_to_all | solution.py:436
  115.3 0.0 copy-done.4
  115.3 0.0 copy-done.5
  115.4 1.8 %all-gather.2 = f32[2,2,256]{2,1,0:T(2,128)S(1)} all-gather(f32[1,2,256]{2,1,0:T(2,128)S(1)} %maximum_bitcast_fusion), channel_id=3, replica_groups=mesh['sp_0'=8,'sp_1'=8,'fs'=4,'tp'=2] {'tp'}, dimensions={0}, use_global_device_ids=true | all-gather | bytes 6144 | tf_op jit(solution)/shard_map/all_gather | solution.py:373
  117.2 0.6 fusion
  117.8 0.0 all-gather.8.cloned.1.call-done
  117.8 10.8 %all-to-all-done.3.recv_ref = bf16[16,80,128]{2,1,0:T(8,128)(2,1)S(1)} async-done(((bf16[16,80,128]{2,1,0:T(8,128)(2,1)}), bf16[16,80,128]{2,1,0:T(8,128)(2,1)S(1)}, u32[]{:S(2)}, u32[]{:S(2)}) %all-to-all-start.3) | async-done | bytes 327712 | tf_op jit(solution)/shard_map/all_to_all | solution.py:436
  128.6 0.0 copy-start
  128.6 0.7 copy-done
  129.3 5.1 %output.1 = bf16[64,2048]{1,0:T(8,128)(2,1)} custom-call(bf16[16,80,128]{2,1,0:T(8,128)(2,1)} %copy-done, f32[4,128]{1,0:T(4,128)} %bitcast.29, f32[4,128]{1,0:T(4,128)} %bitcast.28, bf16[2,2048,512]{2,1,0:T(8,128)(2,1)} %bitcast.21), custom_call_target="tpu_custom_call" | custom-call | tf_op jit(solution)/shard_map/output/pallas_call | solution.py:437
  (4 shorter events, 0.0 us)
Async XLA Ops:
  6.5 67.3 %all-gather.6.cloned.1.call-start = ((), (), s32[]{:S(2)}) async-start(), calls=%async_computation.4 | async-start | bytes 4456448 | tf_op jit(solution)/shard_map/all_gather | solution.py:358
  8.4 109.4 %all-gather.8.cloned.1.call-start = ((), (), s32[]{:S(2)}) async-start(), calls=%async_computation.5 | async-start | bytes 4456448 | tf_op jit(solution)/shard_map/all_gather | solution.py:371
  30.2 58.6 %copy-start.3 = (bf16[31,256]{1,0:T(8,128)(2,1)S(1)}, bf16[31,256]{1,0:T(8,128)(2,1)}, u32[]{:S(2)}) copy-start(bf16[31,256]{1,0:T(8,128)(2,1)} %param.26) | copy-start | bytes 47620
  33.1 40.8 %all-to-all-start.1 = ((bf16[8,64,256]{2,1,0:T(8,128)(2,1)}), bf16[8,64,256]{2,1,0:T(8,128)(2,1)S(1)}, u32[]{:S(2)}, u32[]{:S(2)}) async-start(bf16[8,64,256]{2,1,0:T(8,128)(2,1)} %get-tuple-element.21), calls=%async_computation.1 | async-start | bytes 524288 | tf_op jit(solution)/shard_map/all_to_all | solution.py:369
  73.8 0.7 copy-start.1
  74.5 40.8 %copy-start.4 = (f32[256]{0:T(256)S(1)}, f32[256]{0:T(256)}, u32[]{:S(2)}) copy-start(f32[256]{0:T(256)} %param.27) | copy-start | bytes 3076
  74.5 40.8 %copy-start.5 = (f32[256]{0:T(256)S(1)}, f32[256]{0:T(256)}, u32[]{:S(2)}) copy-start(f32[256]{0:T(256)} %param.23) | copy-start | bytes 3076
  83.1 16.2 %all-to-all-start.2 = ((bf16[8,96,128]{2,1,0:T(8,128)(2,1)}), bf16[8,96,128]{2,1,0:T(8,128)(2,1)S(1)}, u32[]{:S(2)}, u32[]{:S(2)}) async-start(bf16[8,96,128]{2,1,0:T(8,128)(2,1)} %get-tuple-element.23), calls=%async_computation.2 | async-start | bytes 393216 | tf_op jit(solution)/shard_map/all_to_all | solution.py:417
  99.3 0.7 copy-start.2
  102.5 26.1 %all-to-all-start.3 = ((bf16[16,80,128]{2,1,0:T(8,128)(2,1)}), bf16[16,80,128]{2,1,0:T(8,128)(2,1)S(1)}, u32[]{:S(2)}, u32[]{:S(2)}) async-start(bf16[16,80,128]{2,1,0:T(8,128)(2,1)} %merge.1), calls=%async_computation.3 | async-start | bytes 655360 | tf_op jit(solution)/shard_map/all_to_all | solution.py:436
  128.6 0.7 copy-start
Sparse Core Ops, SparseCore 0:
  9.4 50.6 all-gather.5
  62.3 48.2 all-gather.7

commit v4 on v3

--- a/solution.py
+++ b/solution.py
@@ -45,15 +45,14 @@
     return gap * sigmoid(-a)
 
 
-def norm_kernel(x_ref, gain_ref, out_ref):
-    x = x_ref[...].astype(F32)
-    scale = lax.rsqrt(jnp.mean(x * x, axis=1, keepdims=True) + EPS)
-    out_ref[...] = (x * scale * gain_ref[...]).astype(BF16)
-
-
-def first_kernel(
-    rf_ref, rb_ref, rq_ref, cv_ref, cg_ref, ri_ref, ld_ref, rec_ref, conv_ref, out_ref
+def start_kernel(
+    x_ref, gain_ref, rf_ref, rb_ref, rq_ref, cv_ref, cg_ref, ri_ref, ld_ref, rec_ref, conv_ref,
+    norm_ref, out_ref,
 ):
+    for r in range(0, 64, 16):
+        x = x_ref[r : r + 16, :].astype(F32)
+        scale = lax.rsqrt(jnp.mean(x * x, axis=1, keepdims=True) + EPS)
+        norm_ref[r : r + 16, :] = (x * scale * gain_ref[...]).astype(BF16)
     group = lanes(32) // 32
     row = lax.broadcasted_iota(jnp.int32, (32, 128), 0)
     for m in range(2):
@@ -86,7 +85,11 @@
             out_ref[y, :, 640:896] = conv_ref[...]
 
 
-def second_kernel(first_ref, w_ref, w2_ref, cols_ref, ld_ref):
+def second_kernel(
+    first_ref, gap_ref, taps_ref, w_ref, w2_ref, cols_ref, ld_ref, gap_out, taps_out
+):
+    gap_out[...] = gap_ref[...]
+    taps_out[...] = taps_ref[...]
     lane = lanes(8)
     keys, values, gates = [], [], []
     for y in range(8):
@@ -331,6 +334,14 @@
     out_ref[...] = acc.astype(BF16)
 
 
+def near(x):
+    return pltpu.with_memory_space_constraint(x, pltpu.VMEM)
+
+
+def kept(shape, dtype):
+    return pltpu.VMEM(shape, dtype)
+
+
 def full(shape):
     return pl.BlockSpec(shape, lambda *_: (0,) * len(shape))
 
@@ -345,39 +356,39 @@
 ):
     y, z = lax.axis_index(Y), lax.axis_index(Z)
 
-    first = pl.pallas_call(
-        first_kernel, out_shape=jax.ShapeDtypeStruct((8, 32, 896), BF16), name="first"
-    )(
-        rec_forward, rec_backward, rec_query, conv_value, conv_gate, rec_input, log_decay[0],
-        out_rec.T, out_conv.T,
-    )
-    first = lax.all_to_all(first, Y, split_axis=0, concat_axis=0, tiled=True)
-    normed = pl.pallas_call(
-        norm_kernel, out_shape=jax.ShapeDtypeStruct((64, 2048), BF16), name="norm"
-    )(tokens[0], norm_gain.reshape(1, 2048))
-    seq = lax.all_gather(normed, (Y, C), axis=0, tiled=True)
-    second, second2, out_cols, decays = pl.pallas_call(
-        second_kernel,
-        out_shape=[
-            jax.ShapeDtypeStruct((224, 256), BF16),
-            jax.ShapeDtypeStruct((8, 64, 256), BF16),
-            jax.ShapeDtypeStruct((256, 512), BF16),
-            jax.ShapeDtypeStruct((8, 2, 128), F32),
-        ],
-        name="second",
-    )(first)
-    weights2 = lax.all_to_all(second2, Z, split_axis=0, concat_axis=0, tiled=True)
-    weights = lax.all_gather(second, Z, axis=0)
-    out_w = lax.all_gather(out_cols, (C, Z), axis=0, tiled=True).reshape(2, 2048, 512)
-
-    gains = lax.all_gather(jnp.stack([rec_gain, conv_gain]), C)
-    rec_gains = gains[:, 0].reshape(4, 128)
-    conv_gains = gains[:, 1].reshape(4, 128)
     gap = lax.dynamic_index_in_dim(forget_gap.reshape(2, 8, 32), y, 1, keepdims=False)
     gap = jnp.pad(gap.reshape(1, 64), ((0, 0), (0, 64)))
     taps = lax.dynamic_index_in_dim(conv_kernel.reshape(31, 8, 32), y, 1, keepdims=False)
     taps = jnp.pad(taps.astype(F32), ((0, 1), (0, 0)))
-
+    normed, first = pl.pallas_call(
+        start_kernel,
+        out_shape=[kept((64, 2048), BF16), kept((8, 32, 896), BF16)],
+        name="start",
+    )(
+        tokens[0], norm_gain.reshape(1, 2048), rec_forward, rec_backward, rec_query, conv_value,
+        conv_gate, rec_input, log_decay[0], out_rec.T, out_conv.T,
+    )
+    seq = lax.all_gather(normed, (Y, C), axis=0, tiled=True)
+    first = lax.all_to_all(first, Y, split_axis=0, concat_axis=0, tiled=True)
+    second, second2, out_cols, decays, gap, taps = pl.pallas_call(
+        second_kernel,
+        out_shape=[
+            kept((224, 256), BF16),
+            kept((8, 64, 256), BF16),
+            jax.ShapeDtypeStruct((256, 512), BF16),
+            kept((8, 2, 128), F32),
+            kept((1, 128), F32),
+            kept((32, 32), F32),
+        ],
+        name="second",
+    )(near(first), near(gap), near(taps))
+    weights2 = lax.all_to_all(second2, Z, split_axis=0, concat_axis=0, tiled=True)
+    weights = lax.all_gather(second, Z, axis=0)
+    out_w = lax.all_gather(out_cols, (C, Z), axis=0, tiled=True).reshape(2, 2048, 512)
+
+    gains = lax.all_gather(jnp.stack([rec_gain, conv_gain]), C)
+    rec_gains = gains[:, 0].reshape(4, 128)
+    conv_gains = gains[:, 1].reshape(4, 128)
     n = seq.shape[0]
     tile = 256
     pre_a, pre_v, cum, gated, sent, before, offset = pl.pallas_call(
@@ -412,27 +423,27 @@
             pltpu.VMEM((16, 64, 128), F32), pltpu.VMEM((16, 8, 128), F32), pltpu.VMEM((16, 128), F32)
         ],
         name="states",
-    )(seq, weights, weights2, decays, gap)
+    )(seq, near(weights), near(weights2), near(decays), near(gap))
 
     arrived = lax.all_to_all(sent, Z, split_axis=0, concat_axis=0, tiled=True)
     local, decayed, convolved, edges = pl.pallas_call(
         local_kernel,
         out_shape=[
-            jax.ShapeDtypeStruct((n, 128), F32),
-            jax.ShapeDtypeStruct((n, 128), BF16),
-            jax.ShapeDtypeStruct((16, 16, 128), BF16),
-            jax.ShapeDtypeStruct((2, 16, 32), F32),
+            kept((n, 128), F32),
+            kept((n, 128), BF16),
+            kept((16, 16, 128), BF16),
+            kept((2, 16, 32), F32),
         ],
         scratch_shapes=[pltpu.VMEM((n + 32, 32), F32)],
         name="local",
-    )(pre_a, pre_v, cum, gap, before, offset, gated, taps)
+    )(near(pre_a), near(pre_v), near(cum), near(gap), near(before), near(offset), near(gated), near(taps))
     merged = pl.pallas_call(
         merge_kernel,
         in_specs=[pl.BlockSpec(memory_space=pltpu.SMEM)]
         + [pl.BlockSpec(memory_space=pltpu.VMEM)] * 6,
-        out_shape=jax.ShapeDtypeStruct((16, 80, 128), BF16),
+        out_shape=kept((16, 80, 128), BF16),
         name="merge",
-    )(z.reshape(1).astype(jnp.int32), arrived, local, decayed, convolved, edges, taps)
+    )(z.reshape(1).astype(jnp.int32), near(arrived), near(local), near(decayed), near(convolved), near(edges), near(taps))
     mine = lax.all_to_all(merged, (Y, C), split_axis=0, concat_axis=0, tiled=True)
     mixed = pl.pallas_call(
         output_kernel,
@@ -445,7 +456,7 @@
         out_shape=jax.ShapeDtypeStruct((64, 2048), BF16),
         scratch_shapes=[pltpu.VMEM((64, 1024), BF16)],
         name="output",
-    )(mine, rec_gains, conv_gains, out_w)
+    )(near(mine), rec_gains, conv_gains, out_w)
     return mixed[None]
 
 

time: 142 us -> 132 us (0.930)
  blocking collectives: 47.5 us -> 26.8 us
  waiting for transfers between devices: 16.1 us -> 24.5 us
  Pallas kernels: 26.3 us -> 19.9 us
  starting transfers between devices: 33.1 us -> 38.1 us
  local copies, waits for them, and re-layouts: 4.28 us -> 8.04 us
    all_to_all x1 -> x0, blocking collectives: 20 us -> none  [body(): first = lax.all_to_all(first, Y, split_axis=0, concat_axis=0, tiled=True)]
    all_to_all x0 -> x1, waiting for transfers between devices: none -> 11.3 us  [body(): first = lax.all_to_all(first, Y, split_axis=0, concat_axis=0, tiled=True)]
    all_to_all x0 -> x1, starting transfers between devices: none -> 7.65 us  [body(): first = lax.all_to_all(first, Y, split_axis=0, concat_axis=0, tiled=True)]
    pallas_call x4 -> x3, Pallas kernels: 10.1 us -> 5.38 us  [the longest x1 2.34 us: body(): pl.pallas_call(local_kernel, out_shape=[kept((n, 128), F32), kept((n, 128...]
    unnamed x13 -> x17, local copies, waits for them, and re-layouts: 2.12 us -> 5.75 us
    all_to_all x1, waiting for transfers between devices: 5.23 us -> 2.36 us  [body(): arrived = lax.all_to_all(sent, Z, split_axis=0, concat_axis=0, tiled=True)]
    all_to_all x1, starting transfers between devices: 12.8 us -> 10.7 us  [body(): lax.all_to_all(merged, (Y, C), split_axis=0, concat_axis=0, tiled=True)]
    all_gather x1, waiting for transfers between devices: 0.01 us -> 1.43 us  [body(): lax.all_gather(out_cols, (C, Z), axis=0, tiled=True).reshape(2, 2048, 512)]
  transfers between devices with their start and end apart: 5 -> 6, of which waited for: 2 -> 4; matrix products, arithmetic and copies ran while one was open for 2% -> 2% of each run, Pallas kernels for 14% -> 10%
where the time goes in v4:
time: 132 us; the launch traced here: 131 us
  starting transfers between devices  38.1 us (29%)
  blocking collectives  26.8 us (20%)
  waiting for transfers between devices  24.5 us (19%)
  Pallas kernels  19.9 us (15%)
  between operations  13.5 us (10%)
  local copies, waits for them, and re-layouts  8.04 us (6%)
    all_gather x1, blocking collectives, body(): weights = lax.all_gather(second, Z, axis=0)  25 us
    all_to_all x1, starting transfers between devices, body(): lax.all_to_all(second2, Z, split_axis=0, concat_axis=0, tiled=True)  14.2 us
    all_to_all x1, waiting for transfers between devices, body(): first = lax.all_to_all(first, Y, split_axis=0, concat_axis=0, tiled=True)  11.3 us
    all_to_all x1, starting transfers between devices, body(): lax.all_to_all(merged, (Y, C), split_axis=0, concat_axis=0, tiled=True)  10.7 us
    all_to_all x1, waiting for transfers between devices, body(): lax.all_to_all(merged, (Y, C), split_axis=0, concat_axis=0, tiled=True)  9.38 us
    pallas_call x1, Pallas kernels, body(): pl.pallas_call(states_kernel, grid=(n // tile,), in_specs=[spec((tile, 20...  8.23 us
    all_to_all x1, starting transfers between devices, body(): first = lax.all_to_all(first, Y, split_axis=0, concat_axis=0, tiled=True)  7.65 us
    unnamed x17, local copies, waits for them, and re-layouts  5.75 us
  transfers between devices with their start and end apart: 6, of which 4 were waited for; matrix products, arithmetic and copies ran while one was open for 2% of the time, Pallas kernels for 10%

profile of v4, /device:TPU:1, one launch (start us, length us, event | category | flops | bytes accessed | tf_op | source)
XLA Modules:
  0.0 130.9 jit_solution(7135428138625454135)
XLA Ops:
  6.5 0.0 all-gather.6.cloned.1.call-start
  6.5 2.1 %start.1 = (bf16[64,2048]{1,0:T(8,128)(2,1)}, bf16[8,32,896]{2,1,0:T(8,128)(2,1)}) custom-call(bf16[64,2048]{1,0:T(8,128)(2,1)} %bitcast.23, f32[1,2048]{1,0:T(1,128)} %bitcast.29, bf16[32,256]{1,0:T(8,128)(2,1)} %rf_ref.1, bf16[32,256]{1,0:T(8,128)(2,1)} %rb_ref.1, bf16[32,256]{1,0:T(8,128)(2,1)} %rq_ref.1, bf16[32,256]{1,0:T(8,128)(2,1)} %cv_ref.1, ...), custom_call_target="tpu_custom_call" | custom-call | tf_op jit(solution)/shard_map/start/pallas_call | solution.py:363
  8.6 0.0 all-gather.6.cloned.1.call-update
  8.7 7.7 %all-to-all-start = ((bf16[8,32,896]{2,1,0:T(8,128)(2,1)}), bf16[8,32,896]{2,1,0:T(8,128)(2,1)S(1)}, u32[]{:S(2)}, u32[]{:S(2)}) async-start(bf16[8,32,896]{2,1,0:T(8,128)(2,1)} %get-tuple-element.25), calls=%async_computation | async-start | bytes 917504 | tf_op jit(solution)/shard_map/all_to_all | solution.py:372
  16.3 0.0 all-gather.8.cloned.1.call-start
  16.4 0.8 reshape.25
  17.2 0.8 reshape.23
  18.0 0.1 reshape.24
  18.1 11.3 %all-to-all-done.first_ref = bf16[8,32,896]{2,1,0:T(8,128)(2,1)S(1)} async-done(((bf16[8,32,896]{2,1,0:T(8,128)(2,1)}), bf16[8,32,896]{2,1,0:T(8,128)(2,1)S(1)}, u32[]{:S(2)}, u32[]{:S(2)}) %all-to-all-start) | async-done | bytes 458784 | tf_op jit(solution)/shard_map/all_to_all | solution.py:372
  29.4 0.9 second.1
  30.4 0.0 all-gather.8.cloned.1.call-update
  30.4 14.2 %all-to-all-start.1 = ((bf16[8,64,256]{2,1,0:T(8,128)(2,1)}), bf16[8,64,256]{2,1,0:T(8,128)(2,1)S(1)}, u32[]{:S(2)}, u32[]{:S(2)}) async-start(bf16[8,64,256]{2,1,0:T(8,128)(2,1)} %get-tuple-element.27), calls=%async_computation.1 | async-start | bytes 524288 | tf_op jit(solution)/shard_map/all_to_all | solution.py:385
  44.5 25.0 %all-gather = bf16[1792,256]{1,0:T(8,128)(2,1)S(1)} all-gather(bf16[224,256]{1,0:T(8,128)(2,1)S(1)} %get-tuple-element.26), channel_id=2, replica_groups=mesh['sp_0'=8,'sp_1'=8,'fs'=4,'tp'=2] {'sp_0'}, dimensions={0}, use_global_device_ids=true | all-gather | bytes 1032192 | tf_op jit(solution)/shard_map/all_gather | solution.py:386
  69.5 0.0 all-to-all-done.1.w2_ref
  69.6 0.0 all-gather.6.cloned.1.call-done.x_ref
  69.6 0.0 copy-start.6
  69.6 0.0 copy-start.7
  69.6 8.2 %states.1 = (bf16[1024,128]{1,0:T(8,128)(2,1)}, bf16[1024,128]{1,0:T(8,128)(2,1)}, f32[1024,128]{1,0:T(8,128)}, bf16[1024,32]{1,0:T(8,128)(2,1)}, bf16[8,96,128]...) custom-call(bf16[1024,2048]{1,0:T(8,128)(2,1)} %all-gather.6.cloned.1.call-done.x_ref, ...), custom_call_target="tpu_custom_call" | custom-call | tf_op jit(solution)/shard_map/states/pallas_call | solution.py:394
  77.8 5.5 %all-to-all-start.2 = ((bf16[8,96,128]{2,1,0:T(8,128)(2,1)}), bf16[8,96,128]{2,1,0:T(8,128)(2,1)S(1)}, u32[]{:S(2)}, u32[]{:S(2)}) async-start(bf16[8,96,128]{2,1,0:T(8,128)(2,1)} %get-tuple-element.30), calls=%async_computation.2 | async-start | bytes 393216 | tf_op jit(solution)/shard_map/all_to_all | solution.py:428
  83.3 0.0 copy-start
  83.3 1.1 copy-done
  84.4 0.0 copy-start.1
  84.4 1.0 copy-done.1
  85.3 0.0 copy-start.2
  85.3 1.0 copy-done.2
  86.3 0.0 copy-start.3
  86.3 1.0 copy-done.3
  87.2 0.0 copy-start.4
  87.3 0.9 copy-done.4
  88.2 0.0 copy-start.5
  88.2 0.8 copy-done.5
  89.0 2.3 %local.1 = (f32[1024,128]{1,0:T(8,128)S(1)}, bf16[1024,128]{1,0:T(8,128)(2,1)S(1)}, bf16[16,16,128]{2,1,0:T(8,128)(2,1)S(1)}, f32[2,16,32]{2,1,0:T(8,128)S(1)}) custom-call(bf16[1024,128]{1,0:T(8,128)(2,1)S(1)} %copy-done.1, bf16[1024,128]{1,0:T(8,128)(2,1)S(1)} %copy-done.2, f32[1024,128]{1,0:T(8,128)S(1)} %copy-done, ...), custom_call_target="tpu_custom_call" | custom-call | tf_op jit(solution)/shard_map/local/pallas_call | solution.py:429
  91.4 2.4 %all-to-all-done.2.recv_ref = bf16[8,96,128]{2,1,0:T(8,128)(2,1)S(1)} async-done(((bf16[8,96,128]{2,1,0:T(8,128)(2,1)}), bf16[8,96,128]{2,1,0:T(8,128)(2,1)S(1)}, u32[]{:S(2)}, u32[]{:S(2)}) %all-to-all-start.2) | async-done | bytes 196640 | tf_op jit(solution)/shard_map/all_to_all | solution.py:428
  93.7 1.3 %merge.1 = bf16[16,80,128]{2,1,0:T(8,128)(2,1)} custom-call(s32[1]{0:T(128)} %bitcast.z_ref, bf16[8,96,128]{2,1,0:T(8,128)(2,1)S(1)} %all-to-all-done.2.recv_ref, f32[1024,128]{1,0:T(8,128)S(1)} %get-tuple-element.38.local_ref, bf16[1024,128]{1,0:T(8,128)(2,1)S(1)} %get-tuple-element.39.qd_ref, bf16[16,16,128]{2,1,0:T(8,128)(2,1)S(1)} %get-tuple-element.40.conv_ref, ...), custom_call_target="tpu_custom_call" | custom-call | tf_op jit(solution)/shard_map/merge/pallas_call | solution.py:440
  95.1 10.7 %all-to-all-start.3 = ((bf16[16,80,128]{2,1,0:T(8,128)(2,1)}), bf16[16,80,128]{2,1,0:T(8,128)(2,1)S(1)}, u32[]{:S(2)}, u32[]{:S(2)}) async-start(bf16[16,80,128]{2,1,0:T(8,128)(2,1)} %merge.1), calls=%async_computation.3 | async-start | bytes 655360 | tf_op jit(solution)/shard_map/all_to_all | solution.py:447
  105.8 0.0 copy-done.6
  105.8 0.0 copy-done.7
  105.8 1.8 %all-gather.2 = f32[2,2,256]{2,1,0:T(2,128)S(1)} all-gather(f32[1,2,256]{2,1,0:T(2,128)S(1)} %maximum_bitcast_fusion), channel_id=3, replica_groups=mesh['sp_0'=8,'sp_1'=8,'fs'=4,'tp'=2] {'tp'}, dimensions={0}, use_global_device_ids=true | all-gather | bytes 6144 | tf_op jit(solution)/shard_map/all_gather | solution.py:389
  107.7 0.6 fusion
  108.3 1.4 %all-gather.8.cloned.1.call-done = bf16[4096,512]{1,0:T(8,128)(2,1)} async-done(((bf16[256,512]{1,0:T(8,128)(2,1)}), bf16[4096,512]{1,0:T(8,128)(2,1)}) %all-gather.8.cloned.1.call-update) | async-done | bytes 4194320 | tf_op jit(solution)/shard_map/all_gather | solution.py:387
  109.7 9.4 %all-to-all-done.3.recv_ref = bf16[16,80,128]{2,1,0:T(8,128)(2,1)S(1)} async-done(((bf16[16,80,128]{2,1,0:T(8,128)(2,1)}), bf16[16,80,128]{2,1,0:T(8,128)(2,1)S(1)}, u32[]{:S(2)}, u32[]{:S(2)}) %all-to-all-start.3) | async-done | bytes 327712 | tf_op jit(solution)/shard_map/all_to_all | solution.py:447
  119.1 5.0 %output.1 = bf16[64,2048]{1,0:T(8,128)(2,1)} custom-call(bf16[16,80,128]{2,1,0:T(8,128)(2,1)S(1)} %all-to-all-done.3.recv_ref, f32[4,128]{1,0:T(4,128)} %bitcast.28, f32[4,128]{1,0:T(4,128)} %bitcast.27, bf16[2,2048,512]{2,1,0:T(8,128)(2,1)} %bitcast.22), custom_call_target="tpu_custom_call" | custom-call | tf_op jit(solution)/shard_map/output/pallas_call | solution.py:448
  (6 shorter events, 0.1 us)
Async XLA Ops:
  6.5 63.0 %all-gather.6.cloned.1.call-start = ((), (), s32[]{:S(2)}) async-start(), calls=%async_computation.4 | async-start | bytes 4456448 | tf_op jit(solution)/shard_map/all_gather | solution.py:371
  8.7 20.8 %all-to-all-start = ((bf16[8,32,896]{2,1,0:T(8,128)(2,1)}), bf16[8,32,896]{2,1,0:T(8,128)(2,1)S(1)}, u32[]{:S(2)}, u32[]{:S(2)}) async-start(bf16[8,32,896]{2,1,0:T(8,128)(2,1)} %get-tuple-element.25), calls=%async_computation | async-start | bytes 917504 | tf_op jit(solution)/shard_map/all_to_all | solution.py:372
  16.3 93.4 %all-gather.8.cloned.1.call-start = ((), (), s32[]{:S(2)}) async-start(), calls=%async_computation.5 | async-start | bytes 4456448 | tf_op jit(solution)/shard_map/all_gather | solution.py:387
  30.4 39.2 %all-to-all-start.1 = ((bf16[8,64,256]{2,1,0:T(8,128)(2,1)}), bf16[8,64,256]{2,1,0:T(8,128)(2,1)S(1)}, u32[]{:S(2)}, u32[]{:S(2)}) async-start(bf16[8,64,256]{2,1,0:T(8,128)(2,1)} %get-tuple-element.27), calls=%async_computation.1 | async-start | bytes 524288 | tf_op jit(solution)/shard_map/all_to_all | solution.py:385
  69.6 36.2 %copy-start.6 = (f32[256]{0:T(256)S(1)}, f32[256]{0:T(256)}, u32[]{:S(2)}) copy-start(f32[256]{0:T(256)} %param.27) | copy-start | bytes 3076
  69.6 36.2 %copy-start.7 = (f32[256]{0:T(256)S(1)}, f32[256]{0:T(256)}, u32[]{:S(2)}) copy-start(f32[256]{0:T(256)} %param.23) | copy-start | bytes 3076
  77.8 15.9 %all-to-all-start.2 = ((bf16[8,96,128]{2,1,0:T(8,128)(2,1)}), bf16[8,96,128]{2,1,0:T(8,128)(2,1)S(1)}, u32[]{:S(2)}, u32[]{:S(2)}) async-start(bf16[8,96,128]{2,1,0:T(8,128)(2,1)} %get-tuple-element.30), calls=%async_computation.2 | async-start | bytes 393216 | tf_op jit(solution)/shard_map/all_to_all | solution.py:428
  83.3 1.1 copy-start
  84.4 1.0 copy-start.1
  85.3 1.0 copy-start.2
  86.3 1.0 copy-start.3
  87.2 0.9 copy-start.4
  88.2 0.8 copy-start.5
  95.1 24.0 %all-to-all-start.3 = ((bf16[16,80,128]{2,1,0:T(8,128)(2,1)}), bf16[16,80,128]{2,1,0:T(8,128)(2,1)S(1)}, u32[]{:S(2)}, u32[]{:S(2)}) async-start(bf16[16,80,128]{2,1,0:T(8,128)(2,1)} %merge.1), calls=%async_computation.3 | async-start | bytes 655360 | tf_op jit(solution)/shard_map/all_to_all | solution.py:447
Sparse Core Ops, SparseCore 0:
  9.4 50.2 all-gather.5
  61.9 47.7 all-gather.7

commit v5 on v4

--- a/solution.py
+++ b/solution.py
@@ -8,6 +8,8 @@
 
 KD = 128
 BLOCK = 64
+TILE = 256
+SMALL = pltpu.CompilerParams(vmem_limit_bytes=24 * 1024 * 1024)
 EPS = 1e-06
 Z, Y, X, C = "sp_0", "sp_1", "fs", "tp"
 F32, BF16 = jnp.float32, jnp.bfloat16
@@ -113,94 +115,88 @@
 
 
 def states_kernel(
-    x_ref, w_ref, w2_ref, ld_ref, gap_ref,
+    x_hbm, w_ref, w2_ref, ld_ref, gap_ref,
     a_ref, v_ref, c_ref, gated_ref, send_ref, before_ref, offset_ref,
-    chunk_s, chunk_t, edge,
-):
-    step = pl.program_id(0)
-    rows = x_ref.shape[0]
-    acc = jnp.zeros((rows, 224), F32)
-    acc_g = jnp.zeros((rows, 64), F32)
-    for k in range(8):
-        xk = x_ref[:, 256 * k : 256 * (k + 1)]
-        acc += dot(xk, w_ref[k], NT)
-        acc_g += dot(xk, w2_ref[k], NT)
-    pre_v = acc[:, :128].astype(BF16)
-    pre_a = jnp.concatenate([acc[:, 128:], jnp.zeros((rows, 32), F32)], axis=1).astype(BF16)
-    a_ref[...] = pre_a
-    v_ref[...] = pre_v
-    glu = acc_g.astype(BF16).astype(F32)
-    gated = glu[:, 0:32] * sigmoid(glu[:, 32:64])
-    gated_ref[...] = gated.astype(BF16)
-
-    @pl.when(step == 0)
-    def _():
-        edge[...] = jnp.concatenate([gated[:16], gated[:16], gated[:16], gated[:16]], axis=1)
-
-    @pl.when(step == pl.num_programs(0) - 1)
-    def _():
-        last = gated[rows - 16 :]
-        last = jnp.concatenate([last, last, last, last], axis=1)
-        edge[...] = jnp.where(lanes(16) < 32, edge[...], last)
-
+    x_ref, sems, chunk_s, chunk_t,
+):
+    rows = TILE
+    n = x_ref.shape[0] // 64
+    copies = []
+    for t in range(x_ref.shape[0] // rows):
+        at = pl.ds(rows * t, rows)
+        copies.append(pltpu.make_async_copy(x_hbm.at[at], x_ref.at[at], sems.at[t]))
+        copies[-1].start()
     lower, upper = triangles()
     lower_f, upper_f = lower.astype(F32), upper.astype(F32)
     lower_b, upper_b = lower_f.astype(BF16), upper_f.astype(BF16)
     lane = lanes(128)
     lane1 = lanes(1)
-    for b in range(rows // 128):
-        a = pre_a[128 * b : 128 * (b + 1)].astype(F32)
-        v = pre_v[128 * b : 128 * (b + 1)]
-        k = gate_keys(a, gap_ref[...])
-        g = jnp.log1p(-k)
-        ld = ld_ref[b]
-        cum_f = split_dot(lower_b, g) + jnp.sum(lower_f * ld[0:1], axis=1, keepdims=True)
-        cum_b = split_dot(upper_b, g) + jnp.sum(upper_f * ld[1:2], axis=1, keepdims=True)
-        cum = jnp.where(lane < 32, cum_f, cum_b)
-        c_ref[128 * b : 128 * (b + 1), :] = cum
-        for h in range(2):
-            part = slice(64 * h, 64 * (h + 1))
-            cc = cum[part]
-            tot = jnp.where(lane1 < 32, cc[63:64], cc[0:1])
-            kd = (k[part] * jnp.exp(tot - cc)).astype(BF16)
-            st = dot(v[part], kd, TN)
-            packed = st[:64] + pltpu.roll(st[64:], 64, 1)
-            tot8 = jnp.broadcast_to(tot, (8, 128))
-            tot8 = jnp.where(lanes(8) < 64, tot8, pltpu.roll(tot8, 64, 1))
-            idx = step * (rows // 64) + 2 * b + h
-            chunk_s[idx] = packed
-            chunk_t[idx] = tot8
-
-    @pl.when(step == pl.num_programs(0) - 1)
-    def _():
-        n = chunk_s.shape[0]
-        fwd = (lanes(64) % 64) < 32
-        fwd8 = (lanes(8) % 64) < 32
-        s = jnp.zeros((64, 128), F32)
-        off = jnp.zeros((8, 128), F32)
-        befores, offs = [None] * n, [None] * n
-        for i in range(n):
-            j = n - 1 - i
-            befores[i], offs[i] = s, off
-            tt = jnp.where(fwd8, chunk_t[i], chunk_t[j])
-            sc = jnp.where(fwd, chunk_s[i], chunk_s[j])
-            s = s * jnp.exp(tt)[0:1] + sc
-            off = off + tt
-        for i in range(n):
-            j = n - 1 - i
-            before_ref[i] = jnp.where(fwd, befores[i], befores[j]).astype(BF16)
-            offset_ref[i] = jnp.where(fwd8, offs[i], offs[j])
-        dec = jnp.exp(off)[0:1]
-        hi = dec.astype(BF16)
-        lo = (dec - hi.astype(F32)).astype(BF16)
-        row = lax.broadcasted_iota(jnp.int32, (16, 128), 0)
-        tail = jnp.where(row == 0, hi.astype(F32), jnp.where(row == 1, lo.astype(F32), 0.0))
-        s = s.astype(BF16)
-        tail = tail.astype(BF16)
-        for i in range(8):
-            send_ref[i, :64, :] = s
-            send_ref[i, 64:80, :] = tail
-            send_ref[i, 80:96, :] = edge[...].astype(BF16)
+    for t, copy in enumerate(copies):
+        copy.wait()
+        start = rows * t
+        acc = jnp.zeros((rows, 224), F32)
+        acc_g = jnp.zeros((rows, 64), F32)
+        for k in range(8):
+            xk = x_ref[start : start + rows, 256 * k : 256 * (k + 1)]
+            acc += dot(xk, w_ref[k], NT)
+            acc_g += dot(xk, w2_ref[k], NT)
+        pre_v = acc[:, :128].astype(BF16)
+        pre_a = jnp.concatenate([acc[:, 128:], jnp.zeros((rows, 32), F32)], axis=1).astype(BF16)
+        a_ref[start : start + rows, :] = pre_a
+        v_ref[start : start + rows, :] = pre_v
+        glu = acc_g.astype(BF16).astype(F32)
+        gated_ref[start : start + rows, :] = (glu[:, 0:32] * sigmoid(glu[:, 32:64])).astype(BF16)
+        for b in range(rows // 128):
+            a = pre_a[128 * b : 128 * (b + 1)].astype(F32)
+            v = pre_v[128 * b : 128 * (b + 1)]
+            k = gate_keys(a, gap_ref[...])
+            g = jnp.log1p(-k)
+            ld = ld_ref[t * (rows // 128) + b]
+            cum_f = split_dot(lower_b, g) + jnp.sum(lower_f * ld[0:1], axis=1, keepdims=True)
+            cum_b = split_dot(upper_b, g) + jnp.sum(upper_f * ld[1:2], axis=1, keepdims=True)
+            cum = jnp.where(lane < 32, cum_f, cum_b)
+            c_ref[start + 128 * b : start + 128 * (b + 1), :] = cum
+            for h in range(2):
+                part = slice(64 * h, 64 * (h + 1))
+                cc = cum[part]
+                tot = jnp.where(lane1 < 32, cc[63:64], cc[0:1])
+                kd = (k[part] * jnp.exp(tot - cc)).astype(BF16)
+                st = dot(v[part], kd, TN)
+                tot8 = jnp.broadcast_to(tot, (8, 128))
+                tot8 = jnp.where(lanes(8) < 64, tot8, pltpu.roll(tot8, 64, 1))
+                idx = t * (rows // 64) + 2 * b + h
+                chunk_s[idx] = st[:64] + pltpu.roll(st[64:], 64, 1)
+                chunk_t[idx] = tot8
+
+    fwd = (lanes(64) % 64) < 32
+    fwd8 = (lanes(8) % 64) < 32
+    s = jnp.zeros((64, 128), F32)
+    off = jnp.zeros((8, 128), F32)
+    befores, offs = [None] * n, [None] * n
+    for i in range(n):
+        j = n - 1 - i
+        befores[i], offs[i] = s, off
+        tt = jnp.where(fwd8, chunk_t[i], chunk_t[j])
+        sc = jnp.where(fwd, chunk_s[i], chunk_s[j])
+        s = s * jnp.exp(tt)[0:1] + sc
+        off = off + tt
+        if i >= n // 2:
+            for p, q in ((i, j), (j, i)):
+                before_ref[p] = jnp.where(fwd, befores[p], befores[q]).astype(BF16)
+                offset_ref[p] = jnp.where(fwd8, offs[p], offs[q])
+    dec = jnp.exp(off)[0:1]
+    hi = dec.astype(BF16)
+    lo = (dec - hi.astype(F32)).astype(BF16)
+    row = lax.broadcasted_iota(jnp.int32, (16, 128), 0)
+    tail = jnp.where(row == 0, hi.astype(F32), jnp.where(row == 1, lo.astype(F32), 0.0)).astype(BF16)
+    s = s.astype(BF16)
+    head = gated_ref[0:16, :].astype(F32)
+    last = gated_ref[gated_ref.shape[0] - 16 :, :].astype(F32)
+    edge = jnp.concatenate([head, last, last, last], axis=1).astype(BF16)
+    for i in range(8):
+        send_ref[i, :64, :] = s
+        send_ref[i, 64:80, :] = tail
+        send_ref[i, 80:96, :] = edge
 
 
 def local_kernel(
@@ -294,44 +290,51 @@
         send_ref[blk, 64:, :] = packed
 
 
-def output_kernel(recv_ref, rec_gain_ref, conv_gain_ref, w_ref, out_ref, act):
-    @pl.when(pl.program_id(0) == 0)
-    def _():
-        for c in range(2):
-            for h in range(2):
-                rec = sum(recv_ref[(4 * h + q) * 2 + c, :64, :].astype(F32) for q in range(4))
-                rec = rec * lax.rsqrt(jnp.mean(rec * rec, axis=1, keepdims=True) + EPS)
-                rec = rec * rec_gain_ref[2 * c + h : 2 * c + h + 1, :]
-                at = 128 * (4 * c + h)
-                act[:, at : at + 128] = rec.astype(BF16)
-        lane = lanes(16) // 32
-        blocks = []
-        for c in range(2):
-            for m in range(2):
-                parts = [recv_ref[(4 * m + q) * 2 + c, 64:80, :].astype(F32) for q in range(4)]
-                groups = []
-                for g in range(4):
-                    value = jnp.zeros((16, 128), F32)
-                    for q in range(4):
-                        moved = parts[q] if q == g else pltpu.roll(parts[q], (32 * (q - g)) % 128, 1)
-                        value = jnp.where(lane == q, moved, value)
-                    groups.append(value)
-                blocks.append(jnp.concatenate(groups, axis=0))
-        total = sum(jnp.sum(b, axis=1, keepdims=True) for b in blocks)
-        square = sum(jnp.sum(b * b, axis=1, keepdims=True) for b in blocks)
-        mean = total / 512.0
-        scale = lax.rsqrt(square / 512.0 - mean * mean + EPS)
-        for c in range(2):
-            for m in range(2):
-                n = 2 * c + m
-                y = (blocks[n] - mean) * scale * conv_gain_ref[n : n + 1, :]
-                at = 128 * (4 * c + 2 + m)
-                act[:, at : at + 128] = (y * sigmoid(y)).astype(BF16)
-
-    acc = jnp.zeros(out_ref.shape, F32)
+def output_kernel(
+    recv_ref, rec_gain_ref, conv_gain_ref, w0_ref, w_hbm, out_ref, act, w1_ref, sem
+):
+    copy = pltpu.make_async_copy(w_hbm.at[1], w1_ref, sem)
+    copy.start()
     for c in range(2):
-        acc += dot(act[:, 512 * c : 512 * (c + 1)], w_ref[c], NT)
-    out_ref[...] = acc.astype(BF16)
+        for h in range(2):
+            rec = sum(recv_ref[(4 * h + q) * 2 + c, :64, :].astype(F32) for q in range(4))
+            rec = rec * lax.rsqrt(jnp.mean(rec * rec, axis=1, keepdims=True) + EPS)
+            rec = rec * rec_gain_ref[2 * c + h : 2 * c + h + 1, :]
+            at = 128 * (4 * c + h)
+            act[:, at : at + 128] = rec.astype(BF16)
+    lane = lanes(16) // 32
+    blocks = []
+    for c in range(2):
+        for m in range(2):
+            parts = [recv_ref[(4 * m + q) * 2 + c, 64:80, :].astype(F32) for q in range(4)]
+            groups = []
+            for g in range(4):
+                value = jnp.zeros((16, 128), F32)
+                for q in range(4):
+                    moved = parts[q] if q == g else pltpu.roll(parts[q], (32 * (q - g)) % 128, 1)
+                    value = jnp.where(lane == q, moved, value)
+                groups.append(value)
+            blocks.append(jnp.concatenate(groups, axis=0))
+    total = sum(jnp.sum(b, axis=1, keepdims=True) for b in blocks)
+    square = sum(jnp.sum(b * b, axis=1, keepdims=True) for b in blocks)
+    mean = total / 512.0
+    scale = lax.rsqrt(square / 512.0 - mean * mean + EPS)
+    for c in range(2):
+        for m in range(2):
+            n = 2 * c + m
+            y = (blocks[n] - mean) * scale * conv_gain_ref[n : n + 1, :]
+            at = 128 * (4 * c + 2 + m)
+            act[:, at : at + 128] = (y * sigmoid(y)).astype(BF16)
+
+    half = dot(act[:, 0:512], w0_ref[...], NT)
+    copy.wait()
+    out_ref[...] = (half + dot(act[:, 512:1024], w1_ref[...], NT)).astype(BF16)
+
+
+def load_kernel(w_hbm, w_ref, sem):
+    copy = pltpu.make_async_copy(w_hbm.at[0], w_ref, sem)
+    copy.start()
+    copy.wait()
 
 
 def near(x):
@@ -340,14 +343,6 @@
 
 def kept(shape, dtype):
     return pltpu.VMEM(shape, dtype)
-
-
-def full(shape):
-    return pl.BlockSpec(shape, lambda *_: (0,) * len(shape))
-
-
-def spec(shape, at):
-    return pl.BlockSpec(shape, at)
 
 
 def body(
@@ -390,40 +385,25 @@
     rec_gains = gains[:, 0].reshape(4, 128)
     conv_gains = gains[:, 1].reshape(4, 128)
     n = seq.shape[0]
-    tile = 256
     pre_a, pre_v, cum, gated, sent, before, offset = pl.pallas_call(
         states_kernel,
-        grid=(n // tile,),
-        in_specs=[
-            spec((tile, 2048), lambda i: (i, 0)),
-            full((8, 224, 256)),
-            full((8, 64, 256)),
-            spec((tile // 128, 2, 128), lambda i: (i, 0, 0)),
-            full((1, 128)),
-        ],
-        out_specs=[
-            spec((tile, 128), lambda i: (i, 0)),
-            spec((tile, 128), lambda i: (i, 0)),
-            spec((tile, 128), lambda i: (i, 0)),
-            spec((tile, 32), lambda i: (i, 0)),
-            full((8, 96, 128)),
-            full((16, 64, 128)),
-            full((16, 8, 128)),
-        ],
+        in_specs=[pl.BlockSpec(memory_space=pltpu.HBM)]
+        + [pl.BlockSpec(memory_space=pltpu.VMEM)] * 4,
         out_shape=[
-            jax.ShapeDtypeStruct((n, 128), BF16),
-            jax.ShapeDtypeStruct((n, 128), BF16),
-            jax.ShapeDtypeStruct((n, 128), F32),
-            jax.ShapeDtypeStruct((n, 32), BF16),
-            jax.ShapeDtypeStruct((8, 96, 128), BF16),
-            jax.ShapeDtypeStruct((16, 64, 128), BF16),
-            jax.ShapeDtypeStruct((16, 8, 128), F32),
+            kept((n, 128), BF16),
+            kept((n, 128), BF16),
+            kept((n, 128), F32),
+            kept((n, 32), BF16),
+            kept((8, 96, 128), BF16),
+            kept((16, 64, 128), BF16),
+            kept((16, 8, 128), F32),
         ],
         scratch_shapes=[
-            pltpu.VMEM((16, 64, 128), F32), pltpu.VMEM((16, 8, 128), F32), pltpu.VMEM((16, 128), F32)
+            pltpu.VMEM((n, 2048), BF16), pltpu.SemaphoreType.DMA((n // TILE,)),
+            pltpu.VMEM((16, 64, 128), F32), pltpu.VMEM((16, 8, 128), F32),
         ],
-        name="states",
-    )(seq, near(weights), near(weights2), near(decays), near(gap))
+        compiler_params=SMALL, name="states",
+    )(pltpu.with_memory_space_constraint(seq, pltpu.HBM), near(weights), near(weights2), near(decays), near(gap))
 
     arrived = lax.all_to_all(sent, Z, split_axis=0, concat_axis=0, tiled=True)
     local, decayed, convolved, edges = pl.pallas_call(
@@ -435,28 +415,35 @@
             kept((2, 16, 32), F32),
         ],
         scratch_shapes=[pltpu.VMEM((n + 32, 32), F32)],
-        name="local",
+        compiler_params=SMALL, name="local",
     )(near(pre_a), near(pre_v), near(cum), near(gap), near(before), near(offset), near(gated), near(taps))
     merged = pl.pallas_call(
         merge_kernel,
         in_specs=[pl.BlockSpec(memory_space=pltpu.SMEM)]
         + [pl.BlockSpec(memory_space=pltpu.VMEM)] * 6,
         out_shape=kept((16, 80, 128), BF16),
-        name="merge",
+        compiler_params=SMALL, name="merge",
     )(z.reshape(1).astype(jnp.int32), near(arrived), near(local), near(decayed), near(convolved), near(edges), near(taps))
     mine = lax.all_to_all(merged, (Y, C), split_axis=0, concat_axis=0, tiled=True)
+    out_w = pltpu.with_memory_space_constraint(out_w, pltpu.HBM)
+    out_w0 = pl.pallas_call(
+        load_kernel,
+        in_specs=[pl.BlockSpec(memory_space=pltpu.HBM)],
+        out_shape=kept((2048, 512), BF16),
+        scratch_shapes=[pltpu.SemaphoreType.DMA],
+        compiler_params=SMALL,
+        name="load",
+    )(out_w)
     mixed = pl.pallas_call(
         output_kernel,
-        grid=(4,),
-        in_specs=[
-            full((16, 80, 128)), full((4, 128)), full((4, 128)),
-            spec((2, 512, 512), lambda i: (0, i, 0)),
+        in_specs=[pl.BlockSpec(memory_space=pltpu.VMEM)] * 4
+        + [pl.BlockSpec(memory_space=pltpu.HBM)],
+        out_shape=jax.ShapeDtypeStruct((64, 2048), BF16),
+        scratch_shapes=[
+            pltpu.VMEM((64, 1024), BF16), pltpu.VMEM((2048, 512), BF16), pltpu.SemaphoreType.DMA
         ],
-        out_specs=spec((64, 512), lambda i: (0, i)),
-        out_shape=jax.ShapeDtypeStruct((64, 2048), BF16),
-        scratch_shapes=[pltpu.VMEM((64, 1024), BF16)],
-        name="output",
-    )(near(mine), rec_gains, conv_gains, out_w)
+        compiler_params=SMALL, name="output",
+    )(near(mine), rec_gains, conv_gains, near(out_w0), out_w)
     return mixed[None]
 
 

time: 132 us -> 129 us (0.977)
  local copies, waits for them, and re-layouts: 8.04 us -> 1.72 us
  waiting for transfers between devices: 24.5 us -> 28.7 us
    unnamed x17 -> x5, local copies, waits for them, and re-layouts: 5.75 us -> 0.01 us
    all_to_all x1, waiting for transfers between devices: 2.36 us -> 7.55 us  [body(): arrived = lax.all_to_all(sent, Z, split_axis=0, concat_axis=0, tiled=True)]
    all_to_all x1, waiting for transfers between devices: 9.38 us -> 6.24 us  [body(): lax.all_to_all(merged, (Y, C), split_axis=0, concat_axis=0, tiled=True)]
    all_gather x1, waiting for transfers between devices: 1.43 us -> 3.54 us  [body(): lax.all_gather(out_cols, (C, Z), axis=0, tiled=True).reshape(2, 2048, 512)]
    pallas_call x2 -> x3, Pallas kernels: 13.2 us -> 12.7 us  [the longest x1 7.45 us: body(): pl.pallas_call(states_kernel, in_specs=[pl.BlockSpec(memory_space=pltpu.H...]
  transfers between devices with their start and end apart: 6 -> 6, of which waited for: 4 -> 4; matrix products, arithmetic and copies ran while one was open for 2% -> 1% of each run, Pallas kernels for 10% -> 11%
where the time goes in v5:
time: 129 us
  starting transfers between devices  38.5 us (30%)
  waiting for transfers between devices  28.7 us (22%)
  blocking collectives  26.9 us (21%)
  Pallas kernels  19.4 us (15%)
  between operations  13.5 us (10%)
  local copies, waits for them, and re-layouts  1.72 us (1%)
    all_gather x1, blocking collectives, body(): weights = lax.all_gather(second, Z, axis=0)  25 us
    all_to_all x1, starting transfers between devices, body(): lax.all_to_all(second2, Z, split_axis=0, concat_axis=0, tiled=True)  14.1 us
    all_to_all x1, waiting for transfers between devices, body(): first = lax.all_to_all(first, Y, split_axis=0, concat_axis=0, tiled=True)  11.3 us
    all_to_all x1, starting transfers between devices, body(): lax.all_to_all(merged, (Y, C), split_axis=0, concat_axis=0, tiled=True)  11.1 us
    all_to_all x1, starting transfers between devices, body(): first = lax.all_to_all(first, Y, split_axis=0, concat_axis=0, tiled=True)  7.65 us
    all_to_all x1, waiting for transfers between devices, body(): arrived = lax.all_to_all(sent, Z, split_axis=0, concat_axis=0, tiled=True)  7.55 us
    pallas_call x1, Pallas kernels, body(): pl.pallas_call(states_kernel, in_specs=[pl.BlockSpec(memory_space=pltpu.H...  7.45 us
    all_to_all x1, waiting for transfers between devices, body(): lax.all_to_all(merged, (Y, C), split_axis=0, concat_axis=0, tiled=True)  6.24 us
  transfers between devices with their start and end apart: 6, of which 4 were waited for; matrix products, arithmetic and copies ran while one was open for 1% of the time, Pallas kernels for 11%

profile of v5, /device:TPU:1, one launch (start us, length us, event | category | flops | bytes accessed | tf_op | source)
XLA Modules:
  0.0 128.7 jit_solution(693526218836366594)
XLA Ops:
  6.5 0.0 all-gather.6.cloned.1.call-start
  6.5 2.1 %start.1 = (bf16[64,2048]{1,0:T(8,128)(2,1)}, bf16[8,32,896]{2,1,0:T(8,128)(2,1)}) custom-call(bf16[64,2048]{1,0:T(8,128)(2,1)} %bitcast.26, f32[1,2048]{1,0:T(1,128)} %bitcast.30, bf16[32,256]{1,0:T(8,128)(2,1)} %rf_ref.1, bf16[32,256]{1,0:T(8,128)(2,1)} %rb_ref.1, bf16[32,256]{1,0:T(8,128)(2,1)} %rq_ref.1, bf16[32,256]{1,0:T(8,128)(2,1)} %cv_ref.1, ...), custom_call_target="tpu_custom_call" | custom-call | tf_op jit(solution)/shard_map/start/pallas_call | solution.py:358
  8.6 0.0 all-gather.6.cloned.1.call-update
  8.7 7.7 %all-to-all-start = ((bf16[8,32,896]{2,1,0:T(8,128)(2,1)}), bf16[8,32,896]{2,1,0:T(8,128)(2,1)S(1)}, u32[]{:S(2)}, u32[]{:S(2)}) async-start(bf16[8,32,896]{2,1,0:T(8,128)(2,1)} %get-tuple-element.25), calls=%async_computation | async-start | bytes 917504 | tf_op jit(solution)/shard_map/all_to_all | solution.py:367
  16.3 0.0 all-gather.8.cloned.1.call-start
  16.4 0.8 reshape.25
  17.2 0.8 reshape.23
  18.0 0.1 reshape.24
  18.1 11.3 %all-to-all-done.first_ref = bf16[8,32,896]{2,1,0:T(8,128)(2,1)S(1)} async-done(((bf16[8,32,896]{2,1,0:T(8,128)(2,1)}), bf16[8,32,896]{2,1,0:T(8,128)(2,1)S(1)}, u32[]{:S(2)}, u32[]{:S(2)}) %all-to-all-start) | async-done | bytes 458784 | tf_op jit(solution)/shard_map/all_to_all | solution.py:367
  29.4 1.0 second.1
  30.4 0.0 all-gather.8.cloned.1.call-update
  30.4 14.1 %all-to-all-start.1 = ((bf16[8,64,256]{2,1,0:T(8,128)(2,1)}), bf16[8,64,256]{2,1,0:T(8,128)(2,1)S(1)}, u32[]{:S(2)}, u32[]{:S(2)}) async-start(bf16[8,64,256]{2,1,0:T(8,128)(2,1)} %get-tuple-element.27), calls=%async_computation.1 | async-start | bytes 524288 | tf_op jit(solution)/shard_map/all_to_all | solution.py:380
  44.5 25.0 %all-gather = bf16[1792,256]{1,0:T(8,128)(2,1)S(1)} all-gather(bf16[224,256]{1,0:T(8,128)(2,1)S(1)} %get-tuple-element.26), channel_id=2, replica_groups=mesh['sp_0'=8,'sp_1'=8,'fs'=4,'tp'=2] {'sp_0'}, dimensions={0}, use_global_device_ids=true | all-gather | bytes 1032192 | tf_op jit(solution)/shard_map/all_gather | solution.py:381
  69.6 0.0 all-to-all-done.1.w2_ref
  69.6 0.0 all-gather.6.cloned.1.call-done.x_hbm
  69.6 0.0 copy-start
  69.6 0.0 copy-start.1
  69.6 7.5 %states.1 = (bf16[1024,128]{1,0:T(8,128)(2,1)S(1)}, bf16[1024,128]{1,0:T(8,128)(2,1)S(1)}, f32[1024,128]{1,0:T(8,128)S(1)}, bf16[1024,32]{1,0:T(8,128)(2,1)S(1)}...) custom-call(bf16[1024,2048]{1,0:T(8,128)(2,1)} %all-gather.6.cloned.1.call-done.x_hbm, ...), custom_call_target="tpu_custom_call" | custom-call | tf_op jit(solution)/shard_map/states/pallas_call | solution.py:388
  77.0 5.5 %all-to-all-start.2 = ((bf16[8,96,128]{2,1,0:T(8,128)(2,1)}), bf16[8,96,128]{2,1,0:T(8,128)(2,1)S(1)}, u32[]{:S(2)}, u32[]{:S(2)}) async-start(bf16[8,96,128]{2,1,0:T(8,128)(2,1)} %get-tuple-element.30), calls=%async_computation.2 | async-start | bytes 393216 | tf_op jit(solution)/shard_map/all_to_all | solution.py:408
  82.5 2.3 %local.1 = (f32[1024,128]{1,0:T(8,128)S(1)}, bf16[1024,128]{1,0:T(8,128)(2,1)S(1)}, bf16[16,16,128]{2,1,0:T(8,128)(2,1)S(1)}, f32[2,16,32]{2,1,0:T(8,128)S(1)}) custom-call(bf16[1024,128]{1,0:T(8,128)(2,1)S(1)} %get-tuple-element.31.a_ref, bf16[1024,128]{1,0:T(8,128)(2,1)S(1)} %get-tuple-element.32.v_ref, f32[1024,128]{1,0:T(8,128)S(1)} %get-tuple-element.33.c_ref, ...), custom_call_target="tpu_custom_call" | custom-call | tf_op jit(solution)/shard_map/local/pallas_call | solution.py:409
  84.9 7.5 %all-to-all-done.2.recv_ref = bf16[8,96,128]{2,1,0:T(8,128)(2,1)S(1)} async-done(((bf16[8,96,128]{2,1,0:T(8,128)(2,1)}), bf16[8,96,128]{2,1,0:T(8,128)(2,1)S(1)}, u32[]{:S(2)}, u32[]{:S(2)}) %all-to-all-start.2) | async-done | bytes 196640 | tf_op jit(solution)/shard_map/all_to_all | solution.py:408
  92.4 1.3 %merge.1 = bf16[16,80,128]{2,1,0:T(8,128)(2,1)} custom-call(s32[1]{0:T(128)} %bitcast.z_ref, bf16[8,96,128]{2,1,0:T(8,128)(2,1)S(1)} %all-to-all-done.2.recv_ref, f32[1024,128]{1,0:T(8,128)S(1)} %get-tuple-element.38.local_ref, bf16[1024,128]{1,0:T(8,128)(2,1)S(1)} %get-tuple-element.39.qd_ref, bf16[16,16,128]{2,1,0:T(8,128)(2,1)S(1)} %get-tuple-element.40.conv_ref, ...), custom_call_target="tpu_custom_call" | custom-call | tf_op jit(solution)/shard_map/merge/pallas_call | solution.py:420
  93.7 11.1 %all-to-all-start.3 = ((bf16[16,80,128]{2,1,0:T(8,128)(2,1)}), bf16[16,80,128]{2,1,0:T(8,128)(2,1)S(1)}, u32[]{:S(2)}, u32[]{:S(2)}) async-start(bf16[16,80,128]{2,1,0:T(8,128)(2,1)} %merge.1), calls=%async_computation.3 | async-start | bytes 655360 | tf_op jit(solution)/shard_map/all_to_all | solution.py:427
  104.9 0.0 copy-done
  104.9 0.0 copy-done.1
  104.9 1.8 %all-gather.2 = f32[2,2,256]{2,1,0:T(2,128)S(1)} all-gather(f32[1,2,256]{2,1,0:T(2,128)S(1)} %maximum_bitcast_fusion), channel_id=3, replica_groups=mesh['sp_0'=8,'sp_1'=8,'fs'=4,'tp'=2] {'tp'}, dimensions={0}, use_global_device_ids=true | all-gather | bytes 6144 | tf_op jit(solution)/shard_map/all_gather | solution.py:384
  106.7 3.5 %all-gather.8.cloned.1.call-done = bf16[4096,512]{1,0:T(8,128)(2,1)} async-done(((bf16[256,512]{1,0:T(8,128)(2,1)}), bf16[4096,512]{1,0:T(8,128)(2,1)}) %all-gather.8.cloned.1.call-update) | async-done | bytes 4194320 | tf_op jit(solution)/shard_map/all_gather | solution.py:382
  110.3 1.6 %load.1.w0_ref = bf16[2048,512]{1,0:T(8,128)(2,1)S(1)} custom-call(bf16[2,2048,512]{2,1,0:T(8,128)(2,1)} %bitcast.24), custom_call_target="tpu_custom_call" | custom-call | tf_op jit(solution)/shard_map/load/pallas_call | solution.py:429
  111.9 6.2 %all-to-all-done.3.recv_ref = bf16[16,80,128]{2,1,0:T(8,128)(2,1)S(1)} async-done(((bf16[16,80,128]{2,1,0:T(8,128)(2,1)}), bf16[16,80,128]{2,1,0:T(8,128)(2,1)S(1)}, u32[]{:S(2)}, u32[]{:S(2)}) %all-to-all-start.3) | async-done | bytes 327712 | tf_op jit(solution)/shard_map/all_to_all | solution.py:427
  118.1 3.7 %output.1 = bf16[64,2048]{1,0:T(8,128)(2,1)} custom-call(bf16[16,80,128]{2,1,0:T(8,128)(2,1)S(1)} %all-to-all-done.3.recv_ref, f32[4,128]{1,0:T(4,128)S(1)} %bitcast.23, f32[4,128]{1,0:T(4,128)S(1)} %bitcast.22, bf16[2048,512]{1,0:T(8,128)(2,1)S(1)} %load.1.w0_ref, bf16[2,2048,512]{2,1,0:T(8,128)(2,1)} %bitcast.25), custom_call_target="tpu_custom_call" | custom-call | tf_op jit(solution)/shard_map/output/pallas_call | solution.py:437
  (7 shorter events, 0.1 us)
Async XLA Ops:
  6.5 63.0 %all-gather.6.cloned.1.call-start = ((), (), s32[]{:S(2)}) async-start(), calls=%async_computation.4 | async-start | bytes 4456448 | tf_op jit(solution)/shard_map/all_gather | solution.py:366
  8.7 20.8 %all-to-all-start = ((bf16[8,32,896]{2,1,0:T(8,128)(2,1)}), bf16[8,32,896]{2,1,0:T(8,128)(2,1)S(1)}, u32[]{:S(2)}, u32[]{:S(2)}) async-start(bf16[8,32,896]{2,1,0:T(8,128)(2,1)} %get-tuple-element.25), calls=%async_computation | async-start | bytes 917504 | tf_op jit(solution)/shard_map/all_to_all | solution.py:367
  16.3 94.0 %all-gather.8.cloned.1.call-start = ((), (), s32[]{:S(2)}) async-start(), calls=%async_computation.5 | async-start | bytes 4456448 | tf_op jit(solution)/shard_map/all_gather | solution.py:382
  30.4 39.2 %all-to-all-start.1 = ((bf16[8,64,256]{2,1,0:T(8,128)(2,1)}), bf16[8,64,256]{2,1,0:T(8,128)(2,1)S(1)}, u32[]{:S(2)}, u32[]{:S(2)}) async-start(bf16[8,64,256]{2,1,0:T(8,128)(2,1)} %get-tuple-element.27), calls=%async_computation.1 | async-start | bytes 524288 | tf_op jit(solution)/shard_map/all_to_all | solution.py:380
  69.6 35.3 %copy-start = (f32[256]{0:T(256)S(1)}, f32[256]{0:T(256)}, u32[]{:S(2)}) copy-start(f32[256]{0:T(256)} %param.27) | copy-start | bytes 3076
  69.6 35.3 %copy-start.1 = (f32[256]{0:T(256)S(1)}, f32[256]{0:T(256)}, u32[]{:S(2)}) copy-start(f32[256]{0:T(256)} %param.23) | copy-start | bytes 3076
  77.0 15.4 %all-to-all-start.2 = ((bf16[8,96,128]{2,1,0:T(8,128)(2,1)}), bf16[8,96,128]{2,1,0:T(8,128)(2,1)S(1)}, u32[]{:S(2)}, u32[]{:S(2)}) async-start(bf16[8,96,128]{2,1,0:T(8,128)(2,1)} %get-tuple-element.30), calls=%async_computation.2 | async-start | bytes 393216 | tf_op jit(solution)/shard_map/all_to_all | solution.py:408
  93.7 24.4 %all-to-all-start.3 = ((bf16[16,80,128]{2,1,0:T(8,128)(2,1)}), bf16[16,80,128]{2,1,0:T(8,128)(2,1)S(1)}, u32[]{:S(2)}, u32[]{:S(2)}) async-start(bf16[16,80,128]{2,1,0:T(8,128)(2,1)} %merge.1), calls=%async_computation.3 | async-start | bytes 655360 | tf_op jit(solution)/shard_map/all_to_all | solution.py:427
Sparse Core Ops, SparseCore 0:
  9.4 50.2 all-gather.5
  61.8 48.4 all-gather.7

commit v6 on v5

--- a/solution.py
+++ b/solution.py
@@ -40,7 +40,19 @@
 def split_dot(mask, x):
     hi = x.astype(BF16)
     lo = (x - hi.astype(F32)).astype(BF16)
-    return dot(mask, hi, NN) + dot(mask, lo, NN)
+    return dot(mask, jnp.concatenate([hi, lo], axis=0), NN)
+
+
+def project(x_ref, w_ref, rows, width):
+    acc = jnp.zeros((rows.stop - rows.start, width), F32)
+    for k in range(8):
+        acc += dot(x_ref[rows, 256 * k : 256 * (k + 1)], w_ref[k], NT)
+    return acc
+
+
+def gate_product(acc):
+    glu = acc.astype(BF16).astype(F32)
+    return glu[:, 0:32] * sigmoid(glu[:, 32:64])
 
 
 def gate_keys(a, gap):
@@ -115,58 +127,66 @@
 
 
 def states_kernel(
-    x_hbm, w_ref, w2_ref, ld_ref, gap_ref,
-    a_ref, v_ref, c_ref, gated_ref, send_ref, before_ref, offset_ref,
+    z_ref, x_hbm, w_ref, w2_ref, ld_ref, gap_ref,
+    a_ref, v_ref, c_ref, send_ref, before_ref, offset_ref,
     x_ref, sems, chunk_s, chunk_t,
 ):
+    z = z_ref[0]
     rows = TILE
-    n = x_ref.shape[0] // 64
+    total = x_ref.shape[0]
+    n = total // 64
     copies = []
-    for t in range(x_ref.shape[0] // rows):
+    for t in range(total // rows):
         at = pl.ds(rows * t, rows)
         copies.append(pltpu.make_async_copy(x_hbm.at[at], x_ref.at[at], sems.at[t]))
         copies[-1].start()
     lower, upper = triangles()
     lower_f, upper_f = lower.astype(F32), upper.astype(F32)
-    lower_b, upper_b = lower_f.astype(BF16), upper_f.astype(BF16)
+    lower_b = lower_f.astype(BF16)
+    lower_b = jnp.concatenate([lower_b, lower_b], axis=1)
     lane = lanes(128)
     lane1 = lanes(1)
+
+    def gates(b):
+        at = slice(128 * b, 128 * (b + 1))
+        a = a_ref[at, :].astype(F32)
+        v = v_ref[at, :]
+        k = gate_keys(a, gap_ref[...])
+        g = jnp.log1p(-k)
+        ld = ld_ref[b]
+        sums = split_dot(lower_b, g)
+        first, second = sums[63:64], sums[127:128]
+        ends = jnp.concatenate(
+            [jnp.broadcast_to(first, (64, 128)), jnp.broadcast_to(second, (64, 128))], axis=0
+        )
+        cum_f = sums + jnp.sum(lower_f * ld[0:1], axis=1, keepdims=True)
+        cum_b = ends - sums + g + jnp.sum(upper_f * ld[1:2], axis=1, keepdims=True)
+        cum = jnp.where(lane < 32, cum_f, cum_b)
+        c_ref[at, :] = cum
+        for h in range(2):
+            part = slice(64 * h, 64 * (h + 1))
+            cc = cum[part]
+            tot = jnp.where(lane1 < 32, cc[63:64], cc[0:1])
+            kd = (k[part] * jnp.exp(tot - cc)).astype(BF16)
+            st = dot(v[part], kd, TN)
+            tot8 = jnp.broadcast_to(tot, (8, 128))
+            tot8 = jnp.where(lanes(8) < 64, tot8, pltpu.roll(tot8, 64, 1))
+            chunk_s[2 * b + h] = st[:64] + pltpu.roll(st[64:], 64, 1)
+            chunk_t[2 * b + h] = tot8
+
     for t, copy in enumerate(copies):
         copy.wait()
-        start = rows * t
-        acc = jnp.zeros((rows, 224), F32)
-        acc_g = jnp.zeros((rows, 64), F32)
-        for k in range(8):
-            xk = x_ref[start : start + rows, 256 * k : 256 * (k + 1)]
-            acc += dot(xk, w_ref[k], NT)
-            acc_g += dot(xk, w2_ref[k], NT)
-        pre_v = acc[:, :128].astype(BF16)
-        pre_a = jnp.concatenate([acc[:, 128:], jnp.zeros((rows, 32), F32)], axis=1).astype(BF16)
-        a_ref[start : start + rows, :] = pre_a
-        v_ref[start : start + rows, :] = pre_v
-        glu = acc_g.astype(BF16).astype(F32)
-        gated_ref[start : start + rows, :] = (glu[:, 0:32] * sigmoid(glu[:, 32:64])).astype(BF16)
-        for b in range(rows // 128):
-            a = pre_a[128 * b : 128 * (b + 1)].astype(F32)
-            v = pre_v[128 * b : 128 * (b + 1)]
-            k = gate_keys(a, gap_ref[...])
-            g = jnp.log1p(-k)
-            ld = ld_ref[t * (rows // 128) + b]
-            cum_f = split_dot(lower_b, g) + jnp.sum(lower_f * ld[0:1], axis=1, keepdims=True)
-            cum_b = split_dot(upper_b, g) + jnp.sum(upper_f * ld[1:2], axis=1, keepdims=True)
-            cum = jnp.where(lane < 32, cum_f, cum_b)
-            c_ref[start + 128 * b : start + 128 * (b + 1), :] = cum
-            for h in range(2):
-                part = slice(64 * h, 64 * (h + 1))
-                cc = cum[part]
-                tot = jnp.where(lane1 < 32, cc[63:64], cc[0:1])
-                kd = (k[part] * jnp.exp(tot - cc)).astype(BF16)
-                st = dot(v[part], kd, TN)
-                tot8 = jnp.broadcast_to(tot, (8, 128))
-                tot8 = jnp.where(lanes(8) < 64, tot8, pltpu.roll(tot8, 64, 1))
-                idx = t * (rows // 64) + 2 * b + h
-                chunk_s[idx] = st[:64] + pltpu.roll(st[64:], 64, 1)
-                chunk_t[idx] = tot8
+        at = slice(rows * t, rows * (t + 1))
+        acc = project(x_ref, w_ref, at, 224)
+        if t:
+            for b in range(rows // 128):
+                gates((t - 1) * (rows // 128) + b)
+        v_ref[at, :] = acc[:, :128].astype(BF16)
+        a_ref[at, :] = jnp.concatenate([acc[:, 128:], jnp.zeros((rows, 32), F32)], axis=1).astype(BF16)
+    head = gate_product(project(x_ref, w2_ref, slice(0, 16), 64))
+    last = gate_product(project(x_ref, w2_ref, slice(total - 16, total), 64))
+    for b in range(total // 128 - rows // 128, total // 128):
+        gates(b)
 
     fwd = (lanes(64) % 64) < 32
     fwd8 = (lanes(8) % 64) < 32
@@ -184,40 +204,36 @@
             for p, q in ((i, j), (j, i)):
                 before_ref[p] = jnp.where(fwd, befores[p], befores[q]).astype(BF16)
                 offset_ref[p] = jnp.where(fwd8, offs[p], offs[q])
-    dec = jnp.exp(off)[0:1]
-    hi = dec.astype(BF16)
-    lo = (dec - hi.astype(F32)).astype(BF16)
+    dec = jnp.exp(off)
+    hi = dec.astype(BF16).astype(F32)
+    lo = dec - hi
+    fwd32 = (lanes(32) % 64) < 32
+    later = jnp.where(fwd32, s[0:32], pltpu.roll(s[32:64], 32, 1))
+    earlier = jnp.where(fwd32, pltpu.roll(s[0:32], 96, 1), s[32:64])
     row = lax.broadcasted_iota(jnp.int32, (16, 128), 0)
-    tail = jnp.where(row == 0, hi.astype(F32), jnp.where(row == 1, lo.astype(F32), 0.0)).astype(BF16)
-    s = s.astype(BF16)
-    head = gated_ref[0:16, :].astype(F32)
-    last = gated_ref[gated_ref.shape[0] - 16 :, :].astype(F32)
-    edge = jnp.concatenate([head, last, last, last], axis=1).astype(BF16)
+    edge = jnp.concatenate([head, last, last, last], axis=1)
+
+    def with_decay(hi, lo):
+        return jnp.where(lanes(16) < 64, edge, jnp.where(row == 0, hi[0:1], lo[0:1]))
+
+    later_tail = with_decay(hi, lo)
+    earlier_tail = with_decay(pltpu.roll(hi, 96, 1), pltpu.roll(lo, 96, 1))
     for i in range(8):
-        send_ref[i, :64, :] = s
-        send_ref[i, 64:80, :] = tail
-        send_ref[i, 80:96, :] = edge
+        ahead = jnp.where(i > z, 1, 0) > 0
+        send_ref[i, 0:32, :] = jnp.where(ahead, later, earlier).astype(BF16)
+        send_ref[i, 32:48, :] = jnp.where(ahead, later_tail, earlier_tail).astype(BF16)
 
 
 def local_kernel(
-    a_ref, v_ref, c_ref, gap_ref, before_ref, offset_ref, g_ref, taps_ref,
-    out_ref, qd_ref, conv_ref, edge_ref, pad,
+    x_hbm, w2_ref, a_ref, v_ref, c_ref, gap_ref, before_ref, offset_ref, taps_ref,
+    out_ref, qd_ref, conv_ref, edge_ref, x_ref, sems, pad,
 ):
-    n = g_ref.shape[0]
-    zeros = jnp.zeros((16, 32), F32)
-    pad[0:16, :] = zeros
-    pad[16 : 16 + n, :] = g_ref[...].astype(F32)
-    pad[16 + n : 32 + n, :] = zeros
-    taps = taps_ref[...]
-    for blk in range(n // 64):
-        acc = jnp.zeros((64, 32), F32)
-        for j in range(31):
-            acc += pad[64 * blk + j + 1 : 64 * blk + j + 65, :] * taps[j : j + 1, :]
-        conv_ref[blk] = jnp.concatenate([acc[16 * q : 16 * (q + 1)] for q in range(4)], axis=1).astype(BF16)
-        if blk == 0:
-            edge_ref[0] = acc[0:16]
-        if blk == n // 64 - 1:
-            edge_ref[1] = acc[48:64]
+    n = x_ref.shape[0]
+    copies = []
+    for t in range(n // TILE):
+        at = pl.ds(TILE * t, TILE)
+        copies.append(pltpu.make_async_copy(x_hbm.at[at], x_ref.at[at], sems.at[t]))
+        copies[-1].start()
     lower, upper = triangles()
     lane = lanes(128)
     for b in range(a_ref.shape[0] // 128):
@@ -243,6 +259,23 @@
             full = jnp.concatenate([sb, pltpu.roll(sb.astype(F32), 64, 1).astype(BF16)], axis=0)
             out_ref[to, :] = out[part] + dot(qh[part], full, NT)
             qd_ref[to, :] = (qg[part] * jnp.exp(offset_ref[2 * b + h][0:1])).astype(BF16)
+    zeros = jnp.zeros((16, 32), F32)
+    pad[0:16, :] = zeros
+    for t, copy in enumerate(copies):
+        copy.wait()
+        acc = project(x_ref, w2_ref, slice(TILE * t, TILE * (t + 1)), 64)
+        pad[16 + TILE * t : 16 + TILE * (t + 1), :] = gate_product(acc).astype(BF16).astype(F32)
+    pad[16 + n : 32 + n, :] = zeros
+    taps = taps_ref[...]
+    for blk in range(n // 64):
+        acc = jnp.zeros((64, 32), F32)
+        for j in range(31):
+            acc += pad[64 * blk + j + 1 : 64 * blk + j + 65, :] * taps[j : j + 1, :]
+        conv_ref[blk] = jnp.concatenate([acc[16 * q : 16 * (q + 1)] for q in range(4)], axis=1).astype(BF16)
+        if blk == 0:
+            edge_ref[0] = acc[0:16]
+        if blk == n // 64 - 1:
+            edge_ref[1] = acc[48:64]
 
 
 def merge_kernel(z_ref, recv_ref, local_ref, qd_ref, conv_ref, edge_ref, taps_ref, send_ref):
@@ -250,7 +283,7 @@
     heads = jnp.zeros((16, 128), F32)
     tails = jnp.zeros((16, 128), F32)
     for i in range(8):
-        other = recv_ref[i, 80:96, :].astype(F32)
+        other = recv_ref[i, 32:48, :].astype(F32)
         tails = jnp.where(i == z - 1, other, tails)
         heads = jnp.where(i == z + 1, other, heads)
     zeros = jnp.zeros((16, 32), F32)
@@ -266,13 +299,21 @@
     lane16 = lanes(16)
     fwd = (lanes(64) % 64) < 32
     fwd1 = (lanes(1) % 64) < 32
+    states, decays = [], []
+    for i in range(8):
+        packed = recv_ref[i, 0:32, :].astype(F32)
+        states.append((packed, pltpu.roll(packed, 96, 1), pltpu.roll(packed, 32, 1)))
+        parts = recv_ref[i, 32:48, :].astype(F32)
+        both = parts[0:8] + jnp.concatenate([parts[1:8], parts[0:1]], axis=0)
+        both = jnp.where(lanes(8) < 64, pltpu.roll(both, 64, 1), both)
+        decays.append((both[0:1], pltpu.roll(both, 32, 1)[0:1]))
     s = jnp.zeros((64, 128), F32)
     for i in range(8):
         j = 7 - i
-        sc = jnp.where(fwd, recv_ref[i, :64, :].astype(F32), recv_ref[j, :64, :].astype(F32))
-        di = recv_ref[i, 64:80, :].astype(F32)
-        dj = recv_ref[j, 64:80, :].astype(F32)
-        dec = jnp.where(fwd1, di[0:1] + di[1:2], dj[0:1] + dj[1:2])
+        sc_f = jnp.concatenate([states[i][0], states[i][1]], axis=0)
+        sc_b = jnp.concatenate([states[j][2], states[j][0]], axis=0)
+        sc = jnp.where(fwd, sc_f, sc_b)
+        dec = jnp.where(fwd1, decays[i][0], decays[j][1])
         pass_f = jnp.where(i < z, 1, 0)
         pass_b = jnp.where(j > z, 1, 0)
         passed = jnp.where(fwd, pass_f, pass_b) > 0
@@ -385,16 +426,18 @@
     rec_gains = gains[:, 0].reshape(4, 128)
     conv_gains = gains[:, 1].reshape(4, 128)
     n = seq.shape[0]
-    pre_a, pre_v, cum, gated, sent, before, offset = pl.pallas_call(
+    seq = pltpu.with_memory_space_constraint(seq, pltpu.HBM)
+    weights2 = near(weights2)
+    z = z.reshape(1).astype(jnp.int32)
+    pre_a, pre_v, cum, sent, before, offset = pl.pallas_call(
         states_kernel,
-        in_specs=[pl.BlockSpec(memory_space=pltpu.HBM)]
+        in_specs=[pl.BlockSpec(memory_space=pltpu.SMEM), pl.BlockSpec(memory_space=pltpu.HBM)]
         + [pl.BlockSpec(memory_space=pltpu.VMEM)] * 4,
         out_shape=[
             kept((n, 128), BF16),
             kept((n, 128), BF16),
             kept((n, 128), F32),
-            kept((n, 32), BF16),
-            kept((8, 96, 128), BF16),
+            kept((8, 48, 128), BF16),
             kept((16, 64, 128), BF16),
             kept((16, 8, 128), F32),
         ],
@@ -403,7 +446,7 @@
             pltpu.VMEM((16, 64, 128), F32), pltpu.VMEM((16, 8, 128), F32),
         ],
         compiler_params=SMALL, name="states",
-    )(pltpu.with_memory_space_constraint(seq, pltpu.HBM), near(weights), near(weights2), near(decays), near(gap))
+    )(z, seq, near(weights), weights2, near(decays), near(gap))
 
     arrived = lax.all_to_all(sent, Z, split_axis=0, concat_axis=0, tiled=True)
     local, decayed, convolved, edges = pl.pallas_call(
@@ -414,16 +457,24 @@
             kept((16, 16, 128), BF16),
             kept((2, 16, 32), F32),
         ],
-        scratch_shapes=[pltpu.VMEM((n + 32, 32), F32)],
+        in_specs=[pl.BlockSpec(memory_space=pltpu.HBM)]
+        + [pl.BlockSpec(memory_space=pltpu.VMEM)] * 8,
+        scratch_shapes=[
+            pltpu.VMEM((n, 2048), BF16), pltpu.SemaphoreType.DMA((n // TILE,)),
+            pltpu.VMEM((n + 32, 32), F32),
+        ],
         compiler_params=SMALL, name="local",
-    )(near(pre_a), near(pre_v), near(cum), near(gap), near(before), near(offset), near(gated), near(taps))
+    )(
+        seq, weights2, near(pre_a), near(pre_v), near(cum), near(gap), near(before), near(offset),
+        near(taps),
+    )
     merged = pl.pallas_call(
         merge_kernel,
         in_specs=[pl.BlockSpec(memory_space=pltpu.SMEM)]
         + [pl.BlockSpec(memory_space=pltpu.VMEM)] * 6,
         out_shape=kept((16, 80, 128), BF16),
         compiler_params=SMALL, name="merge",
-    )(z.reshape(1).astype(jnp.int32), near(arrived), near(local), near(decayed), near(convolved), near(edges), near(taps))
+    )(z, near(arrived), near(local), near(decayed), near(convolved), near(edges), near(taps))
     mine = lax.all_to_all(merged, (Y, C), split_axis=0, concat_axis=0, tiled=True)
     out_w = pltpu.with_memory_space_constraint(out_w, pltpu.HBM)
     out_w0 = pl.pallas_call(

time: 129 us -> 125 us (0.969)
  waiting for transfers between devices: 28.7 us -> 23.6 us
  Pallas kernels: 19.4 us -> 21.6 us
    all_to_all x1, waiting for transfers between devices: 7.55 us -> 2.46 us  [body(): arrived = lax.all_to_all(sent, Z, split_axis=0, concat_axis=0, tiled=True)]
    pallas_call x1, Pallas kernels: 2.32 us -> 6.29 us  [body(): pl.pallas_call(local_kernel, out_shape=[kept((n, 128), F32), kept((n, 128...]
    all_gather x1, waiting for transfers between devices: 3.54 us -> 5.48 us  [body(): lax.all_gather(out_cols, (C, Z), axis=0, tiled=True).reshape(2, 2048, 512)]
    all_to_all x1, waiting for transfers between devices: 6.24 us -> 4.3 us  [body(): lax.all_to_all(merged, (Y, C), split_axis=0, concat_axis=0, tiled=True)]
    pallas_call x1, Pallas kernels: 7.45 us -> 5.56 us  [body(): pl.pallas_call(states_kernel, in_specs=[pl.BlockSpec(memory_space=pltpu.S...]
  transfers between devices with their start and end apart: 6 -> 6, of which waited for: 4 -> 4; matrix products, arithmetic and copies ran while one was open for 1% -> 1% of each run, Pallas kernels for 11% -> 13%
where the time goes in v6:
time: 125 us
  starting transfers between devices  37.4 us (30%)
  blocking collectives  26.9 us (22%)
  waiting for transfers between devices  23.6 us (19%)
  Pallas kernels  21.6 us (17%)
  between operations  13.5 us (11%)
  local copies, waits for them, and re-layouts  1.73 us (1%)
    all_gather x1, blocking collectives, body(): weights = lax.all_gather(second, Z, axis=0)  25 us
    all_to_all x1, starting transfers between devices, body(): lax.all_to_all(second2, Z, split_axis=0, concat_axis=0, tiled=True)  14.1 us
    all_to_all x1, waiting for transfers between devices, body(): first = lax.all_to_all(first, Y, split_axis=0, concat_axis=0, tiled=True)  11.3 us
    all_to_all x1, starting transfers between devices, body(): lax.all_to_all(merged, (Y, C), split_axis=0, concat_axis=0, tiled=True)  10.1 us
    all_to_all x1, starting transfers between devices, body(): first = lax.all_to_all(first, Y, split_axis=0, concat_axis=0, tiled=True)  7.65 us
    pallas_call x1, Pallas kernels, body(): pl.pallas_call(local_kernel, out_shape=[kept((n, 128), F32), kept((n, 128...  6.29 us
    pallas_call x1, Pallas kernels, body(): pl.pallas_call(states_kernel, in_specs=[pl.BlockSpec(memory_space=pltpu.S...  5.56 us
    all_to_all x1, starting transfers between devices, body(): arrived = lax.all_to_all(sent, Z, split_axis=0, concat_axis=0, tiled=True)  5.5 us
  transfers between devices with their start and end apart: 6, of which 4 were waited for; matrix products, arithmetic and copies ran while one was open for 1% of the time, Pallas kernels for 13%

profile of v6, /device:TPU:1, one launch (start us, length us, event | category | flops | bytes accessed | tf_op | source)
XLA Modules:
  0.0 124.8 jit_solution(2461429975421706725)
XLA Ops:
  6.5 0.0 all-gather.6.cloned.1.call-start
  6.5 2.1 %start.1 = (bf16[64,2048]{1,0:T(8,128)(2,1)}, bf16[8,32,896]{2,1,0:T(8,128)(2,1)}) custom-call(bf16[64,2048]{1,0:T(8,128)(2,1)} %bitcast.26, f32[1,2048]{1,0:T(1,128)} %bitcast.30, bf16[32,256]{1,0:T(8,128)(2,1)} %rf_ref.1, bf16[32,256]{1,0:T(8,128)(2,1)} %rb_ref.1, bf16[32,256]{1,0:T(8,128)(2,1)} %rq_ref.1, bf16[32,256]{1,0:T(8,128)(2,1)} %cv_ref.1, ...), custom_call_target="tpu_custom_call" | custom-call | tf_op jit(solution)/shard_map/start/pallas_call | solution.py:399
  8.6 0.0 all-gather.6.cloned.1.call-update
  8.7 7.7 %all-to-all-start = ((bf16[8,32,896]{2,1,0:T(8,128)(2,1)}), bf16[8,32,896]{2,1,0:T(8,128)(2,1)S(1)}, u32[]{:S(2)}, u32[]{:S(2)}) async-start(bf16[8,32,896]{2,1,0:T(8,128)(2,1)} %get-tuple-element.24), calls=%async_computation | async-start | bytes 917504 | tf_op jit(solution)/shard_map/all_to_all | solution.py:408
  16.3 0.0 all-gather.8.cloned.1.call-start
  16.4 0.8 reshape.25
  17.2 0.8 reshape.23
  18.0 0.1 reshape.24
  18.1 11.3 %all-to-all-done.first_ref = bf16[8,32,896]{2,1,0:T(8,128)(2,1)S(1)} async-done(((bf16[8,32,896]{2,1,0:T(8,128)(2,1)}), bf16[8,32,896]{2,1,0:T(8,128)(2,1)S(1)}, u32[]{:S(2)}, u32[]{:S(2)}) %all-to-all-start) | async-done | bytes 458784 | tf_op jit(solution)/shard_map/all_to_all | solution.py:408
  29.4 1.0 second.1
  30.4 0.0 all-gather.8.cloned.1.call-update
  30.4 14.1 %all-to-all-start.1 = ((bf16[8,64,256]{2,1,0:T(8,128)(2,1)}), bf16[8,64,256]{2,1,0:T(8,128)(2,1)S(1)}, u32[]{:S(2)}, u32[]{:S(2)}) async-start(bf16[8,64,256]{2,1,0:T(8,128)(2,1)} %get-tuple-element.26), calls=%async_computation.1 | async-start | bytes 524288 | tf_op jit(solution)/shard_map/all_to_all | solution.py:421
  44.5 25.0 %all-gather = bf16[1792,256]{1,0:T(8,128)(2,1)S(1)} all-gather(bf16[224,256]{1,0:T(8,128)(2,1)S(1)} %get-tuple-element.25), channel_id=2, replica_groups=mesh['sp_0'=8,'sp_1'=8,'fs'=4,'tp'=2] {'sp_0'}, dimensions={0}, use_global_device_ids=true | all-gather | bytes 1032192 | tf_op jit(solution)/shard_map/all_gather | solution.py:422
  69.6 0.0 all-to-all-done.1.w2_ref
  69.6 0.0 all-gather.6.cloned.1.call-done.x_hbm
  69.6 5.6 %states.1 = (bf16[1024,128]{1,0:T(8,128)(2,1)S(1)}, bf16[1024,128]{1,0:T(8,128)(2,1)S(1)}, f32[1024,128]{1,0:T(8,128)S(1)}, bf16[8,48,128]{2,1,0:T(8,128)(2,1)},...) custom-call(s32[1]{0:T(128)} %bitcast.z_ref, bf16[1024,2048]{1,0:T(8,128)(2,1)} %all-gather.6.cloned.1.call-done.x_hbm, ...), custom_call_target="tpu_custom_call" | custom-call | tf_op jit(solution)/shard_map/states/pallas_call | solution.py:432
  75.1 0.0 copy-start
  75.1 0.0 copy-start.1
  75.2 5.5 %all-to-all-start.2 = ((bf16[8,48,128]{2,1,0:T(8,128)(2,1)}), bf16[8,48,128]{2,1,0:T(8,128)(2,1)S(1)}, u32[]{:S(2)}, u32[]{:S(2)}) async-start(bf16[8,48,128]{2,1,0:T(8,128)(2,1)} %get-tuple-element.29), calls=%async_computation.2 | async-start | bytes 196608 | tf_op jit(solution)/shard_map/all_to_all | solution.py:451
  80.7 6.3 %local.1 = (f32[1024,128]{1,0:T(8,128)S(1)}, bf16[1024,128]{1,0:T(8,128)(2,1)S(1)}, bf16[16,16,128]{2,1,0:T(8,128)(2,1)S(1)}, f32[2,16,32]{2,1,0:T(8,128)S(1)}) custom-call(bf16[1024,2048]{1,0:T(8,128)(2,1)} %all-gather.6.cloned.1.call-done.x_hbm, bf16[8,64,256]{2,1,0:T(8,128)(2,1)S(1)} %all-to-all-done.1.w2_ref, ...), custom_call_target="tpu_custom_call" | custom-call | tf_op jit(solution)/shard_map/local/pallas_call | solution.py:452
  87.0 2.5 %all-to-all-done.2.recv_ref = bf16[8,48,128]{2,1,0:T(8,128)(2,1)S(1)} async-done(((bf16[8,48,128]{2,1,0:T(8,128)(2,1)}), bf16[8,48,128]{2,1,0:T(8,128)(2,1)S(1)}, u32[]{:S(2)}, u32[]{:S(2)}) %all-to-all-start.2) | async-done | bytes 98336 | tf_op jit(solution)/shard_map/all_to_all | solution.py:451
  89.4 1.4 %merge.1 = bf16[16,80,128]{2,1,0:T(8,128)(2,1)} custom-call(s32[1]{0:T(128)} %bitcast.z_ref, bf16[8,48,128]{2,1,0:T(8,128)(2,1)S(1)} %all-to-all-done.2.recv_ref, f32[1024,128]{1,0:T(8,128)S(1)} %get-tuple-element.36.local_ref, bf16[1024,128]{1,0:T(8,128)(2,1)S(1)} %get-tuple-element.37.qd_ref, bf16[16,16,128]{2,1,0:T(8,128)(2,1)S(1)} %get-tuple-element.38.conv_ref, ...), custom_call_target="tpu_custom_call" | custom-call | tf_op jit(solution)/shard_map/merge/pallas_call | solution.py:471
  90.9 10.1 %all-to-all-start.3 = ((bf16[16,80,128]{2,1,0:T(8,128)(2,1)}), bf16[16,80,128]{2,1,0:T(8,128)(2,1)S(1)}, u32[]{:S(2)}, u32[]{:S(2)}) async-start(bf16[16,80,128]{2,1,0:T(8,128)(2,1)} %merge.1), calls=%async_computation.3 | async-start | bytes 655360 | tf_op jit(solution)/shard_map/all_to_all | solution.py:478
  101.0 0.0 copy-done
  101.0 0.0 copy-done.1
  101.0 1.8 %all-gather.2 = f32[2,2,256]{2,1,0:T(2,128)S(1)} all-gather(f32[1,2,256]{2,1,0:T(2,128)S(1)} %maximum_bitcast_fusion), channel_id=3, replica_groups=mesh['sp_0'=8,'sp_1'=8,'fs'=4,'tp'=2] {'tp'}, dimensions={0}, use_global_device_ids=true | all-gather | bytes 6144 | tf_op jit(solution)/shard_map/all_gather | solution.py:425
  102.8 5.5 %all-gather.8.cloned.1.call-done = bf16[4096,512]{1,0:T(8,128)(2,1)} async-done(((bf16[256,512]{1,0:T(8,128)(2,1)}), bf16[4096,512]{1,0:T(8,128)(2,1)}) %all-gather.8.cloned.1.call-update) | async-done | bytes 4194320 | tf_op jit(solution)/shard_map/all_gather | solution.py:423
  108.3 1.6 %load.1.w0_ref = bf16[2048,512]{1,0:T(8,128)(2,1)S(1)} custom-call(bf16[2,2048,512]{2,1,0:T(8,128)(2,1)} %bitcast.24), custom_call_target="tpu_custom_call" | custom-call | tf_op jit(solution)/shard_map/load/pallas_call | solution.py:480
  109.9 4.3 %all-to-all-done.3.recv_ref = bf16[16,80,128]{2,1,0:T(8,128)(2,1)S(1)} async-done(((bf16[16,80,128]{2,1,0:T(8,128)(2,1)}), bf16[16,80,128]{2,1,0:T(8,128)(2,1)S(1)}, u32[]{:S(2)}, u32[]{:S(2)}) %all-to-all-start.3) | async-done | bytes 327712 | tf_op jit(solution)/shard_map/all_to_all | solution.py:478
  114.2 3.7 %output.1 = bf16[64,2048]{1,0:T(8,128)(2,1)} custom-call(bf16[16,80,128]{2,1,0:T(8,128)(2,1)S(1)} %all-to-all-done.3.recv_ref, f32[4,128]{1,0:T(4,128)S(1)} %bitcast.23, f32[4,128]{1,0:T(4,128)S(1)} %bitcast.22, bf16[2048,512]{1,0:T(8,128)(2,1)S(1)} %load.1.w0_ref, bf16[2,2048,512]{2,1,0:T(8,128)(2,1)} %bitcast.25), custom_call_target="tpu_custom_call" | custom-call | tf_op jit(solution)/shard_map/output/pallas_call | solution.py:488
  (7 shorter events, 0.1 us)
Async XLA Ops:
  6.5 63.0 %all-gather.6.cloned.1.call-start = ((), (), s32[]{:S(2)}) async-start(), calls=%async_computation.4 | async-start | bytes 4456448 | tf_op jit(solution)/shard_map/all_gather | solution.py:407
  8.7 20.8 %all-to-all-start = ((bf16[8,32,896]{2,1,0:T(8,128)(2,1)}), bf16[8,32,896]{2,1,0:T(8,128)(2,1)S(1)}, u32[]{:S(2)}, u32[]{:S(2)}) async-start(bf16[8,32,896]{2,1,0:T(8,128)(2,1)} %get-tuple-element.24), calls=%async_computation | async-start | bytes 917504 | tf_op jit(solution)/shard_map/all_to_all | solution.py:408
  16.3 92.0 %all-gather.8.cloned.1.call-start = ((), (), s32[]{:S(2)}) async-start(), calls=%async_computation.5 | async-start | bytes 4456448 | tf_op jit(solution)/shard_map/all_gather | solution.py:423
  30.4 39.2 %all-to-all-start.1 = ((bf16[8,64,256]{2,1,0:T(8,128)(2,1)}), bf16[8,64,256]{2,1,0:T(8,128)(2,1)S(1)}, u32[]{:S(2)}, u32[]{:S(2)}) async-start(bf16[8,64,256]{2,1,0:T(8,128)(2,1)} %get-tuple-element.26), calls=%async_computation.1 | async-start | bytes 524288 | tf_op jit(solution)/shard_map/all_to_all | solution.py:421
  75.1 25.8 %copy-start = (f32[256]{0:T(256)S(1)}, f32[256]{0:T(256)}, u32[]{:S(2)}) copy-start(f32[256]{0:T(256)} %param.27) | copy-start | bytes 3076
  75.1 25.8 %copy-start.1 = (f32[256]{0:T(256)S(1)}, f32[256]{0:T(256)}, u32[]{:S(2)}) copy-start(f32[256]{0:T(256)} %param.23) | copy-start | bytes 3076
  75.2 14.3 %all-to-all-start.2 = ((bf16[8,48,128]{2,1,0:T(8,128)(2,1)}), bf16[8,48,128]{2,1,0:T(8,128)(2,1)S(1)}, u32[]{:S(2)}, u32[]{:S(2)}) async-start(bf16[8,48,128]{2,1,0:T(8,128)(2,1)} %get-tuple-element.29), calls=%async_computation.2 | async-start | bytes 196608 | tf_op jit(solution)/shard_map/all_to_all | solution.py:451
  90.9 23.4 %all-to-all-start.3 = ((bf16[16,80,128]{2,1,0:T(8,128)(2,1)}), bf16[16,80,128]{2,1,0:T(8,128)(2,1)S(1)}, u32[]{:S(2)}, u32[]{:S(2)}) async-start(bf16[16,80,128]{2,1,0:T(8,128)(2,1)} %merge.1), calls=%async_computation.3 | async-start | bytes 655360 | tf_op jit(solution)/shard_map/all_to_all | solution.py:478
Sparse Core Ops, SparseCore 0:
  9.4 50.2 all-gather.5
  61.8 46.4 all-gather.7
